TPU v7x, 512 devices: a 4x2x32 block of a 4x8x32 slice. The times are simulated.
512 devices in a mesh: grp: 2 (over y), kv: 64 (over z, core), tp: 4 (over x).
Axes of the slice: x: 4, y: 2, z: 32, core: 2. Of those that a mesh axis runs over, the one named last changes fastest.
The devices are a block of a 4x8x32 slice.
Arguments:
- hidden_states: bfloat16 [128, 4096], P('grp', 'kv'), parts along dimension 0, may hold values from -6 to 6
- w_query: bfloat16 [4096, 2048], P('kv', 'tp'), may hold values from -0.09375 to 0.09375
- w_key: bfloat16 [4096, 2048], P('kv', 'tp'), may hold values from -0.09375 to 0.09375
- w_value: bfloat16 [4096, 2048], P('kv', 'tp'), may hold values from -0.09375 to 0.09375
- query_gain: float32 [64], replicated, may hold values from 1.2 to 1.8
- key_gain: float32 [64], replicated, may hold values from 1.2 to 1.8
- lambda_head: float32 [16], P('tp'), may hold values from 0.3 to 0.8
- head_gain: float32 [128], replicated, may hold values from 0.1 to 1.9
- w_output: bfloat16 [2048, 4096], P('tp', 'kv'), may hold values from -0.125 to 0.125
- cache_keys: bfloat16 [8, 16384, 16, 128], P('grp', 'kv', 'tp'), parts along dimension 0
- cache_values: bfloat16 [8, 16384, 16, 128], P('grp', 'kv', 'tp'), parts along dimension 0, may hold values from -6 to 6
- past_lengths: int32 [8], P('grp'), parts along dimension 0, may hold values from 8192 to 16352
- accepted: int32 [8], P('grp'), parts along dimension 0, may hold values from 1 to 8
- parents: int32 [8, 16], P('grp'), parts along dimension 0, may hold values from -1 to 14, as said below
Outputs:
- attended: bfloat16 [128, 4096], P(('grp', 'tp'), 'kv'), parts along dimension 0
- new_cache_keys: bfloat16 [8, 16384, 16, 128], P('grp', 'kv', 'tp'), parts along dimension 0
- new_cache_values: bfloat16 [8, 16384, 16, 128], P('grp', 'kv', 'tp'), parts along dimension 0
There are 2 independent parts, one for each index of `grp`. A program takes and returns all parts, laid end to end along the dimension named above; an argument that names none is the same for every part. Nothing has to cross between parts.
Inputs may be any that keep to these rules, and one draw needn't show every extreme that they name: parents[s, 0] is -1 and parents[s, j] lies in 0 to j - 1 for j >= 1.
All inputs are finite; a program needn't handle non-finite values.
Results may differ from a plain program's by a relative error of at most 0.0095.
The roundings to bfloat16 on the way count: a program that leaves them out, or rounds other values in their place, can miss the bound.
Values may be sent and summed in bfloat16 or wider, within the bound.
No kernel may reach another device: no remote copies, remote signals or barrier semaphores. Data moves between devices by JAX's collectives and lax.ppermute only.
A program may use at most 64 MiB of HBM per device.

v0:
```python
import math

import jax
import jax.numpy as jnp
from jax import lax
from jax.sharding import PartitionSpec as P

epsilon = 1e-06
floor_value = -1e30


def in_blocks(x, dim, devices):
    dims = x.shape
    blocks = x.reshape(*dims[:dim], devices, dims[dim] // devices, *dims[dim + 1 :])
    return jnp.moveaxis(blocks, dim, 0)


def summed_on_arrival(x, axis, dim):
    devices = lax.axis_size(axis)
    blocks = lax.all_to_all(in_blocks(x, dim, devices), axis, 0, 0, tiled=True)
    return jnp.sum(blocks, axis=0)


def sent_together(arrays, axis, dim, along):
    ends, at = ([], 0)
    for a in arrays[:-1]:
        at += a.shape[along]
        ends.append(at)
    both = jnp.concatenate(arrays, axis=along)
    return tuple(jnp.split(summed_on_arrival(both, axis, dim), ends, axis=along))


def side_by_side(arrays, axis, dim, along):
    ends, at = ([], 0)
    for a in arrays[:-1]:
        at += a.shape[along]
        ends.append(at)
    both = jnp.concatenate(arrays, axis=along)
    return tuple(jnp.split(lax.all_gather(both, axis, axis=dim, tiled=True), ends, axis=along))


def side_by_side_2(arrays, axis, split_dim, concat_dim, along):
    widths = [math.prod(a.shape[along:]) for a in arrays]
    both = jnp.concatenate(
        [a.reshape(*a.shape[:along], w) for a, w in zip(arrays, widths)], axis=along
    )
    whole = lax.all_to_all(both, axis, split_axis=split_dim, concat_axis=concat_dim, tiled=True)
    blocks = jnp.split(whole, [sum(widths[:k]) for k in range(1, len(widths))], axis=along)
    return tuple(
        (b.reshape(*whole.shape[:along], *a.shape[along:]) for a, b in zip(arrays, blocks))
    )


def joined_along(blocks, dim):
    dims = list(blocks.shape[1:])
    dims[dim] *= blocks.shape[0]
    return jnp.moveaxis(blocks, 0, dim).reshape(dims)


def from_everyone(x, axis):
    copies = jnp.broadcast_to(x, (lax.axis_size(axis), *x.shape))
    return lax.all_to_all(copies, axis, split_axis=0, concat_axis=0, tiled=True)


def gathered_copies(x, axis, dim):
    return joined_along(from_everyone(x, axis), dim)


def sum_at_owner(x, axis, dim):
    blocks = in_blocks(x, dim, lax.axis_size(axis))
    arrived = lax.all_to_all(blocks, axis, split_axis=0, concat_axis=0, tiled=True)
    return arrived.astype(jnp.float32).sum(axis=0)


def group_norm(projected, gain_vector):
    shaped = projected.reshape(projected.shape[0], -1, gain_vector.shape[0])
    factor = lax.rsqrt(jnp.mean(shaped * shaped, axis=-1, keepdims=True) + epsilon)
    return (shaped * factor * gain_vector).reshape(projected.shape[0], -1)


def finish_rows(query_terms, key_terms, value_terms, query_gain, key_gain):
    return (
        group_norm(query_terms, query_gain).astype(jnp.bfloat16),
        group_norm(key_terms, key_gain).astype(jnp.bfloat16),
        value_terms.astype(jnp.bfloat16),
    )


def ancestry(parents):
    proposals = parents.shape[1]
    orders = jnp.arange(proposals, dtype=jnp.int32)
    reached = (parents[:, :, None] == orders[None, None, :]).astype(jnp.float32)
    reached = reached + (orders[:, None] == orders[None, :]).astype(jnp.float32)[None]
    for repeat in range((proposals - 1).bit_length()):
        reached = jnp.minimum(
            jnp.einsum("sjk,ski->sji", reached, reached, precision=lax.Precision.HIGHEST), 1.0
        )
    return reached


def partial_softmax(scores, visible, values, tokens):
    masked = jnp.where(visible, scores, floor_value)
    block_max = jnp.max(masked, axis=-1)
    weights = jnp.where(visible, jnp.exp(masked - block_max[..., None]), 0.0)
    block_sum = jnp.sum(weights, axis=-1)
    block_acc = jnp.einsum(
        "sqhcp,sphv->sqhcv",
        weights.astype(jnp.bfloat16),
        values,
        preferred_element_type=jnp.float32,
    )
    heads = block_max.shape[2]
    return (
        block_max.reshape(tokens, heads, 2),
        block_sum.reshape(tokens, heads, 2),
        block_acc.reshape(tokens, heads, 2, block_acc.shape[-1]),
    )


def finish_heads(totals, combined, lambda_head, head_gain):
    first_map = combined[:, :, 0] / totals[:, :, 0:1]
    second_map = combined[:, :, 1] / totals[:, :, 1:2]
    mixture = first_map - lambda_head[None, :, None] * second_map
    factor = lax.rsqrt(jnp.mean(mixture * mixture, axis=-1, keepdims=True) + epsilon)
    return (mixture * factor * head_gain).astype(jnp.bfloat16).reshape(mixture.shape[0], -1)


def on_device(
    hidden_states,
    w_query,
    w_key,
    w_value,
    query_gain,
    key_gain,
    lambda_head,
    head_gain,
    w_output,
    cache_keys,
    cache_values,
    past_lengths,
    accepted,
    parents,
):
    seq_count, proposals = parents.shape
    tokens = hidden_states.shape[0]
    heads = lambda_head.shape[0]
    head_dim = query_gain.shape[0]
    value_dim = head_gain.shape[0]
    positions_dev = cache_keys.shape[1]
    query_terms = jnp.dot(hidden_states, w_query, preferred_element_type=jnp.float32)
    key_terms = jnp.dot(hidden_states, w_key, preferred_element_type=jnp.float32)
    value_terms = jnp.dot(hidden_states, w_value, preferred_element_type=jnp.float32)
    shares = sent_together((query_terms, key_terms, value_terms), "kv", 0, 1)
    own_query, own_key, own_value = finish_rows(
        shares[0], shares[1], shares[2], query_gain, key_gain
    )
    queries, keys_new, values_new = side_by_side((own_query, own_key, own_value), "kv", 0, 1)
    queries = queries.reshape(seq_count, proposals, heads, 2, head_dim)
    keys_new = keys_new.reshape(seq_count, proposals, heads, 2 * head_dim)
    values_new = values_new.reshape(seq_count, proposals, heads, value_dim)
    score_scale = head_dim ** (-0.5)
    offset = lax.axis_index("kv") * positions_dev
    positions = offset + jnp.arange(positions_dev, dtype=jnp.int32)
    valid_len = past_lengths + accepted
    cache_split = cache_keys.reshape(seq_count, positions_dev, heads, 2, head_dim)
    scores = (
        jnp.einsum("sqhcd,sphcd->sqhcp", queries, cache_split, preferred_element_type=jnp.float32)
        * score_scale
    )
    visible = (positions[None, :] < valid_len[:, None])[:, None, None, None, :]
    cache_part = partial_softmax(scores, visible, cache_values, tokens)
    tree_keys = keys_new.reshape(seq_count, proposals, heads, 2, head_dim)
    tree_scores = (
        jnp.einsum("sqhcd,skhcd->sqhck", queries, tree_keys, preferred_element_type=jnp.float32)
        * score_scale
    )
    reached = ancestry(parents)
    tree_part = partial_softmax(
        tree_scores, (reached > 0.5)[:, :, None, None, :], values_new, tokens
    )
    row_count = tokens // lax.axis_size("kv")
    arrived = side_by_side_2(
        (cache_part[0][None], cache_part[1][None], cache_part[2][None]), "kv", 1, 0, 4
    )
    first_row = lax.axis_index("kv") * row_count
    own_tree = tuple(
        (lax.dynamic_slice_in_dim(member, first_row, row_count, 0) for member in tree_part)
    )
    highest = jnp.maximum(jnp.max(arrived[0], axis=0), own_tree[0])
    factors = jnp.exp(arrived[0] - highest[None])
    tree_factor = jnp.exp(own_tree[0] - highest)
    totals = jnp.sum(arrived[1] * factors, axis=0) + own_tree[1] * tree_factor
    combined = (
        jnp.sum(arrived[2] * factors[..., None], axis=0) + own_tree[2] * tree_factor[..., None]
    )
    own_heads = finish_heads(totals, combined, lambda_head, head_gain)
    head_out = gathered_copies(own_heads, "kv", 0)
    attended = sum_at_owner(
        jnp.dot(head_out, w_output, preferred_element_type=jnp.float32).astype(jnp.bfloat16),
        "tp",
        0,
    ).astype(jnp.bfloat16)
    slots = jnp.arange(proposals, dtype=jnp.int32)
    landing = positions[None, :, None] - valid_len[:, None, None] == slots[None, None, :]
    onehot = landing.astype(jnp.bfloat16)
    written = jnp.any(landing, axis=2)[:, :, None, None]
    placed_keys = jnp.einsum(
        "spj,sjhd->sphd", onehot, keys_new, preferred_element_type=jnp.float32
    ).astype(jnp.bfloat16)
    placed_values = jnp.einsum(
        "spj,sjhd->sphd", onehot, values_new, preferred_element_type=jnp.float32
    ).astype(jnp.bfloat16)
    new_cache_keys = jnp.where(written, placed_keys, cache_keys)
    new_cache_values = jnp.where(written, placed_values, cache_values)
    return (attended, new_cache_keys, new_cache_values)


def solution(mesh):
    placed = (
        P("grp", "kv"),
        P("kv", "tp"),
        P("kv", "tp"),
        P("kv", "tp"),
        P(),
        P(),
        P("tp"),
        P(),
        P("tp", "kv"),
        P("grp", "kv", "tp", None),
        P("grp", "kv", "tp", None),
        P("grp"),
        P("grp"),
        P("grp", None),
    )
    return jax.shard_map(
        on_device,
        mesh=mesh,
        in_specs=placed,
        out_specs=(P(("grp", "tp"), "kv"), P("grp", "kv", "tp", None), P("grp", "kv", "tp", None)),
        check_vma=False,
    )
```

profile of v0, /device:TPU:40, one launch (start us, length us, event | category | flops | bytes accessed | tf_op | source)
XLA Modules:
  0.0 284.9 jit_solution(11622419342932096347)
XLA Ops:
  0.6 0.8 copy-done
  1.5 0.8 fusion.59
  2.3 1.0 fusion.60
  3.3 1.0 fusion.61
  4.4 1.2 copy.243
  5.6 47.3 %all-to-all-start = ((f32[64,1,1536]{2,1,0:T(1,128)}), f32[64,1,1536]{2,1,0:T(1,128)S(1)}, u32[]{:S(2)}, u32[]{:S(2)}) async-start(f32[64,1,1536]{2,1,0:T(1,128)} %copy.243), calls=%async_computation | async-start | bytes 786432 | tf_op jit(solution)/shard_map/all_to_all | solution.py:20
  53.1 0.6 copy.244
  53.8 52.0 %all-to-all-done = f32[64,1,1536]{2,1,0:T(1,128)S(1)} async-done(((f32[64,1,1536]{2,1,0:T(1,128)}), f32[64,1,1536]{2,1,0:T(1,128)S(1)}, u32[]{:S(2)}, u32[]{:S(2)}) %all-to-all-start) | async-done | bytes 393248 | tf_op jit(solution)/shard_map/all_to_all | solution.py:20
  105.8 0.3 reduce_sum.90
  106.2 0.1 reduce_sum.92
  106.9 53.9 %all-gather = bf16[64,1,1536]{2,1,0:T(2,128)(2,1)S(1)} all-gather(bf16[1,1,1536]{2,1,0:T(2,128)(2,1)S(1)} %maximum_bitcast_fusion.1), channel_id=1, replica_groups=mesh['grp'=2,'kv'=64,'tp'=4] {'kv'}, dimensions={0}, use_global_device_ids=true | all-gather | bytes 199680 | tf_op jit(solution)/shard_map/all_gather | solution.py:39
  160.9 0.1 reshape.455
  161.0 0.4 fusion.57
  161.4 0.3 fusion.10
  161.7 0.2 reshape_broadcast_in_dim_reshape.9
  161.8 1.6 convolution_bitcast_fusion.1
  163.5 0.2 reshape_broadcast_in_dim_reshape.8
  163.6 0.3 pad_maximum_fusion
  164.0 1.2 copy.252
  165.2 8.2 %all-to-all-start.1 = ((f32[1,64,4,2,130]{4,3,2,0,1:T(2,128)}), f32[1,64,4,2,130]{4,3,2,0,1:T(2,128)S(1)}, u32[]{:S(2)}, u32[]{:S(2)}) async-start(f32[1,64,4,2,130]{4,3,2,0,1:T(2,128)} %copy.252), calls=%async_computation.1 | async-start | bytes 1048576 | tf_op jit(solution)/shard_map/all_to_all | solution.py:47
  173.4 0.2 convolution_minimum_fusion.3
  173.6 0.2 convolution_minimum_fusion.2
  173.8 0.2 convolution_minimum_fusion.1
  173.9 0.2 fusion.6
  174.2 0.1 reshape_reshape.3
  174.3 0.2 fusion.58
  174.6 0.1 copy.259
  174.8 0.1 copy.282
  175.0 0.2 convolution_bitcast_fusion
  175.3 0.1 copy.287
  175.4 62.1 %all-to-all-done.1 = f32[1,64,4,2,130]{4,3,2,0,1:T(2,128)S(1)} async-done(((f32[1,64,4,2,130]{4,3,2,0,1:T(2,128)}), f32[1,64,4,2,130]{4,3,2,0,1:T(2,128)S(1)}, u32[]{:S(2)}, u32[]{:S(2)}) %all-to-all-start.1) | async-done | bytes 266272 | tf_op jit(solution)/shard_map/all_to_all | solution.py:47
  237.6 0.8 copy.253
  238.5 0.2 fusion.45
  238.7 0.4 fusion.8
  239.7 0.5 broadcast.246
  240.2 1.0 reduce.19
  241.3 0.7 reshape.483
  241.9 6.7 %all-to-all-start.2 = ((bf16[64,2,256]{2,1,0:T(2,128)(2,1)}), bf16[64,2,256]{2,1,0:T(2,128)(2,1)S(1)}, u32[]{:S(2)}, u32[]{:S(2)}) async-start(bf16[64,2,256]{2,1,0:T(2,128)(2,1)} %reshape.483), calls=%async_computation.2 | async-start | bytes 131072 | tf_op jit(solution)/shard_map/all_to_all | solution.py:62
  248.7 0.5 fusion.1
  249.2 24.2 %all-to-all-done.2 = bf16[64,2,256]{2,1,0:T(2,128)(2,1)S(1)} async-done(((bf16[64,2,256]{2,1,0:T(2,128)(2,1)}), bf16[64,2,256]{2,1,0:T(2,128)(2,1)S(1)}, u32[]{:S(2)}, u32[]{:S(2)}) %all-to-all-start.2) | async-done | bytes 65568 | tf_op jit(solution)/shard_map/all_to_all | solution.py:62
  273.5 0.1 convolution_convert_fusion.2
  273.6 0.7 reshape.485
  274.3 4.6 %all-to-all-start.3 = ((bf16[4,2,512]{2,1,0:T(2,128)(2,1)}), bf16[4,2,512]{2,1,0:T(2,128)(2,1)S(1)}, u32[]{:S(2)}, u32[]{:S(2)}) async-start(bf16[4,2,512]{2,1,0:T(2,128)(2,1)} %reshape.485), calls=%async_computation.3 | async-start | bytes 16384 | tf_op jit(solution)/shard_map/all_to_all | solution.py:71
  278.9 0.5 fusion
  279.4 1.8 copy.272
  281.2 1.8 copy.273
  283.0 1.3 all-to-all-done.3
  284.3 0.6 reduce_sum.101
  (76 shorter events, 2.5 us)
Async XLA Ops:
  0.6 0.8 copy-start
  4.3 48.6 %copy-start.5 = (f32[64]{0:T(128)S(1)}, f32[64]{0:T(128)}, u32[]{:S(2)}) copy-start(f32[64]{0:T(128)} %param.18) | copy-start | bytes 772
  4.3 48.6 %copy-start.6 = (f32[64]{0:T(128)S(1)}, f32[64]{0:T(128)}, u32[]{:S(2)}) copy-start(f32[64]{0:T(128)} %param.19) | copy-start | bytes 772
  4.4 48.7 %copy-start.1 = (bf16[4,256,4,128]{3,2,1,0:T(4,128)(2,1)S(1)}, bf16[4,256,4,128]{3,2,1,0:T(4,128)(2,1)}, u32[]{:S(2)}) copy-start(bf16[4,256,4,128]{3,2,1,0:T(4,128)(2,1)} %param.23) | copy-start | bytes 3145732
  5.6 100.3 %all-to-all-start = ((f32[64,1,1536]{2,1,0:T(1,128)}), f32[64,1,1536]{2,1,0:T(1,128)S(1)}, u32[]{:S(2)}, u32[]{:S(2)}) async-start(f32[64,1,1536]{2,1,0:T(1,128)} %copy.243), calls=%async_computation | async-start | bytes 786432 | tf_op jit(solution)/shard_map/all_to_all | solution.py:20
  53.1 0.7 copy-start.9
  53.1 0.7 copy-start.10
  164.0 9.4 %copy-start.8 = (s32[4,16]{1,0:T(4,128)S(1)}, s32[4,16]{1,0:T(4,128)}, u32[]{:S(2)}) copy-start(s32[4,16]{1,0:T(4,128)} %param.27) | copy-start | bytes 772
  165.2 72.4 %all-to-all-start.1 = ((f32[1,64,4,2,130]{4,3,2,0,1:T(2,128)}), f32[1,64,4,2,130]{4,3,2,0,1:T(2,128)S(1)}, u32[]{:S(2)}, u32[]{:S(2)}) async-start(f32[1,64,4,2,130]{4,3,2,0,1:T(2,128)} %copy.252), calls=%async_computation.1 | async-start | bytes 1048576 | tf_op jit(solution)/shard_map/all_to_all | solution.py:47
  175.4 63.9 %copy-start.3 = (f32[4]{0:T(128)S(1)}, f32[4]{0:T(128)}, u32[]{:S(2)}) copy-start(f32[4]{0:T(128)} %param.20) | copy-start | bytes 52
  238.3 1.3 copy-start.4
  239.0 9.7 %copy-start.7 = (bf16[4,256,4,128]{3,2,1,0:T(4,128)(2,1)S(1)}, bf16[4,256,4,128]{3,2,1,0:T(4,128)(2,1)}, u32[]{:S(2)}) copy-start(bf16[4,256,4,128]{3,2,1,0:T(4,128)(2,1)} %param.24) | copy-start | bytes 3145732
  241.9 31.5 %all-to-all-start.2 = ((bf16[64,2,256]{2,1,0:T(2,128)(2,1)}), bf16[64,2,256]{2,1,0:T(2,128)(2,1)S(1)}, u32[]{:S(2)}, u32[]{:S(2)}) async-start(bf16[64,2,256]{2,1,0:T(2,128)(2,1)} %reshape.483), calls=%async_computation.2 | async-start | bytes 131072 | tf_op jit(solution)/shard_map/all_to_all | solution.py:62
  248.7 24.8 %copy-start.2 = (bf16[512,64]{0,1:T(8,128)(2,1)S(1)}, bf16[512,64]{0,1:T(8,128)(2,1)}, u32[]{:S(2)}) copy-start(bf16[512,64]{0,1:T(8,128)(2,1)} %param.22) | copy-start | bytes 196612
  274.3 9.9 %all-to-all-start.3 = ((bf16[4,2,512]{2,1,0:T(2,128)(2,1)}), bf16[4,2,512]{2,1,0:T(2,128)(2,1)S(1)}, u32[]{:S(2)}, u32[]{:S(2)}) async-start(bf16[4,2,512]{2,1,0:T(2,128)(2,1)} %reshape.485), calls=%async_computation.3 | async-start | bytes 16384 | tf_op jit(solution)/shard_map/all_to_all | solution.py:71
where the time goes:
time: 286 us; the launch traced here: 285 us
  waiting for transfers between devices  140 us (49%)
  starting transfers between devices  66.7 us (23%)
  blocking collectives  53.9 us (19%)
  local copies, waits for them, and re-layouts  12.6 us (4%)
  matrix products  7.11 us (2%)
  other arithmetic  3.95 us (1%)
    all_to_all x1, waiting for transfers between devices, side_by_side_2(): lax.all_to_all(both, axis, split_axis=split_dim, concat_axis=concat_dim,...  62.1 us
    all_gather x1, blocking collectives, side_by_side(): lax.all_gather(both, axis, axis=dim, tiled=True)  53.9 us
    all_to_all x1, waiting for transfers between devices, summed_on_arrival(): blocks = lax.all_to_all(in_blocks(x, dim, devices), axis, 0, 0, tiled=True)  52 us
    all_to_all x1, starting transfers between devices, summed_on_arrival(): blocks = lax.all_to_all(in_blocks(x, dim, devices), axis, 0, 0, tiled=True)  47.3 us
    all_to_all x1, waiting for transfers between devices, from_everyone(): return lax.all_to_all(copies, axis, split_axis=0, concat_axis=0, tiled=True)  24.2 us
    all_to_all x1, starting transfers between devices, side_by_side_2(): lax.all_to_all(both, axis, split_axis=split_dim, concat_axis=concat_dim,...  8.15 us
    unnamed x31, local copies, waits for them, and re-layouts  6.75 us
    all_to_all x1, starting transfers between devices, from_everyone(): return lax.all_to_all(copies, axis, split_axis=0, concat_axis=0, tiled=True)  6.66 us
  transfers between devices with their start and end apart: 4, of which 4 were waited for; matrix products, arithmetic and copies ran while one was open for 3% of the time, Pallas kernels for 0%

commit v1 on v0

v1 whole, which is shorter than its diff:
```python
import functools
import math

import jax
import jax.numpy as jnp
from jax import lax
from jax.experimental import pallas as pl
from jax.experimental.pallas import tpu as pltpu
from jax.sharding import Mesh
from jax.sharding import PartitionSpec as P

epsilon = 1e-06
floor_value = -1e30
f32 = jnp.float32
bf16 = jnp.bfloat16
interpreted = False
near_chips = 4
near_cores = 2
far, chip, core, tp = "far", "chip", "core", "tp"
near = (chip, core)
near_terms = 2
far_terms = 2

vmem = pl.BlockSpec(memory_space=pltpu.VMEM)
smem = pl.BlockSpec(memory_space=pltpu.SMEM)
anywhere = pl.BlockSpec(memory_space=pl.ANY)


def iota(shape, dim):
    return lax.broadcasted_iota(jnp.int32, shape, dim)


def call(body, out_shape, in_specs, out_specs=vmem, flops=1000000, room=4, **rest):
    return pl.pallas_call(
        body,
        out_shape=out_shape,
        in_specs=in_specs,
        out_specs=out_specs,
        interpret=interpreted,
        compiler_params=pltpu.CompilerParams(vmem_limit_bytes=room << 20),
        cost_estimate=pl.CostEstimate(flops=flops, bytes_accessed=1000000, transcendentals=0),
        **rest,
    )


def terms_of(x, count):
    terms = []
    for _ in range(count):
        terms.append(x.astype(bf16))
        x = x - terms[-1].astype(f32)
    return terms


def parts_of(x):
    high = x.astype(bf16).astype(f32)
    middle = (x - high).astype(bf16).astype(f32)
    return high, middle, x - high - middle


def project(hidden_ref, query_ref, key_ref, value_ref, out_ref):
    hidden = hidden_ref[...]
    width = query_ref.shape[1]
    at = 0
    for ref, count in ((query_ref, near_terms), (key_ref, 1), (value_ref, 1)):
        sums = jnp.dot(hidden, ref[...], preferred_element_type=f32)
        for term in terms_of(sums, count):
            out_ref[:, at : at + width] = term
            at += width


def arrived_sum(arrived_ref, width, terms):
    total = arrived_ref[0].astype(f32)
    for k in range(1, arrived_ref.shape[0]):
        total = total + arrived_ref[k].astype(f32)
    query = total[:, :width]
    for k in range(1, terms):
        query = query + total[:, k * width : (k + 1) * width]
    return query, total[:, terms * width :]


def sum_near(arrived_ref, out_ref, *, width):
    query, rest = arrived_sum(arrived_ref, width, near_terms)
    terms = terms_of(query, far_terms)
    for k in range(out_ref.shape[0]):
        for i, term in enumerate(terms):
            out_ref[k, :, i * width : (i + 1) * width] = term
        row = [rest[k : k + 1, 128 * i : 128 * (i + 1)] for i in range(8)]
        out_ref[k, :, far_terms * width :] = jnp.concatenate(row, axis=0).astype(bf16)


def normed(x, gain, lane, half):
    squares = x * x
    first = jnp.sum(jnp.where(lane < half, squares, 0.0), axis=-1, keepdims=True)
    second = jnp.sum(jnp.where(lane < half, 0.0, squares), axis=-1, keepdims=True)
    mean = jnp.where(lane < half, first, second) / half
    return x * lax.rsqrt(mean + epsilon) * gain


def finish_rows(arrived_ref, query_gain_ref, key_gain_ref, query_ref, row_ref):
    width = query_ref.shape[2]
    total, row = arrived_sum(arrived_ref, width, far_terms)
    lane = iota((8, 128), 1)
    for i in range(width // 128):
        at = slice(128 * i, 128 * (i + 1))
        part = normed(total[:, at], query_gain_ref[...], lane, 64).astype(bf16)
        for k in range(query_ref.shape[0]):
            query_ref[k, :, at] = part
    row = jnp.where(iota((8, 128), 0) < 4, normed(row, key_gain_ref[...], lane, 64), row)
    row_ref[...] = row.astype(bf16)


def attend(
    place_ref,
    past_ref,
    accepted_ref,
    parents_ref,
    lambda_ref,
    query_ref,
    row_ref,
    keys_ref,
    values_ref,
    out_ref,
    keys_out_ref,
    values_out_ref,
    sems,
):
    keys_copy = pltpu.make_async_copy(keys_ref, keys_out_ref, sems.at[0])
    values_copy = pltpu.make_async_copy(values_ref, values_out_ref, sems.at[1])
    keys_copy.start()
    values_copy.start()
    own, offset = place_ref[0], place_ref[1]
    seqs, proposals = parents_ref.shape
    own_seq, own_order = own // proposals, lax.rem(own, proposals)
    below = jnp.int32(0)
    for j in range(proposals):
        parent = parents_ref[own_seq, j]
        above = jnp.where(parent >= 0, (below >> jnp.maximum(parent, 0)) & 1, 0)
        below = below | (jnp.where(own_order == j, 1, above) << j)
    rows, columns = 128, keys_ref.shape[1]
    row = iota((rows, 128), 0)
    lane = iota((rows, 128), 1)
    row_head, row_comp = row & 3, (row >> 3) & 1
    row_order = 2 * (row >> 4) + ((row >> 2) & 1)
    spread = (iota((rows, proposals), 1) == row_order[:, :proposals]).astype(bf16)
    head_at = [row_head == h for h in range(4)]
    comp_at = (lane >= 64) == (row_comp == 1)
    line = iota((rows, columns), 0)
    column = iota((rows, columns), 1)
    same_head = (column & 3) == (line & 3)
    position = offset + (column >> 2)
    under = ((below >> row_order[:, :1]) & 1) == 1
    scale = jnp.ones((rows, 1), f32)
    for h in range(4):
        mine = (row_head[:, :1] == h) & (row_comp[:, :1] == 1)
        scale = jnp.where(mine, lambda_ref[h], scale)
    new_row = row_ref[...].astype(f32)
    new_key = jnp.concatenate([new_row[:4]] * (rows // 4), axis=0)
    new_value = jnp.concatenate([new_row[4:]] * (rows // 4), axis=0)
    for s in range(seqs):
        wide = jnp.dot(
            spread, query_ref[s * proposals : (s + 1) * proposals, :], preferred_element_type=f32
        )
        query = jnp.zeros((rows, 128), f32)
        for h in range(4):
            query = jnp.where(head_at[h], wide[:, 128 * h : 128 * (h + 1)], query)
        query = jnp.where(comp_at, query, 0.0)
        scores = lax.dot_general(
            query.astype(bf16),
            keys_ref[s],
            (((1,), (1,)), ((), ())),
            preferred_element_type=f32,
        )
        visible = same_head & (position < past_ref[s] + accepted_ref[s])
        masked = jnp.where(visible, scores * 0.125, floor_value)
        tree_score = jnp.sum(query * new_key, axis=-1, keepdims=True) * 0.125
        tree_visible = under & (own_seq == s)
        tree_masked = jnp.where(tree_visible, tree_score, floor_value)
        top = jnp.maximum(jnp.max(masked, axis=-1, keepdims=True), tree_masked)
        weights = jnp.where(visible, jnp.exp(masked - top), 0.0)
        tree_weight = jnp.where(tree_visible, jnp.exp(tree_masked - top), 0.0)
        total = jnp.sum(weights, axis=-1, keepdims=True) + tree_weight
        acc = jnp.dot(weights.astype(bf16), values_ref[s], preferred_element_type=f32)
        acc = (acc + tree_weight.astype(bf16).astype(f32) * new_value) * scale
        acc = acc.astype(bf16)
        stats = jnp.zeros((rows, 128), f32)
        for k, part in enumerate((*parts_of(top), *parts_of(total))):
            stats = jnp.where(lane == k, part, stats)
        stats = jnp.transpose(stats)[:8].astype(bf16)
        for r in range(out_ref.shape[0]):
            out_ref[r, s, :16, :] = acc[16 * r : 16 * (r + 1)]
            out_ref[r, s, 16:, :] = stats
    keys_copy.wait()
    values_copy.wait()


def stat_rows(stats):
    return stats[0:1] + stats[1:2] + stats[2:3], stats[3:4] + stats[4:5] + stats[5:6]


def combine_near(place_ref, arrived_ref, row_ref, out_ref, factor_ref):
    me = place_ref[2]
    sources, groups = arrived_ref.shape[:2]
    tiles, factors = [], []
    lane = iota((8, 128), 1)
    packed = jnp.zeros((8, 128), f32)
    for g in range(groups):
        tops, sums = zip(*[stat_rows(arrived_ref[r, g, 16:, :].astype(f32)) for r in range(sources)])
        top = functools.reduce(jnp.maximum, tops)
        scales = [jnp.exp(t - top) for t in tops]
        total = sum(s * f for s, f in zip(sums, scales))
        factors.extend(scales)
        zero = jnp.zeros((1, 128), f32)
        stats = jnp.concatenate([*parts_of(top), *parts_of(total), zero, zero], axis=0)
        moved = pltpu.roll(stats, lax.rem(128 + 16 * g - 16 * me, 128), 1)
        packed = jnp.where((lane >> 4) == g, moved, packed)
    count = sources * groups
    wide = jnp.concatenate(factors + [jnp.zeros((128 - count, 128), f32)], axis=0)
    factor_ref[...] = jnp.transpose(wide)
    mine = factor_ref[pl.ds(pl.multiple_of(16 * me, 16), 16), :]
    for g in range(groups):
        acc = jnp.zeros((16, 128), f32)
        for r in range(sources):
            at = g * sources + r
            acc = acc + arrived_ref[r, g, :16, :].astype(f32) * mine[:, at : at + 1]
        tiles.append(acc.astype(bf16))
    for k in range(out_ref.shape[0]):
        for g in range(groups):
            out_ref[k, 16 * g : 16 * (g + 1), :] = tiles[g]
        out_ref[k, 64:72, :] = packed.astype(bf16)
        out_ref[k, 72:80, :] = row_ref[...]


def combine_far(arrived_ref, gain_ref, out_ref):
    sources = arrived_ref.shape[0]
    tops, sums = zip(*[stat_rows(arrived_ref[q, 64:72, :].astype(f32)) for q in range(sources)])
    top = functools.reduce(jnp.maximum, tops)
    scales = [jnp.exp(t - top) for t in tops]
    total = sum(s * f for s, f in zip(sums, scales))
    wide = jnp.concatenate(scales + [total, jnp.zeros((127 - sources, 128), f32)], axis=0)
    columns = jnp.transpose(wide)[:64]
    acc = jnp.zeros((64, 128), f32)
    for q in range(sources):
        acc = acc + arrived_ref[q, :64, :].astype(f32) * columns[:, q : q + 1]
    acc = acc / columns[:, sources : sources + 1]
    heads = []
    for g in range(4):
        mixture = acc[16 * g : 16 * g + 8] - acc[16 * g + 8 : 16 * g + 16]
        mean = jnp.mean(mixture * mixture, axis=-1, keepdims=True)
        heads.append((mixture * lax.rsqrt(mean + epsilon) * gain_ref[...]).astype(bf16))
    for k in range(out_ref.shape[0]):
        for g in range(4):
            out_ref[k, 8 * g : 8 * (g + 1), :] = heads[g]
        for q in range(sources):
            out_ref[k, 32 + 8 * q : 40 + 8 * q, :] = arrived_ref[q, 72:80, :]


def finish(
    place_ref,
    past_ref,
    accepted_ref,
    arrived_ref,
    weight_ref,
    keys_ref,
    values_ref,
    out_ref,
    keys_out_ref,
    values_out_ref,
    key_rows,
    value_rows,
    sem,
):
    del keys_ref, values_ref
    sources = arrived_ref.shape[0]
    heads = jnp.concatenate([arrived_ref[r, :32, :] for r in range(sources)], axis=0)
    count = heads.shape[0]
    to = iota((count, count), 0)
    source = ((to >> 1) & 7) * 32 + (to >> 6) * 8 + (to & 1) * 4 + ((to >> 4) & 3)
    order = (iota((count, count), 1) == source).astype(bf16)
    heads = jnp.dot(order, heads, preferred_element_type=f32).astype(bf16)
    total = jnp.zeros(out_ref.shape, f32)
    for g in range(4):
        left = jnp.concatenate(
            [heads[64 * g + 16 * h : 64 * g + 16 * (h + 1)] for h in range(4)], axis=1
        )
        group = lax.dot_general(
            left, weight_ref[g], (((1,), (1,)), ((), ())), preferred_element_type=f32
        )
        total = total + group.astype(bf16).astype(f32)
    out_ref[...] = total.astype(bf16)
    offset = place_ref[1]
    seqs, positions_dev = keys_out_ref.shape[:2]
    proposals = key_rows.shape[0]
    for s in range(seqs):
        first = past_ref[s] + accepted_ref[s] - offset

        @pl.when((first > -proposals) & (first < positions_dev))
        def _():
            for j in range(proposals):
                r, q = divmod(s * proposals + j, sources)
                key_rows[j] = arrived_ref[r, 32 + 8 * q : 36 + 8 * q, :]
                value_rows[j] = arrived_ref[r, 36 + 8 * q : 40 + 8 * q, :]
            for j in range(proposals):

                @pl.when((first + j >= 0) & (first + j < positions_dev))
                def _():
                    at = jnp.clip(first + j, 0, positions_dev - 1)
                    copies = [
                        pltpu.make_async_copy(rows.at[j], whole.at[s, at], sem.at[k])
                        for k, (rows, whole) in enumerate(
                            ((key_rows, keys_out_ref), (value_rows, values_out_ref))
                        )
                    ]
                    for c in copies:
                        c.start()
                    for c in copies:
                        c.wait()


def on_device(
    hidden_states,
    w_query,
    w_key,
    w_value,
    query_gain,
    key_gain,
    lambda_head,
    head_gain,
    w_output,
    cache_keys,
    cache_values,
    past_lengths,
    accepted,
    parents,
):
    shape = jax.ShapeDtypeStruct
    seqs, proposals = parents.shape
    tokens = hidden_states.shape[0]
    width = w_query.shape[1]
    positions_dev, heads = cache_keys.shape[1:3]
    nears, fars, tps = (math.prod(lax.axis_size(a) for a in axes) for axes in (near, (far,), (tp,)))
    chunk = tokens // nears
    near_index, far_index = lax.axis_index(near), lax.axis_index(far)
    shard = far_index * nears + near_index
    place = jnp.stack([near_index * chunk + far_index, shard * positions_dev, near_index])
    place = place.astype(jnp.int32)
    two_query = jnp.concatenate([query_gain, query_gain])[None]
    two_key = jnp.concatenate([key_gain, key_gain])[None]

    terms = call(project, shape((tokens, (near_terms + 2) * width), bf16), [vmem] * 4)(
        hidden_states, w_query, w_key, w_value
    )
    terms = lax.all_to_all(
        terms.reshape(nears, chunk, -1), near, 0, 0, tiled=True
    )
    shared = call(
        functools.partial(sum_near, width=width),
        shape((fars, chunk, far_terms * width + 128), bf16),
        [vmem],
    )(terms)
    shared = lax.all_to_all(shared, far, 0, 0, tiled=True)
    query, row = call(
        finish_rows,
        (shape((nears, chunk, width), bf16), shape((8, 128), bf16)),
        [vmem] * 3,
        (vmem, vmem),
    )(shared, two_query, two_key)
    query = lax.all_to_all(query, near, 0, 0, tiled=True).reshape(tokens, width)
    flat = (seqs, positions_dev * heads, 128)
    part, keys_copy, values_copy = call(
        attend,
        (
            shape((nears, tps, 24, 128), bf16),
            shape(flat, bf16),
            shape(flat, bf16),
        ),
        [smem] * 5 + [vmem] * 4,
        (vmem, anywhere, anywhere),
        scratch_shapes=[pltpu.SemaphoreType.DMA((2,))],
        flops=10000000,
        room=16,
    )(
        place,
        past_lengths,
        accepted,
        parents,
        lambda_head,
        query,
        row,
        cache_keys.reshape(flat),
        cache_values.reshape(flat),
    )
    part = lax.all_to_all(
        part.reshape(nears * tps, 24, 128), (*near, tp), 0, 0, tiled=True
    )
    part = call(
        combine_near,
        shape((fars, 80, 128), bf16),
        [smem, vmem, vmem],
        scratch_shapes=[pltpu.VMEM((128, 128), f32)],
    )(place, part.reshape(nears, tps, 24, 128), row)
    part = lax.all_to_all(part, far, 0, 0, tiled=True)
    mixed = call(combine_far, shape((nears, 96, 128), bf16), [vmem] * 2)(part, head_gain[None])
    mixed = lax.all_to_all(mixed, near, 0, 0, tiled=True)
    weight = jnp.broadcast_to(w_output.T[None], (tps, *w_output.T.shape))
    weight = lax.all_to_all(weight, tp, 0, 0, tiled=True)
    whole = cache_keys.shape
    return call(
        finish,
        (
            shape((proposals, w_output.shape[1]), bf16),
            shape(whole, bf16),
            shape(whole, bf16),
        ),
        [smem] * 3 + [vmem] * 2 + [anywhere] * 2,
        (vmem, anywhere, anywhere),
        scratch_shapes=[
            pltpu.VMEM((proposals, heads, 128), bf16),
            pltpu.VMEM((proposals, heads, 128), bf16),
            pltpu.SemaphoreType.DMA((2,)),
        ],
        input_output_aliases={5: 1, 6: 2},
    )(
        place,
        past_lengths,
        accepted,
        mixed,
        weight,
        keys_copy.reshape(whole),
        values_copy.reshape(whole),
    )


def solution(mesh):
    groups, shards, tps = (mesh.shape[a] for a in ("grp", "kv", "tp"))
    split = (groups, shards // (near_chips * near_cores), near_chips, near_cores, tps)
    finer = Mesh(mesh.devices.reshape(split), ("grp", far, chip, core, tp))
    kv = (far, chip, core)
    cache = P("grp", kv, tp, None)
    placed = (
        P("grp", kv),
        P(kv, tp),
        P(kv, tp),
        P(kv, tp),
        P(),
        P(),
        P(tp),
        P(),
        P(tp, kv),
        cache,
        cache,
        P("grp"),
        P("grp"),
        P("grp", None),
    )
    return jax.shard_map(
        on_device,
        mesh=finer,
        in_specs=placed,
        out_specs=(P(("grp", tp), kv), cache, cache),
        check_vma=False,
    )
```

time: 286 us -> 184 us (0.64)
  waiting for transfers between devices: 140 us -> 40.7 us
  blocking collectives: 53.9 us -> 78.4 us
  starting transfers between devices: 66.7 us -> 49.3 us
  Pallas kernels: 0 us -> 7.4 us
  matrix products: 7.11 us -> 0 us
  local copies, waits for them, and re-layouts: 12.6 us -> 6.62 us
  other arithmetic: 3.95 us -> 0.15 us
    all_to_all x4 -> x3, waiting for transfers between devices: 140 us -> 40.7 us  [the longest x1 29.2 us: on_device(): shared = lax.all_to_all(shared, far, 0, 0, tiled=True)]
    all_to_all x0 -> x4, blocking collectives: none -> 78.4 us  [the longest x1 32.4 us: on_device(): part = lax.all_to_all(part, far, 0, 0, tiled=True)]
    all_gather x1 -> x0, blocking collectives: 53.9 us -> none  [side_by_side(): lax.all_gather(both, axis, axis=dim, tiled=True)]
    all_to_all x4 -> x3, starting transfers between devices: 66.7 us -> 49.3 us  [the longest x1 40.9 us: on_device(): shared = lax.all_to_all(shared, far, 0, 0, tiled=True)]
    pallas_call x0 -> x7, Pallas kernels: none -> 7.4 us  [the longest x1 2.98 us: on_device(): call(attend, (shape((nears, tps, 24, 128), bf16), shape(flat, bf16), shap...]
    dot_general x14 -> x0, matrix products: 7.11 us -> none  [the longest x2 1.81 us: partial_softmax(): jnp.einsum('sqhcp,sphv->sqhcv', weights.astype(jnp.bfloat16), values, pre...]
    unnamed x31 -> x28, local copies, waits for them, and re-layouts: 6.75 us -> 5.9 us
  transfers between devices with their start and end apart: 4 -> 3, of which waited for: 4 -> 3; matrix products, arithmetic and copies ran while one was open for 3% -> 0% of each run, Pallas kernels for 0% -> 0%
where the time goes in v1:
time: 184 us; the launch traced here: 183 us
  blocking collectives  78.4 us (43%)
  starting transfers between devices  49.3 us (27%)
  waiting for transfers between devices  40.7 us (22%)
  Pallas kernels  7.4 us (4%)
  local copies, waits for them, and re-layouts  6.62 us (4%)
    all_to_all x1, starting transfers between devices, on_device(): shared = lax.all_to_all(shared, far, 0, 0, tiled=True)  40.9 us
    all_to_all x1, blocking collectives, on_device(): part = lax.all_to_all(part, far, 0, 0, tiled=True)  32.4 us
    all_to_all x1, waiting for transfers between devices, on_device(): shared = lax.all_to_all(shared, far, 0, 0, tiled=True)  29.2 us
    all_to_all x1, blocking collectives, on_device(): lax.all_to_all(terms.reshape(nears, chunk, -1), near, 0, 0, tiled=True)  18 us
    all_to_all x1, blocking collectives, on_device(): lax.all_to_all(part.reshape(nears * tps, 24, 128), (*near, tp), 0, 0, til...  14.9 us
    all_to_all x1, blocking collectives, on_device(): mixed = lax.all_to_all(mixed, near, 0, 0, tiled=True)  13.1 us
    unnamed x28, local copies, waits for them, and re-layouts  5.9 us
    all_to_all x1, waiting for transfers between devices, on_device(): query = lax.all_to_all(query, near, 0, 0, tiled=True).reshape(tokens, width)  5.84 us
  transfers between devices with their start and end apart: 3, of which 3 were waited for; matrix products, arithmetic and copies ran while one was open for 0% of the time, Pallas kernels for 0%

profile of v1, /device:TPU:40, one launch (start us, length us, event | category | flops | bytes accessed | tf_op | source)
XLA Modules:
  0.0 183.2 jit_solution(12441397958289085535)
XLA Ops:
  0.6 0.0 copy-start
  0.6 0.0 copy-start.2
  0.7 0.9 copy-done.2
  1.6 0.0 copy-start.3
  1.6 0.8 copy-done.3
  2.4 0.0 copy-start.4
  2.4 0.8 copy-done.4
  3.2 0.0 copy-start.5
  3.3 0.7 copy-done.5
  4.0 0.2 shard_map.157
  4.2 18.0 %all_to_all.35.arrived_ref = bf16[8,8,2048]{2,1,0:T(8,128)(2,1)S(1)} all-to-all(bf16[8,8,2048]{2,1,0:T(8,128)(2,1)S(1)} %bitcast.19), channel_id=1, replica_groups=mesh['grp'=2,'far'=8,'chip'=4,'core'=2,'tp'=4] {'chip','core'}, dimensions={0} | all-to-all | bytes 524288 | tf_op jit(solution)/shard_map/all_to_all | solution.py:352
  22.2 0.7 shard_map.158
  22.9 0.0 copy-start.12
  22.9 0.0 copy-start.13
  22.9 40.9 %all-to-all-start.1 = ((bf16[8,8,1152]{2,1,0:T(8,128)(2,1)}), bf16[8,8,1152]{2,1,0:T(8,128)(2,1)S(1)}, u32[]{:S(2)}, u32[]{:S(2)}) async-start(bf16[8,8,1152]{2,1,0:T(8,128)(2,1)} %shard_map.158), calls=%async_computation.1 | async-start | bytes 294912 | tf_op jit(solution)/shard_map/all_to_all | solution.py:360
  63.7 0.0 copy-done.12
  63.8 0.0 copy-done.13
  63.8 0.1 maximum_bitcast_fusion
  63.8 29.2 %all-to-all-done.1.arrived_ref = bf16[8,8,1152]{2,1,0:T(8,128)(2,1)S(1)} async-done(((bf16[8,8,1152]{2,1,0:T(8,128)(2,1)}), bf16[8,8,1152]{2,1,0:T(8,128)(2,1)S(1)}, u32[]{:S(2)}, u32[]{:S(2)}) %all-to-all-start.1) | async-done | bytes 147488 | tf_op jit(solution)/shard_map/all_to_all | solution.py:360
  93.0 0.7 shard_map.159
  93.8 4.0 %all-to-all-start.2 = ((bf16[8,8,512]{2,1,0:T(8,128)(2,1)}), bf16[8,8,512]{2,1,0:T(8,128)(2,1)S(1)}, u32[]{:S(2)}, u32[]{:S(2)}) async-start(bf16[8,8,512]{2,1,0:T(8,128)(2,1)} %get-tuple-element.8), calls=%async_computation.2 | async-start | bytes 131072 | tf_op jit(solution)/shard_map/all_to_all | solution.py:367
  97.7 0.1 pad_add_fusion.place_ref
  97.8 5.8 %all-to-all-done.2 = bf16[8,8,512]{2,1,0:T(8,128)(2,1)S(1)} async-done(((bf16[8,8,512]{2,1,0:T(8,128)(2,1)}), bf16[8,8,512]{2,1,0:T(8,128)(2,1)S(1)}, u32[]{:S(2)}, u32[]{:S(2)}) %all-to-all-start.2) | async-done | bytes 65568 | tf_op jit(solution)/shard_map/all_to_all | solution.py:367
  103.7 0.0 copy-start.6
  103.7 0.0 copy-start.7
  103.7 0.0 copy-start.8
  103.7 0.0 copy-start.9
  103.7 0.0 copy-done
  103.7 0.7 copy-done.6
  104.3 0.0 copy-done.7
  104.3 0.0 copy-done.8
  104.4 0.0 copy-done.9
  104.4 0.0 copy-start.1
  104.4 1.2 copy-done.1
  105.6 3.0 %shard_map.160 = (bf16[8,4,24,128]{3,2,1,0:T(8,128)(2,1)S(1)}, bf16[4,1024,128]{2,1,0:T(8,128)(2,1)}, bf16[4,1024,128]{2,1,0:T(8,128)(2,1)}) custom-call(s32[3]{0:T(128)S(1)} %pad_add_fusion.place_ref, s32[4]{0:T(128)S(1)} %copy-done.7, s32[4]{0:T(128)S(1)} %copy-done.8, s32[4,16]{1,0:T(4,128)S(1)} %copy-done.6, f32[4]{0:T(128)S(1)} %copy-done.9, ...), custom_call_target="tpu_custom_call" | custom-call | flops 10000000 | bytes 1000000 | tf_op jit(solution)/shard_map/pallas_call | solution.py:369
  108.6 14.9 %all_to_all.36 = bf16[32,24,128]{2,1,0:T(8,128)(2,1)S(1)} all-to-all(bf16[32,24,128]{2,1,0:T(8,128)(2,1)S(1)} %bitcast.22), channel_id=1, replica_groups=mesh['grp'=2,'far'=8,'chip'=4,'core'=2,'tp'=4] {'chip','core','tp'}, dimensions={0} | all-to-all | bytes 393216 | tf_op jit(solution)/shard_map/all_to_all | solution.py:392
  123.5 0.9 shard_map.161
  124.4 0.0 copy-start.11
  124.4 32.4 %all_to_all.37.arrived_ref = bf16[8,80,128]{2,1,0:T(8,128)(2,1)S(1)} all-to-all(bf16[8,80,128]{2,1,0:T(8,128)(2,1)S(1)} %shard_map.161), channel_id=1, replica_groups=mesh['grp'=2,'far'=8,'chip'=4,'core'=2,'tp'=4] {'far'}, dimensions={0} | all-to-all | bytes 327680 | tf_op jit(solution)/shard_map/all_to_all | solution.py:401
  156.8 0.0 copy-done.11
  156.8 0.7 broadcast_in_dim.18
  157.5 4.4 %all-to-all-start.6 = ((bf16[4,64,512]{2,1,0:T(8,128)(2,1)}), bf16[4,64,512]{2,1,0:T(8,128)(2,1)S(1)}, u32[]{:S(2)}, u32[]{:S(2)}) async-start(bf16[4,64,512]{2,1,0:T(8,128)(2,1)} %broadcast_in_dim.18), calls=%async_computation.6 | async-start | bytes 524288 | tf_op jit(solution)/shard_map/all_to_all | solution.py:405
  161.9 0.0 copy-start.10
  161.9 0.7 copy-done.10
  162.6 0.4 shard_map.162
  163.0 5.6 %all-to-all-done.6.weight_ref = bf16[4,64,512]{2,1,0:T(8,128)(2,1)S(1)} async-done(((bf16[4,64,512]{2,1,0:T(8,128)(2,1)}), bf16[4,64,512]{2,1,0:T(8,128)(2,1)S(1)}, u32[]{:S(2)}, u32[]{:S(2)}) %all-to-all-start.6) | async-done | bytes 262176 | tf_op jit(solution)/shard_map/all_to_all | solution.py:405
  168.6 13.1 %all_to_all.38.arrived_ref = bf16[8,96,128]{2,1,0:T(8,128)(2,1)S(1)} all-to-all(bf16[8,96,128]{2,1,0:T(8,128)(2,1)S(1)} %shard_map.162), channel_id=1, replica_groups=mesh['grp'=2,'far'=8,'chip'=4,'core'=2,'tp'=4] {'chip','core'}, dimensions={0} | all-to-all | bytes 393216 | tf_op jit(solution)/shard_map/all_to_all | solution.py:403
  181.7 1.5 shard_map.163
Async XLA Ops:
  0.6 103.0 %copy-start = (bf16[4,256,4,128]{3,2,1,0:T(4,128)(2,1)S(1)}, bf16[4,256,4,128]{3,2,1,0:T(4,128)(2,1)}, u32[]{:S(2)}) copy-start(bf16[4,256,4,128]{3,2,1,0:T(4,128)(2,1)} %param.23) | copy-start | bytes 3145732
  0.6 0.9 copy-start.2
  1.6 0.8 copy-start.3
  2.4 0.8 copy-start.4
  3.2 0.7 copy-start.5
  22.9 40.9 %copy-start.12 = (f32[64]{0:T(128)S(1)}, f32[64]{0:T(128)}, u32[]{:S(2)}) copy-start(f32[64]{0:T(128)} %param.18) | copy-start | bytes 772
  22.9 40.9 %copy-start.13 = (f32[64]{0:T(128)S(1)}, f32[64]{0:T(128)}, u32[]{:S(2)}) copy-start(f32[64]{0:T(128)} %param.19) | copy-start | bytes 772
  22.9 70.2 %all-to-all-start.1 = ((bf16[8,8,1152]{2,1,0:T(8,128)(2,1)}), bf16[8,8,1152]{2,1,0:T(8,128)(2,1)S(1)}, u32[]{:S(2)}, u32[]{:S(2)}) async-start(bf16[8,8,1152]{2,1,0:T(8,128)(2,1)} %shard_map.158), calls=%async_computation.1 | async-start | bytes 294912 | tf_op jit(solution)/shard_map/all_to_all | solution.py:360
  93.8 9.9 %all-to-all-start.2 = ((bf16[8,8,512]{2,1,0:T(8,128)(2,1)}), bf16[8,8,512]{2,1,0:T(8,128)(2,1)S(1)}, u32[]{:S(2)}, u32[]{:S(2)}) async-start(bf16[8,8,512]{2,1,0:T(8,128)(2,1)} %get-tuple-element.8), calls=%async_computation.2 | async-start | bytes 131072 | tf_op jit(solution)/shard_map/all_to_all | solution.py:367
  103.7 0.7 copy-start.6
  103.7 0.7 copy-start.7
  103.7 0.7 copy-start.8
  103.7 0.7 copy-start.9
  104.4 1.2 copy-start.1
  124.4 32.4 %copy-start.11 = (bf16[512,64]{0,1:T(8,128)(2,1)S(1)}, bf16[512,64]{0,1:T(8,128)(2,1)}, u32[]{:S(2)}) copy-start(bf16[512,64]{0,1:T(8,128)(2,1)} %param.22) | copy-start | bytes 196612
  157.5 11.1 %all-to-all-start.6 = ((bf16[4,64,512]{2,1,0:T(8,128)(2,1)}), bf16[4,64,512]{2,1,0:T(8,128)(2,1)S(1)}, u32[]{:S(2)}, u32[]{:S(2)}) async-start(bf16[4,64,512]{2,1,0:T(8,128)(2,1)} %broadcast_in_dim.18), calls=%async_computation.6 | async-start | bytes 524288 | tf_op jit(solution)/shard_map/all_to_all | solution.py:405
  161.9 0.7 copy-start.10

commit v2 on v1

--- a/solution.py
+++ b/solution.py
@@ -8,6 +8,7 @@
 from jax.experimental.pallas import tpu as pltpu
 from jax.sharding import Mesh
 from jax.sharding import PartitionSpec as P
+
 
 epsilon = 1e-06
 floor_value = -1e30
@@ -20,10 +21,15 @@
 near = (chip, core)
 near_terms = 2
 far_terms = 2
+rows = 128
 
 vmem = pl.BlockSpec(memory_space=pltpu.VMEM)
 smem = pl.BlockSpec(memory_space=pltpu.SMEM)
-anywhere = pl.BlockSpec(memory_space=pl.ANY)
+hbm = pl.BlockSpec(memory_space=pltpu.HBM)
+
+
+def near_place():
+    return lax.axis_index(chip) * lax.axis_size(core) + lax.axis_index(core)
 
 
 def iota(shape, dim):
@@ -57,12 +63,18 @@
     return high, middle, x - high - middle
 
 
-def project(hidden_ref, query_ref, key_ref, value_ref, out_ref):
-    hidden = hidden_ref[...]
+def project(hidden_ref, query_ref, key_ref, value_ref, out_ref, hidden, weights, sems):
     width = query_ref.shape[1]
+    copies = [pltpu.make_async_copy(hidden_ref, hidden, sems.at[3])]
+    for k, ref in enumerate((query_ref, key_ref, value_ref)):
+        copies.append(pltpu.make_async_copy(ref, weights.at[k], sems.at[k]))
+    for c in copies:
+        c.start()
     at = 0
-    for ref, count in ((query_ref, near_terms), (key_ref, 1), (value_ref, 1)):
-        sums = jnp.dot(hidden, ref[...], preferred_element_type=f32)
+    copies[0].wait()
+    for k, count in enumerate((near_terms, 1, 1)):
+        copies[k + 1].wait()
+        sums = jnp.dot(hidden[...], weights[k], preferred_element_type=f32)
         for term in terms_of(sums, count):
             out_ref[:, at : at + width] = term
             at += width
@@ -100,43 +112,84 @@
     width = query_ref.shape[2]
     total, row = arrived_sum(arrived_ref, width, far_terms)
     lane = iota((8, 128), 1)
+    query_gain = jnp.concatenate([query_gain_ref[...]] * 2, axis=1)
+    key_gain = jnp.concatenate([key_gain_ref[...]] * 2, axis=1)
     for i in range(width // 128):
         at = slice(128 * i, 128 * (i + 1))
-        part = normed(total[:, at], query_gain_ref[...], lane, 64).astype(bf16)
+        part = normed(total[:, at], query_gain, lane, 64).astype(bf16)
         for k in range(query_ref.shape[0]):
             query_ref[k, :, at] = part
-    row = jnp.where(iota((8, 128), 0) < 4, normed(row, key_gain_ref[...], lane, 64), row)
+    row = jnp.where(iota((8, 128), 0) < 4, normed(row, key_gain, lane, 64), row)
     row_ref[...] = row.astype(bf16)
 
 
-def attend(
-    place_ref,
+def stage(
     past_ref,
     accepted_ref,
     parents_ref,
     lambda_ref,
-    query_ref,
-    row_ref,
     keys_ref,
     values_ref,
-    out_ref,
+    keys_vmem_ref,
+    values_vmem_ref,
     keys_out_ref,
     values_out_ref,
+    limit_ref,
+    under_ref,
+    scale_ref,
     sems,
 ):
-    keys_copy = pltpu.make_async_copy(keys_ref, keys_out_ref, sems.at[0])
-    values_copy = pltpu.make_async_copy(values_ref, values_out_ref, sems.at[1])
-    keys_copy.start()
-    values_copy.start()
-    own, offset = place_ref[0], place_ref[1]
+    taken = [
+        pltpu.make_async_copy(keys_ref, keys_vmem_ref, sems.at[0]),
+        pltpu.make_async_copy(values_ref, values_vmem_ref, sems.at[1]),
+    ]
+    put = [
+        pltpu.make_async_copy(keys_vmem_ref, keys_out_ref, sems.at[2]),
+        pltpu.make_async_copy(values_vmem_ref, values_out_ref, sems.at[3]),
+    ]
+    for c in taken:
+        c.start()
     seqs, proposals = parents_ref.shape
+    nears = lax.axis_size(near)
+    far_index = lax.axis_index(far)
+    own = near_place() * (seqs * proposals // nears) + far_index
+    offset = (far_index * nears + near_place()) * (keys_ref.shape[1] // 4)
     own_seq, own_order = own // proposals, lax.rem(own, proposals)
     below = jnp.int32(0)
     for j in range(proposals):
         parent = parents_ref[own_seq, j]
         above = jnp.where(parent >= 0, (below >> jnp.maximum(parent, 0)) & 1, 0)
         below = below | (jnp.where(own_order == j, 1, above) << j)
-    rows, columns = 128, keys_ref.shape[1]
+    row = iota((rows, 128), 0)
+    under = (below >> (2 * (row >> 4) + ((row >> 2) & 1))) & 1
+    limit = jnp.zeros((8, 128), jnp.int32)
+    for s in range(seqs):
+        limit = jnp.where(iota((8, 128), 0) == s, past_ref[s] + accepted_ref[s] - offset, limit)
+        under_ref[s] = jnp.where(own_seq == s, under, 0).astype(f32)
+    limit_ref[...] = limit
+    scale = jnp.ones((rows, 128), f32)
+    for h in range(4):
+        scale = jnp.where(((row & 3) == h) & (((row >> 3) & 1) == 1), lambda_ref[h], scale)
+    scale_ref[...] = scale
+    for c, d in zip(taken, put):
+        c.wait()
+        d.start()
+    for d in put:
+        d.wait()
+
+
+def attend(
+    limit_ref,
+    under_ref,
+    scale_ref,
+    query_ref,
+    row_ref,
+    keys_ref,
+    values_ref,
+    out_ref,
+):
+    seqs, columns = keys_ref.shape[:2]
+    proposals = query_ref.shape[0] // seqs
     row = iota((rows, 128), 0)
     lane = iota((rows, 128), 1)
     row_head, row_comp = row & 3, (row >> 3) & 1
@@ -144,15 +197,10 @@
     spread = (iota((rows, proposals), 1) == row_order[:, :proposals]).astype(bf16)
     head_at = [row_head == h for h in range(4)]
     comp_at = (lane >= 64) == (row_comp == 1)
-    line = iota((rows, columns), 0)
     column = iota((rows, columns), 1)
-    same_head = (column & 3) == (line & 3)
-    position = offset + (column >> 2)
-    under = ((below >> row_order[:, :1]) & 1) == 1
-    scale = jnp.ones((rows, 1), f32)
-    for h in range(4):
-        mine = (row_head[:, :1] == h) & (row_comp[:, :1] == 1)
-        scale = jnp.where(mine, lambda_ref[h], scale)
+    same_head = (column & 3) == (iota((rows, columns), 0) & 3)
+    position = jnp.where(same_head, column >> 2, columns)
+    scale = scale_ref[...]
     new_row = row_ref[...].astype(f32)
     new_key = jnp.concatenate([new_row[:4]] * (rows // 4), axis=0)
     new_value = jnp.concatenate([new_row[4:]] * (rows // 4), axis=0)
@@ -170,10 +218,10 @@
             (((1,), (1,)), ((), ())),
             preferred_element_type=f32,
         )
-        visible = same_head & (position < past_ref[s] + accepted_ref[s])
+        visible = position < jnp.minimum(limit_ref[s : s + 1, :1], columns)
         masked = jnp.where(visible, scores * 0.125, floor_value)
         tree_score = jnp.sum(query * new_key, axis=-1, keepdims=True) * 0.125
-        tree_visible = under & (own_seq == s)
+        tree_visible = under_ref[s, :, :1] > 0.5
         tree_masked = jnp.where(tree_visible, tree_score, floor_value)
         top = jnp.maximum(jnp.max(masked, axis=-1, keepdims=True), tree_masked)
         weights = jnp.where(visible, jnp.exp(masked - top), 0.0)
@@ -189,16 +237,14 @@
         for r in range(out_ref.shape[0]):
             out_ref[r, s, :16, :] = acc[16 * r : 16 * (r + 1)]
             out_ref[r, s, 16:, :] = stats
-    keys_copy.wait()
-    values_copy.wait()
 
 
 def stat_rows(stats):
     return stats[0:1] + stats[1:2] + stats[2:3], stats[3:4] + stats[4:5] + stats[5:6]
 
 
-def combine_near(place_ref, arrived_ref, row_ref, out_ref, factor_ref):
-    me = place_ref[2]
+def combine_near(arrived_ref, row_ref, out_ref, factor_ref):
+    me = near_place()
     sources, groups = arrived_ref.shape[:2]
     tiles, factors = [], []
     lane = iota((8, 128), 1)
@@ -255,20 +301,30 @@
 
 
 def finish(
-    place_ref,
     past_ref,
     accepted_ref,
     arrived_ref,
-    weight_ref,
+    own_ref,
+    first_ref,
+    second_ref,
+    third_ref,
     keys_ref,
     values_ref,
     out_ref,
     keys_out_ref,
     values_out_ref,
+    heads_ref,
     key_rows,
     value_rows,
+    lengths,
     sem,
 ):
+    known = [
+        pltpu.make_async_copy(past_ref, lengths.at[0], sem.at[0]),
+        pltpu.make_async_copy(accepted_ref, lengths.at[1], sem.at[1]),
+    ]
+    for c in known:
+        c.start()
     del keys_ref, values_ref
     sources = arrived_ref.shape[0]
     heads = jnp.concatenate([arrived_ref[r, :32, :] for r in range(sources)], axis=0)
@@ -276,22 +332,24 @@
     to = iota((count, count), 0)
     source = ((to >> 1) & 7) * 32 + (to >> 6) * 8 + (to & 1) * 4 + ((to >> 4) & 3)
     order = (iota((count, count), 1) == source).astype(bf16)
-    heads = jnp.dot(order, heads, preferred_element_type=f32).astype(bf16)
+    heads_ref[...] = jnp.dot(order, heads, preferred_element_type=f32)
     total = jnp.zeros(out_ref.shape, f32)
-    for g in range(4):
-        left = jnp.concatenate(
-            [heads[64 * g + 16 * h : 64 * g + 16 * (h + 1)] for h in range(4)], axis=1
-        )
+    for k, weight_ref in enumerate((own_ref, first_ref, second_ref, third_ref)):
+        g = lax.rem(lax.axis_index(tp) + 4 - k, 4)
+        mine = heads_ref[pl.ds(pl.multiple_of(64 * g, 64), 64), :].astype(bf16)
+        left = jnp.concatenate([mine[16 * h : 16 * (h + 1)] for h in range(4)], axis=1)
         group = lax.dot_general(
-            left, weight_ref[g], (((1,), (1,)), ((), ())), preferred_element_type=f32
+            left, weight_ref[...], (((1,), (1,)), ((), ())), preferred_element_type=f32
         )
         total = total + group.astype(bf16).astype(f32)
     out_ref[...] = total.astype(bf16)
-    offset = place_ref[1]
+    for c in known:
+        c.wait()
     seqs, positions_dev = keys_out_ref.shape[:2]
+    offset = (lax.axis_index(far) * lax.axis_size(near) + near_place()) * positions_dev
     proposals = key_rows.shape[0]
     for s in range(seqs):
-        first = past_ref[s] + accepted_ref[s] - offset
+        first = lengths[0, s] + lengths[1, s] - offset
 
         @pl.when((first > -proposals) & (first < positions_dev))
         def _():
@@ -304,15 +362,15 @@
                 @pl.when((first + j >= 0) & (first + j < positions_dev))
                 def _():
                     at = jnp.clip(first + j, 0, positions_dev - 1)
-                    copies = [
+                    writes = [
                         pltpu.make_async_copy(rows.at[j], whole.at[s, at], sem.at[k])
                         for k, (rows, whole) in enumerate(
                             ((key_rows, keys_out_ref), (value_rows, values_out_ref))
                         )
                     ]
-                    for c in copies:
+                    for c in writes:
                         c.start()
-                    for c in copies:
+                    for c in writes:
                         c.wait()
 
 
@@ -339,16 +397,16 @@
     positions_dev, heads = cache_keys.shape[1:3]
     nears, fars, tps = (math.prod(lax.axis_size(a) for a in axes) for axes in (near, (far,), (tp,)))
     chunk = tokens // nears
-    near_index, far_index = lax.axis_index(near), lax.axis_index(far)
-    shard = far_index * nears + near_index
-    place = jnp.stack([near_index * chunk + far_index, shard * positions_dev, near_index])
-    place = place.astype(jnp.int32)
-    two_query = jnp.concatenate([query_gain, query_gain])[None]
-    two_key = jnp.concatenate([key_gain, key_gain])[None]
-
-    terms = call(project, shape((tokens, (near_terms + 2) * width), bf16), [vmem] * 4)(
-        hidden_states, w_query, w_key, w_value
-    )
+    terms = call(
+        project,
+        shape((tokens, (near_terms + 2) * width), bf16),
+        [hbm] * 4,
+        scratch_shapes=[
+            pltpu.VMEM(hidden_states.shape, bf16),
+            pltpu.VMEM((3, *w_query.shape), bf16),
+            pltpu.SemaphoreType.DMA((4,)),
+        ],
+    )(hidden_states, w_query, w_key, w_value)
     terms = lax.all_to_all(
         terms.reshape(nears, chunk, -1), near, 0, 0, tiled=True
     )
@@ -363,46 +421,48 @@
         (shape((nears, chunk, width), bf16), shape((8, 128), bf16)),
         [vmem] * 3,
         (vmem, vmem),
-    )(shared, two_query, two_key)
+    )(shared, query_gain[None], key_gain[None])
     query = lax.all_to_all(query, near, 0, 0, tiled=True).reshape(tokens, width)
     flat = (seqs, positions_dev * heads, 128)
-    part, keys_copy, values_copy = call(
-        attend,
+    keys, values, keys_copy, values_copy, limit, under, scale = call(
+        stage,
         (
-            shape((nears, tps, 24, 128), bf16),
-            shape(flat, bf16),
-            shape(flat, bf16),
+            *[shape(flat, bf16)] * 4,
+            shape((8, 128), jnp.int32),
+            shape((seqs, rows, 128), f32),
+            shape((rows, 128), f32),
         ),
-        [smem] * 5 + [vmem] * 4,
-        (vmem, anywhere, anywhere),
-        scratch_shapes=[pltpu.SemaphoreType.DMA((2,))],
-        flops=10000000,
-        room=16,
+        [smem] * 4 + [hbm] * 2,
+        (vmem, vmem, hbm, hbm, vmem, vmem, vmem),
+        scratch_shapes=[pltpu.SemaphoreType.DMA((4,))],
     )(
-        place,
         past_lengths,
         accepted,
         parents,
         lambda_head,
-        query,
-        row,
         cache_keys.reshape(flat),
         cache_values.reshape(flat),
     )
+    part = call(
+        attend, shape((nears, tps, 24, 128), bf16), [vmem] * 7, flops=10000000, room=16
+    )(limit, under, scale, query, row, keys, values)
     part = lax.all_to_all(
         part.reshape(nears * tps, 24, 128), (*near, tp), 0, 0, tiled=True
     )
     part = call(
         combine_near,
         shape((fars, 80, 128), bf16),
-        [smem, vmem, vmem],
+        [vmem, vmem],
         scratch_shapes=[pltpu.VMEM((128, 128), f32)],
-    )(place, part.reshape(nears, tps, 24, 128), row)
+    )(part.reshape(nears, tps, 24, 128), row)
     part = lax.all_to_all(part, far, 0, 0, tiled=True)
     mixed = call(combine_far, shape((nears, 96, 128), bf16), [vmem] * 2)(part, head_gain[None])
     mixed = lax.all_to_all(mixed, near, 0, 0, tiled=True)
-    weight = jnp.broadcast_to(w_output.T[None], (tps, *w_output.T.shape))
-    weight = lax.all_to_all(weight, tp, 0, 0, tiled=True)
+    own = w_output.T
+    weights = [own]
+    for k in range(1, tps):
+        ring = [(i, (i + k) % tps) for i in range(tps)]
+        weights.append(lax.ppermute(own, tp, ring))
     whole = cache_keys.shape
     return call(
         finish,
@@ -411,23 +471,17 @@
             shape(whole, bf16),
             shape(whole, bf16),
         ),
-        [smem] * 3 + [vmem] * 2 + [anywhere] * 2,
-        (vmem, anywhere, anywhere),
+        [hbm] * 2 + [vmem] * 5 + [hbm] * 2,
+        (vmem, hbm, hbm),
         scratch_shapes=[
+            pltpu.VMEM((256, 128), f32),
             pltpu.VMEM((proposals, heads, 128), bf16),
             pltpu.VMEM((proposals, heads, 128), bf16),
+            pltpu.SMEM((2, seqs), jnp.int32),
             pltpu.SemaphoreType.DMA((2,)),
         ],
-        input_output_aliases={5: 1, 6: 2},
-    )(
-        place,
-        past_lengths,
-        accepted,
-        mixed,
-        weight,
-        keys_copy.reshape(whole),
-        values_copy.reshape(whole),
-    )
+        input_output_aliases={7: 1, 8: 2},
+    )(past_lengths, accepted, mixed, *weights, keys_copy.reshape(whole), values_copy.reshape(whole))
 
 
 def solution(mesh):

time: 184 us -> 180 us (0.978)
  blocking collectives: 78.4 us -> 136 us
  waiting for transfers between devices: 40.7 us -> 7.22 us
  starting transfers between devices: 49.3 us -> 19.7 us
    all_to_all x1, blocking collectives: 13.1 us -> 69.8 us  [on_device(): shared = lax.all_to_all(shared, far, 0, 0, tiled=True)]
    all_to_all x2 -> x1, starting transfers between devices: 45.3 us -> 6.19 us  [on_device(): mixed = lax.all_to_all(mixed, near, 0, 0, tiled=True)]
    all_to_all x2 -> x1, waiting for transfers between devices: 34.8 us -> 0.01 us  [on_device(): mixed = lax.all_to_all(mixed, near, 0, 0, tiled=True)]
    ppermute x0 -> x3, starting transfers between devices: none -> 9.49 us  [on_device(): weights.append(lax.ppermute(own, tp, ring))]
    ppermute x0 -> x3, waiting for transfers between devices: none -> 5.43 us  [on_device(): weights.append(lax.ppermute(own, tp, ring))]
    all_to_all x1, waiting for transfers between devices: 5.84 us -> 1.78 us  [on_device(): query = lax.all_to_all(query, near, 0, 0, tiled=True).reshape(tokens, width)]
    pallas_call x3 -> x4, Pallas kernels: 4.06 us -> 5.85 us  [the longest x1 2.58 us: on_device(): call(attend, shape((nears, tps, 24, 128), bf16), [vmem] * 7, flops=100000...]
  transfers between devices with their start and end apart: 3 -> 5, of which waited for: 3 -> 3; matrix products, arithmetic and copies ran while one was open for 0% -> 0% of each run, Pallas kernels for 0% -> 1%
where the time goes in v2:
time: 180 us; the launch traced here: 179 us
  blocking collectives  136 us (76%)
  starting transfers between devices  19.7 us (11%)
  Pallas kernels  9.11 us (5%)
  waiting for transfers between devices  7.22 us (4%)
  local copies, waits for them, and re-layouts  6.54 us (4%)
    all_to_all x1, blocking collectives, on_device(): shared = lax.all_to_all(shared, far, 0, 0, tiled=True)  69.8 us
    all_to_all x1, blocking collectives, on_device(): part = lax.all_to_all(part, far, 0, 0, tiled=True)  32.3 us
    all_to_all x1, blocking collectives, on_device(): lax.all_to_all(terms.reshape(nears, chunk, -1), near, 0, 0, tiled=True)  18 us
    all_to_all x1, blocking collectives, on_device(): lax.all_to_all(part.reshape(nears * tps, 24, 128), (*near, tp), 0, 0, til...  16 us
    ppermute x3, starting transfers between devices, on_device(): weights.append(lax.ppermute(own, tp, ring))  9.49 us
    unnamed x28, local copies, waits for them, and re-layouts  6.54 us
    all_to_all x1, starting transfers between devices, on_device(): mixed = lax.all_to_all(mixed, near, 0, 0, tiled=True)  6.19 us
    ppermute x3, waiting for transfers between devices, on_device(): weights.append(lax.ppermute(own, tp, ring))  5.43 us
  transfers between devices with their start and end apart: 5, of which 3 were waited for; matrix products, arithmetic and copies ran while one was open for 0% of the time, Pallas kernels for 1%

profile of v2, /device:TPU:40, one launch (start us, length us, event | category | flops | bytes accessed | tf_op | source)
XLA Modules:
  0.0 179.5 jit_solution(16016786366277026983)
XLA Ops:
  0.6 0.0 copy-start
  0.6 0.0 copy-start.3
  0.7 0.9 copy-done.3
  1.6 0.0 copy-start.4
  1.6 0.8 copy-done.4
  2.4 0.0 copy-start.5
  2.4 0.8 copy-done.5
  3.2 0.0 copy-start.6
  3.3 0.7 copy-done.6
  4.0 0.7 shard_map.158
  4.7 18.0 %all_to_all.30.arrived_ref = bf16[8,8,2048]{2,1,0:T(8,128)(2,1)S(1)} all-to-all(bf16[8,8,2048]{2,1,0:T(8,128)(2,1)S(1)} %bitcast.14), channel_id=1, replica_groups=mesh['grp'=2,'far'=8,'chip'=4,'core'=2,'tp'=4] {'chip','core'}, dimensions={0} | all-to-all | bytes 524288 | tf_op jit(solution)/shard_map/all_to_all | solution.py:410
  22.7 0.1 shard_map.159
  22.7 69.8 %all_to_all.31.arrived_ref = bf16[8,8,1152]{2,1,0:T(8,128)(2,1)S(1)} all-to-all(bf16[8,8,1152]{2,1,0:T(8,128)(2,1)S(1)} %shard_map.159), channel_id=1, replica_groups=mesh['grp'=2,'far'=8,'chip'=4,'core'=2,'tp'=4] {'far'}, dimensions={0} | all-to-all | bytes 294912 | tf_op jit(solution)/shard_map/all_to_all | solution.py:418
  92.6 0.0 copy-start.10
  92.6 0.0 copy-start.11
  92.6 0.7 copy-done.10
  93.2 0.0 copy-done.11
  93.2 0.7 shard_map.160
  94.0 4.0 %all-to-all-start.2 = ((bf16[8,8,512]{2,1,0:T(8,128)(2,1)}), bf16[8,8,512]{2,1,0:T(8,128)(2,1)S(1)}, u32[]{:S(2)}, u32[]{:S(2)}) async-start(bf16[8,8,512]{2,1,0:T(8,128)(2,1)} %get-tuple-element.15), calls=%async_computation.2 | async-start | bytes 131072 | tf_op jit(solution)/shard_map/all_to_all | solution.py:425
  98.0 0.0 copy-start.7
  98.0 0.0 copy-start.8
  98.0 0.0 copy-start.9
  98.0 0.0 copy-start.12
  98.0 0.0 copy-done
  98.0 0.6 copy-done.7
  98.6 0.0 copy-done.8
  98.6 0.0 copy-done.9
  98.6 0.0 copy-done.12
  98.7 0.0 copy-start.1
  98.7 1.2 copy-done.1
  99.9 2.2 %shard_map.157 = (bf16[4,1024,128]{2,1,0:T(8,128)(2,1)S(1)}, bf16[4,1024,128]{2,1,0:T(8,128)(2,1)S(1)}, bf16[4,1024,128]{2,1,0:T(8,128)(2,1)}, bf16[4,1024,128]{...) custom-call(s32[4]{0:T(128)S(1)} %copy-done.8, s32[4]{0:T(128)S(1)} %copy-done.9, ...), custom_call_target="tpu_custom_call" | custom-call | flops 1000000 | bytes 1000000 | tf_op jit(solution)/shard_map/pallas_call | solution.py:427
  102.1 1.8 all-to-all-done.2
  103.9 2.6 %shard_map.161 = bf16[8,4,24,128]{3,2,1,0:T(8,128)(2,1)S(1)} custom-call(s32[8,128]{1,0:T(8,128)S(1)} %get-tuple-element.12.limit_ref, f32[4,128,128]{2,1,0:T(8,128)S(1)} %get-tuple-element.13.under_ref, f32[128,128]{1,0:T(8,128)S(1)} %get-tuple-element.14.scale_ref, bf16[64,512]{1,0:T(8,128)(2,1)S(1)} %bitcast.17, ...), custom_call_target="tpu_custom_call" | custom-call | flops 10000000 | bytes 1000000 | tf_op jit(solution)/shard_map/pallas_call | solution.py:446
  106.5 16.0 %all_to_all.32 = bf16[32,24,128]{2,1,0:T(8,128)(2,1)S(1)} all-to-all(bf16[32,24,128]{2,1,0:T(8,128)(2,1)S(1)} %bitcast.15), channel_id=1, replica_groups=mesh['grp'=2,'far'=8,'chip'=4,'core'=2,'tp'=4] {'chip','core','tp'}, dimensions={0} | all-to-all | bytes 393216 | tf_op jit(solution)/shard_map/all_to_all | solution.py:449
  122.5 0.4 shard_map.162
  122.9 32.3 %all_to_all.33.arrived_ref = bf16[8,80,128]{2,1,0:T(8,128)(2,1)S(1)} all-to-all(bf16[8,80,128]{2,1,0:T(8,128)(2,1)S(1)} %shard_map.162), channel_id=1, replica_groups=mesh['grp'=2,'far'=8,'chip'=4,'core'=2,'tp'=4] {'far'}, dimensions={0} | all-to-all | bytes 327680 | tf_op jit(solution)/shard_map/all_to_all | solution.py:458
  155.2 0.7 copy-done.13
  155.8 1.1 shard_map.163
  156.9 6.2 %all-to-all-start.5 = ((bf16[8,96,128]{2,1,0:T(8,128)(2,1)}), bf16[8,96,128]{2,1,0:T(8,128)(2,1)S(1)}, u32[]{:S(2)}, u32[]{:S(2)}) async-start(bf16[8,96,128]{2,1,0:T(8,128)(2,1)} %shard_map.163), calls=%async_computation.5 | async-start | bytes 393216 | tf_op jit(solution)/shard_map/all_to_all | solution.py:460
  163.1 0.0 copy-done.2
  163.1 2.8 %collective-permute-start.2 = (bf16[64,512]{1,0:T(8,128)(2,1)S(1)}, bf16[64,512]{1,0:T(8,128)(2,1)S(1)}, u32[]{:S(2)}, u32[]{:S(2)}) collective-permute-start(bf16[64,512]{1,0:T(8,128)(2,1)S(1)} %bitcast.18), channel_id=1, source_target_pairs={{0,3},{1,0},{2,1},{3,2},{4,7},{5,4},{6,5},{7,6},{8,11},{9,8},{10,9... | collective-permute-start | bytes 196616 | tf_op jit(solution)/shard_map/ppermute | solution.py:465
  165.9 4.8 %collective-permute-start.1 = (bf16[64,512]{1,0:T(8,128)(2,1)S(1)}, bf16[64,512]{1,0:T(8,128)(2,1)S(1)}, u32[]{:S(2)}, u32[]{:S(2)}) collective-permute-start(bf16[64,512]{1,0:T(8,128)(2,1)S(1)} %bitcast.19), channel_id=1, source_target_pairs={{0,2},{1,3},{2,0},{3,1},{4,6},{5,7},{6,4},{7,5},{8,10},{9,11},{10,... | collective-permute-start | bytes 196616 | tf_op jit(solution)/shard_map/ppermute | solution.py:465
  170.7 2.0 %collective-permute-start = (bf16[64,512]{1,0:T(8,128)(2,1)S(1)}, bf16[64,512]{1,0:T(8,128)(2,1)S(1)}, u32[]{:S(2)}, u32[]{:S(2)}) collective-permute-start(bf16[64,512]{1,0:T(8,128)(2,1)S(1)} %bitcast.20), channel_id=1, source_target_pairs={{0,1},{1,2},{2,3},{3,0},{4,5},{5,6},{6,7},{7,4},{8,9},{9,10},{10,1... | collective-permute-start | bytes 196616 | tf_op jit(solution)/shard_map/ppermute | solution.py:465
  172.6 0.0 collective-permute-done.2.third_ref
  172.6 0.9 collective-permute-done.1.second_ref
  173.6 4.5 %collective-permute-done.first_ref = bf16[64,512]{1,0:T(8,128)(2,1)S(1)} collective-permute-done((bf16[64,512]{1,0:T(8,128)(2,1)S(1)}, bf16[64,512]{1,0:T(8,128)(2,1)S(1)}, u32[]{:S(2)}, u32[]{:S(2)}) %collective-permute-start) | collective-permute-done | bytes 65568 | tf_op jit(solution)/shard_map/ppermute | solution.py:465
  178.1 0.0 all-to-all-done.5.arrived_ref
  178.1 1.4 shard_map.164
  (2 shorter events, 0.0 us)
Async XLA Ops:
  0.6 97.4 %copy-start = (bf16[4,256,4,128]{3,2,1,0:T(4,128)(2,1)S(1)}, bf16[4,256,4,128]{3,2,1,0:T(4,128)(2,1)}, u32[]{:S(2)}) copy-start(bf16[4,256,4,128]{3,2,1,0:T(4,128)(2,1)} %param.23) | copy-start | bytes 3145732
  0.6 0.9 copy-start.3
  1.6 0.8 copy-start.4
  2.4 0.8 copy-start.5
  3.2 0.7 copy-start.6
  92.6 0.7 copy-start.10
  92.6 0.7 copy-start.11
  94.0 9.9 %all-to-all-start.2 = ((bf16[8,8,512]{2,1,0:T(8,128)(2,1)}), bf16[8,8,512]{2,1,0:T(8,128)(2,1)S(1)}, u32[]{:S(2)}, u32[]{:S(2)}) async-start(bf16[8,8,512]{2,1,0:T(8,128)(2,1)} %get-tuple-element.15), calls=%async_computation.2 | async-start | bytes 131072 | tf_op jit(solution)/shard_map/all_to_all | solution.py:425
  98.0 0.7 copy-start.7
  98.0 0.7 copy-start.8
  98.0 0.7 copy-start.9
  98.0 0.7 copy-start.12
  98.7 1.2 copy-start.1
  155.2 0.7 copy-start.13
  156.9 6.2 %copy-start.2 = (bf16[512,64]{0,1:T(8,128)(2,1)S(1)}, bf16[512,64]{0,1:T(8,128)(2,1)}, u32[]{:S(2)}) copy-start(bf16[512,64]{0,1:T(8,128)(2,1)} %param.22) | copy-start | bytes 196612
  156.9 21.2 %all-to-all-start.5 = ((bf16[8,96,128]{2,1,0:T(8,128)(2,1)}), bf16[8,96,128]{2,1,0:T(8,128)(2,1)S(1)}, u32[]{:S(2)}, u32[]{:S(2)}) async-start(bf16[8,96,128]{2,1,0:T(8,128)(2,1)} %shard_map.163), calls=%async_computation.5 | async-start | bytes 393216 | tf_op jit(solution)/shard_map/all_to_all | solution.py:460
  163.1 9.5 %collective-permute-start.2 = (bf16[64,512]{1,0:T(8,128)(2,1)S(1)}, bf16[64,512]{1,0:T(8,128)(2,1)S(1)}, u32[]{:S(2)}, u32[]{:S(2)}) collective-permute-start(bf16[64,512]{1,0:T(8,128)(2,1)S(1)} %bitcast.18), channel_id=1, source_target_pairs={{0,3},{1,0},{2,1},{3,2},{4,7},{5,4},{6,5},{7,6},{8,11},{9,8},{10,9... | collective-permute-start | bytes 196616 | tf_op jit(solution)/shard_map/ppermute | solution.py:465
  165.9 7.7 %collective-permute-start.1 = (bf16[64,512]{1,0:T(8,128)(2,1)S(1)}, bf16[64,512]{1,0:T(8,128)(2,1)S(1)}, u32[]{:S(2)}, u32[]{:S(2)}) collective-permute-start(bf16[64,512]{1,0:T(8,128)(2,1)S(1)} %bitcast.19), channel_id=1, source_target_pairs={{0,2},{1,3},{2,0},{3,1},{4,6},{5,7},{6,4},{7,5},{8,10},{9,11},{10,... | collective-permute-start | bytes 196616 | tf_op jit(solution)/shard_map/ppermute | solution.py:465
  170.7 7.4 %collective-permute-start = (bf16[64,512]{1,0:T(8,128)(2,1)S(1)}, bf16[64,512]{1,0:T(8,128)(2,1)S(1)}, u32[]{:S(2)}, u32[]{:S(2)}) collective-permute-start(bf16[64,512]{1,0:T(8,128)(2,1)S(1)} %bitcast.20), channel_id=1, source_target_pairs={{0,1},{1,2},{2,3},{3,0},{4,5},{5,6},{6,7},{7,4},{8,9},{9,10},{10,1... | collective-permute-start | bytes 196616 | tf_op jit(solution)/shard_map/ppermute | solution.py:465

commit v3 on v2

--- a/solution.py
+++ b/solution.py
@@ -43,7 +43,7 @@
         in_specs=in_specs,
         out_specs=out_specs,
         interpret=interpreted,
-        compiler_params=pltpu.CompilerParams(vmem_limit_bytes=room << 20),
+        compiler_params=pltpu.CompilerParams(vmem_limit_bytes=int(room * 1024) << 10),
         cost_estimate=pl.CostEstimate(flops=flops, bytes_accessed=1000000, transcendentals=0),
         **rest,
     )
@@ -108,12 +108,12 @@
     return x * lax.rsqrt(mean + epsilon) * gain
 
 
-def finish_rows(arrived_ref, query_gain_ref, key_gain_ref, query_ref, row_ref):
+def finish_rows(arrived_ref, facts_ref, query_ref, row_ref):
+    gains = facts_ref[facts_ref.shape[0] - 8 :]
     width = query_ref.shape[2]
     total, row = arrived_sum(arrived_ref, width, far_terms)
     lane = iota((8, 128), 1)
-    query_gain = jnp.concatenate([query_gain_ref[...]] * 2, axis=1)
-    key_gain = jnp.concatenate([key_gain_ref[...]] * 2, axis=1)
+    query_gain, key_gain = gains[0:1], gains[1:2]
     for i in range(width // 128):
         at = slice(128 * i, 128 * (i + 1))
         part = normed(total[:, at], query_gain, lane, 64).astype(bf16)
@@ -128,15 +128,16 @@
     accepted_ref,
     parents_ref,
     lambda_ref,
+    query_gain_ref,
+    key_gain_ref,
+    head_gain_ref,
     keys_ref,
     values_ref,
     keys_vmem_ref,
     values_vmem_ref,
     keys_out_ref,
     values_out_ref,
-    limit_ref,
-    under_ref,
-    scale_ref,
+    facts_ref,
     sems,
 ):
     taken = [
@@ -165,12 +166,16 @@
     limit = jnp.zeros((8, 128), jnp.int32)
     for s in range(seqs):
         limit = jnp.where(iota((8, 128), 0) == s, past_ref[s] + accepted_ref[s] - offset, limit)
-        under_ref[s] = jnp.where(own_seq == s, under, 0).astype(f32)
-    limit_ref[...] = limit
+        facts_ref[rows * s : rows * (s + 1)] = jnp.where(own_seq == s, under, 0).astype(f32)
     scale = jnp.ones((rows, 128), f32)
     for h in range(4):
         scale = jnp.where(((row & 3) == h) & (((row >> 3) & 1) == 1), lambda_ref[h], scale)
-    scale_ref[...] = scale
+    facts_ref[rows * seqs : rows * (seqs + 1)] = scale
+    last = rows * (seqs + 1)
+    facts_ref[last : last + 8] = limit.astype(f32)
+    gains = [jnp.concatenate([ref[...]] * 2, axis=1) for ref in (query_gain_ref, key_gain_ref)]
+    gains += [head_gain_ref[...], jnp.zeros((5, 128), f32)]
+    facts_ref[last + 8 :] = jnp.concatenate(gains, axis=0)
     for c, d in zip(taken, put):
         c.wait()
         d.start()
@@ -179,9 +184,7 @@
 
 
 def attend(
-    limit_ref,
-    under_ref,
-    scale_ref,
+    facts_ref,
     query_ref,
     row_ref,
     keys_ref,
@@ -199,8 +202,10 @@
     comp_at = (lane >= 64) == (row_comp == 1)
     column = iota((rows, columns), 1)
     same_head = (column & 3) == (iota((rows, columns), 0) & 3)
-    position = jnp.where(same_head, column >> 2, columns)
-    scale = scale_ref[...]
+    position = jnp.where(same_head, (column >> 2).astype(f32), float(columns))
+    scale = facts_ref[rows * seqs : rows * (seqs + 1)]
+    last = rows * (seqs + 1)
+    limits = facts_ref[last : last + 8]
     new_row = row_ref[...].astype(f32)
     new_key = jnp.concatenate([new_row[:4]] * (rows // 4), axis=0)
     new_value = jnp.concatenate([new_row[4:]] * (rows // 4), axis=0)
@@ -218,10 +223,10 @@
             (((1,), (1,)), ((), ())),
             preferred_element_type=f32,
         )
-        visible = position < jnp.minimum(limit_ref[s : s + 1, :1], columns)
+        visible = position < jnp.minimum(limits[s : s + 1, :1], float(columns))
         masked = jnp.where(visible, scores * 0.125, floor_value)
         tree_score = jnp.sum(query * new_key, axis=-1, keepdims=True) * 0.125
-        tree_visible = under_ref[s, :, :1] > 0.5
+        tree_visible = facts_ref[rows * s : rows * (s + 1), :1] > 0.5
         tree_masked = jnp.where(tree_visible, tree_score, floor_value)
         top = jnp.maximum(jnp.max(masked, axis=-1, keepdims=True), tree_masked)
         weights = jnp.where(visible, jnp.exp(masked - top), 0.0)
@@ -401,6 +406,7 @@
         project,
         shape((tokens, (near_terms + 2) * width), bf16),
         [hbm] * 4,
+        room=65182 / 1024,
         scratch_shapes=[
             pltpu.VMEM(hidden_states.shape, bf16),
             pltpu.VMEM((3, *w_query.shape), bf16),
@@ -416,36 +422,37 @@
         [vmem],
     )(terms)
     shared = lax.all_to_all(shared, far, 0, 0, tiled=True)
-    query, row = call(
-        finish_rows,
-        (shape((nears, chunk, width), bf16), shape((8, 128), bf16)),
-        [vmem] * 3,
-        (vmem, vmem),
-    )(shared, query_gain[None], key_gain[None])
-    query = lax.all_to_all(query, near, 0, 0, tiled=True).reshape(tokens, width)
     flat = (seqs, positions_dev * heads, 128)
-    keys, values, keys_copy, values_copy, limit, under, scale = call(
+    keys, values, keys_copy, values_copy, facts = call(
         stage,
         (
             *[shape(flat, bf16)] * 4,
-            shape((8, 128), jnp.int32),
-            shape((seqs, rows, 128), f32),
-            shape((rows, 128), f32),
+            shape((rows * (seqs + 1) + 16, 128), f32),
         ),
-        [smem] * 4 + [hbm] * 2,
-        (vmem, vmem, hbm, hbm, vmem, vmem, vmem),
+        [smem] * 4 + [vmem] * 3 + [hbm] * 2,
+        (vmem, vmem, hbm, hbm, vmem),
         scratch_shapes=[pltpu.SemaphoreType.DMA((4,))],
     )(
         past_lengths,
         accepted,
         parents,
         lambda_head,
+        query_gain[None],
+        key_gain[None],
+        head_gain[None],
         cache_keys.reshape(flat),
         cache_values.reshape(flat),
     )
+    query, row = call(
+        finish_rows,
+        (shape((nears, chunk, width), bf16), shape((8, 128), bf16)),
+        [vmem] * 2,
+        (vmem, vmem),
+    )(shared, facts)
+    query = lax.all_to_all(query, near, 0, 0, tiled=True).reshape(tokens, width)
     part = call(
-        attend, shape((nears, tps, 24, 128), bf16), [vmem] * 7, flops=10000000, room=16
-    )(limit, under, scale, query, row, keys, values)
+        attend, shape((nears, tps, 24, 128), bf16), [vmem] * 5, flops=10000000, room=16
+    )(facts, query, row, keys, values)
     part = lax.all_to_all(
         part.reshape(nears * tps, 24, 128), (*near, tp), 0, 0, tiled=True
     )

time: 180 us -> 177 us (0.983)
  blocking collectives: 136 us -> 75.1 us
  starting transfers between devices: 19.7 us -> 56.6 us
  waiting for transfers between devices: 7.22 us -> 30.7 us
  local copies, waits for them, and re-layouts: 6.54 us -> 1.88 us
  Pallas kernels: 9.11 us -> 11.4 us
    all_to_all x1, blocking collectives: 69.8 us -> 9.7 us  [on_device(): query = lax.all_to_all(query, near, 0, 0, tiled=True).reshape(tokens, width)]
    all_to_all x1, starting transfers between devices: 3.98 us -> 40.9 us  [on_device(): shared = lax.all_to_all(shared, far, 0, 0, tiled=True)]
    all_to_all x1, waiting for transfers between devices: 1.78 us -> 25.2 us  [on_device(): shared = lax.all_to_all(shared, far, 0, 0, tiled=True)]
    unnamed x28 -> x20, local copies, waits for them, and re-layouts: 6.54 us -> 1.88 us
where the time goes in v3:
time: 177 us; the launch traced here: 176 us
  blocking collectives  75.1 us (42%)
  starting transfers between devices  56.6 us (32%)
  waiting for transfers between devices  30.7 us (17%)
  Pallas kernels  11.4 us (6%)
  local copies, waits for them, and re-layouts  1.88 us (1%)
    all_to_all x1, starting transfers between devices, on_device(): shared = lax.all_to_all(shared, far, 0, 0, tiled=True)  40.9 us
    all_to_all x1, blocking collectives, on_device(): part = lax.all_to_all(part, far, 0, 0, tiled=True)  32.2 us
    all_to_all x1, waiting for transfers between devices, on_device(): shared = lax.all_to_all(shared, far, 0, 0, tiled=True)  25.2 us
    all_to_all x1, blocking collectives, on_device(): lax.all_to_all(terms.reshape(nears, chunk, -1), near, 0, 0, tiled=True)  18.3 us
    all_to_all x1, blocking collectives, on_device(): lax.all_to_all(part.reshape(nears * tps, 24, 128), (*near, tp), 0, 0, til...  14.9 us
    all_to_all x1, blocking collectives, on_device(): query = lax.all_to_all(query, near, 0, 0, tiled=True).reshape(tokens, width)  9.7 us
    ppermute x3, starting transfers between devices, on_device(): weights.append(lax.ppermute(own, tp, ring))  9.49 us
    all_to_all x1, starting transfers between devices, on_device(): mixed = lax.all_to_all(mixed, near, 0, 0, tiled=True)  6.19 us
  transfers between devices with their start and end apart: 5, of which 3 were waited for; matrix products, arithmetic and copies ran while one was open for 0% of the time, Pallas kernels for 1%

profile of v3, /device:TPU:40, one launch (start us, length us, event | category | flops | bytes accessed | tf_op | source)
XLA Modules:
  0.0 176.4 jit_solution(3313066241687349895)
XLA Ops:
  0.6 2.0 %shard_map.158 = bf16[64,2048]{1,0:T(8,128)(2,1)} custom-call(bf16[64,64]{1,0:T(8,128)(2,1)} %hidden_ref.1, bf16[64,512]{1,0:T(8,128)(2,1)} %query_ref.1, bf16[64,512]{1,0:T(8,128)(2,1)} %key_ref.1, bf16[64,512]{1,0:T(8,128)(2,1)} %value_ref.1), custom_call_target="tpu_custom_call" | custom-call | flops 1000000 | bytes 1000000 | tf_op jit(solution)/shard_map/pallas_call | solution.py:405
  2.7 0.0 copy-start
  2.7 18.3 %all_to_all.30.arrived_ref = bf16[8,8,2048]{2,1,0:T(8,128)(2,1)S(1)} all-to-all(bf16[8,8,2048]{2,1,0:T(8,128)(2,1)} %bitcast.27), channel_id=1, replica_groups=mesh['grp'=2,'far'=8,'chip'=4,'core'=2,'tp'=4] {'chip','core'}, dimensions={0} | all-to-all | bytes 524288 | tf_op jit(solution)/shard_map/all_to_all | solution.py:416
  21.0 0.7 shard_map.159
  21.7 0.0 copy-start.7
  21.7 0.0 copy-start.8
  21.7 0.0 copy-start.9
  21.7 40.9 %all-to-all-start.1 = ((bf16[8,8,1152]{2,1,0:T(8,128)(2,1)}), bf16[8,8,1152]{2,1,0:T(8,128)(2,1)}, u32[]{:S(2)}, u32[]{:S(2)}) async-start(bf16[8,8,1152]{2,1,0:T(8,128)(2,1)} %shard_map.159), calls=%async_computation.1 | async-start | bytes 294912 | tf_op jit(solution)/shard_map/all_to_all | solution.py:424
  62.6 0.0 copy-start.3
  62.6 0.0 copy-start.4
  62.6 0.0 copy-start.5
  62.6 0.0 copy-start.6
  62.7 0.0 copy-done
  62.7 0.0 copy-done.7
  62.7 0.0 copy-done.8
  62.7 0.0 copy-done.9
  62.7 0.6 copy-done.3
  63.3 0.0 copy-done.4
  63.3 0.0 copy-done.5
  63.3 0.0 copy-done.6
  63.3 0.0 copy-start.1
  63.3 1.2 copy-done.1
  64.5 2.2 %shard_map.157 = (bf16[4,1024,128]{2,1,0:T(8,128)(2,1)S(1)}, bf16[4,1024,128]{2,1,0:T(8,128)(2,1)S(1)}, bf16[4,1024,128]{2,1,0:T(8,128)(2,1)}, bf16[4,1024,128]{2,1,0:T(8,128)(2,1)}, f32[656,128]{1,0:T(8,128)S(1)}) custom-call(s32[4]{0:T(128)S(1)} %copy-done.5, s32[4]{0:T(128)S(1)} %copy-done.6, s32[4,16]{1,0:T(4,128)S(1)} %copy-done.3, f32[4]{0:T(128)S(1)} %copy-done.7, ...), custom_call_target="tpu_custom_call" | custom-call | flops 1000000 | bytes 1000000 | tf_op jit(solution)/shard_map/pallas_call | solution.py:426
  66.8 25.2 %all-to-all-done.1.arrived_ref = bf16[8,8,1152]{2,1,0:T(8,128)(2,1)} async-done(((bf16[8,8,1152]{2,1,0:T(8,128)(2,1)}), bf16[8,8,1152]{2,1,0:T(8,128)(2,1)}, u32[]{:S(2)}, u32[]{:S(2)}) %all-to-all-start.1) | async-done | bytes 147488 | tf_op jit(solution)/shard_map/all_to_all | solution.py:424
  92.0 1.0 shard_map.160
  93.0 9.7 %all_to_all.31 = bf16[8,8,512]{2,1,0:T(8,128)(2,1)S(1)} all-to-all(bf16[8,8,512]{2,1,0:T(8,128)(2,1)S(1)} %get-tuple-element.11), channel_id=1, replica_groups=mesh['grp'=2,'far'=8,'chip'=4,'core'=2,'tp'=4] {'chip','core'}, dimensions={0} | all-to-all | bytes 131072 | tf_op jit(solution)/shard_map/all_to_all | solution.py:452
  102.7 2.6 %shard_map.161 = bf16[8,4,24,128]{3,2,1,0:T(8,128)(2,1)S(1)} custom-call(f32[656,128]{1,0:T(8,128)S(1)} %get-tuple-element.10.facts_ref, bf16[64,512]{1,0:T(8,128)(2,1)S(1)} %bitcast.16, bf16[8,128]{1,0:T(8,128)(2,1)S(1)} %get-tuple-element.12.row_ref, bf16[4,1024,128]{2,1,0:T(8,128)(2,1)S(1)} %get-tuple-element.13.keys_ref, ...), custom_call_target="tpu_custom_call" | custom-call | flops 10000000 | bytes 1000000 | tf_op jit(solution)/shard_map/pallas_call | solution.py:453
  105.3 14.9 %all_to_all.32 = bf16[32,24,128]{2,1,0:T(8,128)(2,1)S(1)} all-to-all(bf16[32,24,128]{2,1,0:T(8,128)(2,1)S(1)} %bitcast.14), channel_id=1, replica_groups=mesh['grp'=2,'far'=8,'chip'=4,'core'=2,'tp'=4] {'chip','core','tp'}, dimensions={0} | all-to-all | bytes 393216 | tf_op jit(solution)/shard_map/all_to_all | solution.py:456
  120.2 0.4 shard_map.162
  120.5 32.2 %all_to_all.33.arrived_ref = bf16[8,80,128]{2,1,0:T(8,128)(2,1)S(1)} all-to-all(bf16[8,80,128]{2,1,0:T(8,128)(2,1)S(1)} %shard_map.162), channel_id=1, replica_groups=mesh['grp'=2,'far'=8,'chip'=4,'core'=2,'tp'=4] {'far'}, dimensions={0} | all-to-all | bytes 327680 | tf_op jit(solution)/shard_map/all_to_all | solution.py:465
  152.8 1.1 shard_map.163
  153.8 0.0 copy-start.2
  153.8 6.2 %all-to-all-start.5 = ((bf16[8,96,128]{2,1,0:T(8,128)(2,1)}), bf16[8,96,128]{2,1,0:T(8,128)(2,1)S(1)}, u32[]{:S(2)}, u32[]{:S(2)}) async-start(bf16[8,96,128]{2,1,0:T(8,128)(2,1)} %shard_map.163), calls=%async_computation.5 | async-start | bytes 393216 | tf_op jit(solution)/shard_map/all_to_all | solution.py:467
  160.0 0.0 copy-done.2
  160.0 2.8 %collective-permute-start.2 = (bf16[64,512]{1,0:T(8,128)(2,1)S(1)}, bf16[64,512]{1,0:T(8,128)(2,1)S(1)}, u32[]{:S(2)}, u32[]{:S(2)}) collective-permute-start(bf16[64,512]{1,0:T(8,128)(2,1)S(1)} %bitcast.17), channel_id=1, source_target_pairs={{0,3},{1,0},{2,1},{3,2},{4,7},{5,4},{6,5},{7,6},{8,11},{9,8},{10,9... | collective-permute-start | bytes 196616 | tf_op jit(solution)/shard_map/ppermute | solution.py:472
  162.8 4.8 %collective-permute-start.1 = (bf16[64,512]{1,0:T(8,128)(2,1)S(1)}, bf16[64,512]{1,0:T(8,128)(2,1)S(1)}, u32[]{:S(2)}, u32[]{:S(2)}) collective-permute-start(bf16[64,512]{1,0:T(8,128)(2,1)S(1)} %bitcast.18), channel_id=1, source_target_pairs={{0,2},{1,3},{2,0},{3,1},{4,6},{5,7},{6,4},{7,5},{8,10},{9,11},{10,... | collective-permute-start | bytes 196616 | tf_op jit(solution)/shard_map/ppermute | solution.py:472
  167.6 2.0 %collective-permute-start = (bf16[64,512]{1,0:T(8,128)(2,1)S(1)}, bf16[64,512]{1,0:T(8,128)(2,1)S(1)}, u32[]{:S(2)}, u32[]{:S(2)}) collective-permute-start(bf16[64,512]{1,0:T(8,128)(2,1)S(1)} %bitcast.19), channel_id=1, source_target_pairs={{0,1},{1,2},{2,3},{3,0},{4,5},{5,6},{6,7},{7,4},{8,9},{9,10},{10,1... | collective-permute-start | bytes 196616 | tf_op jit(solution)/shard_map/ppermute | solution.py:472
  169.5 0.0 collective-permute-done.2.third_ref
  169.5 0.9 collective-permute-done.1.second_ref
  170.5 4.5 %collective-permute-done.first_ref = bf16[64,512]{1,0:T(8,128)(2,1)S(1)} collective-permute-done((bf16[64,512]{1,0:T(8,128)(2,1)S(1)}, bf16[64,512]{1,0:T(8,128)(2,1)S(1)}, u32[]{:S(2)}, u32[]{:S(2)}) %collective-permute-start) | collective-permute-done | bytes 65568 | tf_op jit(solution)/shard_map/ppermute | solution.py:472
  175.0 0.0 all-to-all-done.5.arrived_ref
  175.0 1.4 shard_map.164
Async XLA Ops:
  2.7 60.0 %copy-start = (bf16[4,256,4,128]{3,2,1,0:T(4,128)(2,1)S(1)}, bf16[4,256,4,128]{3,2,1,0:T(4,128)(2,1)}, u32[]{:S(2)}) copy-start(bf16[4,256,4,128]{3,2,1,0:T(4,128)(2,1)} %param.23) | copy-start | bytes 3145732
  21.7 40.9 %copy-start.7 = (f32[4]{0:T(128)S(1)}, f32[4]{0:T(128)}, u32[]{:S(2)}) copy-start(f32[4]{0:T(128)} %lambda_ref.1) | copy-start | bytes 52
  21.7 40.9 %copy-start.8 = (f32[64]{0:T(128)S(1)}, f32[64]{0:T(128)}, u32[]{:S(2)}) copy-start(f32[64]{0:T(128)} %param.18) | copy-start | bytes 772
  21.7 41.0 %copy-start.9 = (f32[64]{0:T(128)S(1)}, f32[64]{0:T(128)}, u32[]{:S(2)}) copy-start(f32[64]{0:T(128)} %param.19) | copy-start | bytes 772
  21.7 70.3 %all-to-all-start.1 = ((bf16[8,8,1152]{2,1,0:T(8,128)(2,1)}), bf16[8,8,1152]{2,1,0:T(8,128)(2,1)}, u32[]{:S(2)}, u32[]{:S(2)}) async-start(bf16[8,8,1152]{2,1,0:T(8,128)(2,1)} %shard_map.159), calls=%async_computation.1 | async-start | bytes 294912 | tf_op jit(solution)/shard_map/all_to_all | solution.py:424
  62.6 0.7 copy-start.3
  62.6 0.7 copy-start.4
  62.6 0.7 copy-start.5
  62.6 0.7 copy-start.6
  63.3 1.2 copy-start.1
  153.8 6.2 %copy-start.2 = (bf16[512,64]{0,1:T(8,128)(2,1)S(1)}, bf16[512,64]{0,1:T(8,128)(2,1)}, u32[]{:S(2)}) copy-start(bf16[512,64]{0,1:T(8,128)(2,1)} %param.22) | copy-start | bytes 196612
  153.8 21.2 %all-to-all-start.5 = ((bf16[8,96,128]{2,1,0:T(8,128)(2,1)}), bf16[8,96,128]{2,1,0:T(8,128)(2,1)S(1)}, u32[]{:S(2)}, u32[]{:S(2)}) async-start(bf16[8,96,128]{2,1,0:T(8,128)(2,1)} %shard_map.163), calls=%async_computation.5 | async-start | bytes 393216 | tf_op jit(solution)/shard_map/all_to_all | solution.py:467
  160.0 9.5 %collective-permute-start.2 = (bf16[64,512]{1,0:T(8,128)(2,1)S(1)}, bf16[64,512]{1,0:T(8,128)(2,1)S(1)}, u32[]{:S(2)}, u32[]{:S(2)}) collective-permute-start(bf16[64,512]{1,0:T(8,128)(2,1)S(1)} %bitcast.17), channel_id=1, source_target_pairs={{0,3},{1,0},{2,1},{3,2},{4,7},{5,4},{6,5},{7,6},{8,11},{9,8},{10,9... | collective-permute-start | bytes 196616 | tf_op jit(solution)/shard_map/ppermute | solution.py:472
  162.8 7.7 %collective-permute-start.1 = (bf16[64,512]{1,0:T(8,128)(2,1)S(1)}, bf16[64,512]{1,0:T(8,128)(2,1)S(1)}, u32[]{:S(2)}, u32[]{:S(2)}) collective-permute-start(bf16[64,512]{1,0:T(8,128)(2,1)S(1)} %bitcast.18), channel_id=1, source_target_pairs={{0,2},{1,3},{2,0},{3,1},{4,6},{5,7},{6,4},{7,5},{8,10},{9,11},{10,... | collective-permute-start | bytes 196616 | tf_op jit(solution)/shard_map/ppermute | solution.py:472
  167.6 7.4 %collective-permute-start = (bf16[64,512]{1,0:T(8,128)(2,1)S(1)}, bf16[64,512]{1,0:T(8,128)(2,1)S(1)}, u32[]{:S(2)}, u32[]{:S(2)}) collective-permute-start(bf16[64,512]{1,0:T(8,128)(2,1)S(1)} %bitcast.19), channel_id=1, source_target_pairs={{0,1},{1,2},{2,3},{3,0},{4,5},{5,6},{6,7},{7,4},{8,9},{9,10},{10,1... | collective-permute-start | bytes 196616 | tf_op jit(solution)/shard_map/ppermute | solution.py:472

commit v4 on v3

--- a/solution.py
+++ b/solution.py
@@ -90,13 +90,13 @@
     return query, total[:, terms * width :]
 
 
-def sum_near(arrived_ref, out_ref, *, width):
+def sum_near(arrived_ref, out_ref, *, width, order):
     query, rest = arrived_sum(arrived_ref, width, near_terms)
     terms = terms_of(query, far_terms)
-    for k in range(out_ref.shape[0]):
+    for k, to in enumerate(order):
         for i, term in enumerate(terms):
             out_ref[k, :, i * width : (i + 1) * width] = term
-        row = [rest[k : k + 1, 128 * i : 128 * (i + 1)] for i in range(8)]
+        row = [rest[to : to + 1, 128 * i : 128 * (i + 1)] for i in range(8)]
         out_ref[k, :, far_terms * width :] = jnp.concatenate(row, axis=0).astype(bf16)
 
 
@@ -281,7 +281,7 @@
         out_ref[k, 72:80, :] = row_ref[...]
 
 
-def combine_far(arrived_ref, gain_ref, out_ref):
+def combine_far(arrived_ref, gain_ref, out_ref, *, order):
     sources = arrived_ref.shape[0]
     tops, sums = zip(*[stat_rows(arrived_ref[q, 64:72, :].astype(f32)) for q in range(sources)])
     top = functools.reduce(jnp.maximum, tops)
@@ -301,8 +301,9 @@
     for k in range(out_ref.shape[0]):
         for g in range(4):
             out_ref[k, 8 * g : 8 * (g + 1), :] = heads[g]
-        for q in range(sources):
-            out_ref[k, 32 + 8 * q : 40 + 8 * q, :] = arrived_ref[q, 72:80, :]
+        for q, source in enumerate(order):
+            at = 32 + 8 * source
+            out_ref[k, at : at + 8, :] = arrived_ref[q, 72:80, :]
 
 
 def finish(
@@ -402,6 +403,9 @@
     positions_dev, heads = cache_keys.shape[1:3]
     nears, fars, tps = (math.prod(lax.axis_size(a) for a in axes) for axes in (near, (far,), (tp,)))
     chunk = tokens // nears
+    apart = [min(b + 1, fars - 1 - b) for b in range(fars)]
+    first_order = sorted(range(fars), key=lambda b: -apart[b])
+    second_order = list(reversed(range(fars)))
     terms = call(
         project,
         shape((tokens, (near_terms + 2) * width), bf16),
@@ -417,11 +421,13 @@
         terms.reshape(nears, chunk, -1), near, 0, 0, tiled=True
     )
     shared = call(
-        functools.partial(sum_near, width=width),
+        functools.partial(sum_near, width=width, order=first_order),
         shape((fars, chunk, far_terms * width + 128), bf16),
         [vmem],
     )(terms)
-    shared = lax.all_to_all(shared, far, 0, 0, tiled=True)
+    shared = lax.all_to_all(
+        shared, far, 0, 0, tiled=True, axis_index_groups=[first_order]
+    )
     flat = (seqs, positions_dev * heads, 128)
     keys, values, keys_copy, values_copy, facts = call(
         stage,
@@ -462,8 +468,14 @@
         [vmem, vmem],
         scratch_shapes=[pltpu.VMEM((128, 128), f32)],
     )(part.reshape(nears, tps, 24, 128), row)
-    part = lax.all_to_all(part, far, 0, 0, tiled=True)
-    mixed = call(combine_far, shape((nears, 96, 128), bf16), [vmem] * 2)(part, head_gain[None])
+    part = lax.all_to_all(
+        part, far, 0, 0, tiled=True, axis_index_groups=[second_order]
+    )
+    mixed = call(
+        functools.partial(combine_far, order=second_order),
+        shape((nears, 96, 128), bf16),
+        [vmem] * 2,
+    )(part, head_gain[None])
     mixed = lax.all_to_all(mixed, near, 0, 0, tiled=True)
     own = w_output.T
     weights = [own]

time: 177 us -> 191 us (1.079)
  starting transfers between devices: 56.6 us -> 71.8 us
  waiting for transfers between devices: 30.7 us -> 16.2 us
  blocking collectives: 75.1 us -> 88.3 us
    all_to_all x1, starting transfers between devices: 40.9 us -> 55.9 us  [on_device(): lax.all_to_all(shared, far, 0, 0, tiled=True, axis_index_groups=[first_or...]
    all_to_all x1, waiting for transfers between devices: 25.2 us -> 10.7 us  [on_device(): lax.all_to_all(shared, far, 0, 0, tiled=True, axis_index_groups=[first_or...]
    all_to_all x1, blocking collectives: 32.2 us -> 45.1 us  [on_device(): lax.all_to_all(part, far, 0, 0, tiled=True, axis_index_groups=[second_ord...]
where the time goes in v4:
time: 191 us; the launch traced here: 190 us
  blocking collectives  88.3 us (46%)
  starting transfers between devices  71.8 us (38%)
  waiting for transfers between devices  16.2 us (8%)
  Pallas kernels  11.4 us (6%)
    all_to_all x1, starting transfers between devices, on_device(): lax.all_to_all(shared, far, 0, 0, tiled=True, axis_index_groups=[first_or...  55.9 us
    all_to_all x1, blocking collectives, on_device(): lax.all_to_all(part, far, 0, 0, tiled=True, axis_index_groups=[second_ord...  45.1 us
    all_to_all x1, blocking collectives, on_device(): lax.all_to_all(terms.reshape(nears, chunk, -1), near, 0, 0, tiled=True)  18.3 us
    all_to_all x1, blocking collectives, on_device(): lax.all_to_all(part.reshape(nears * tps, 24, 128), (*near, tp), 0, 0, til...  14.9 us
    all_to_all x1, waiting for transfers between devices, on_device(): lax.all_to_all(shared, far, 0, 0, tiled=True, axis_index_groups=[first_or...  10.7 us
    all_to_all x1, blocking collectives, on_device(): query = lax.all_to_all(query, near, 0, 0, tiled=True).reshape(tokens, width)  9.94 us
    ppermute x3, starting transfers between devices, on_device(): weights.append(lax.ppermute(own, tp, ring))  8.38 us
    all_to_all x1, starting transfers between devices, on_device(): mixed = lax.all_to_all(mixed, near, 0, 0, tiled=True)  7.57 us
  transfers between devices with their start and end apart: 5, of which 3 were waited for; matrix products, arithmetic and copies ran while one was open for 0% of the time, Pallas kernels for 1%

profile of v4, /device:TPU:40, one launch (start us, length us, event | category | flops | bytes accessed | tf_op | source)
XLA Modules:
  0.0 190.3 jit_solution(9947104425069410699)
XLA Ops:
  0.6 2.0 %shard_map.158 = bf16[64,2048]{1,0:T(8,128)(2,1)} custom-call(bf16[64,64]{1,0:T(8,128)(2,1)} %hidden_ref.1, bf16[64,512]{1,0:T(8,128)(2,1)} %query_ref.1, bf16[64,512]{1,0:T(8,128)(2,1)} %key_ref.1, bf16[64,512]{1,0:T(8,128)(2,1)} %value_ref.1), custom_call_target="tpu_custom_call" | custom-call | flops 1000000 | bytes 1000000 | tf_op jit(solution)/shard_map/pallas_call | solution.py:409
  2.7 0.0 copy-start
  2.7 18.3 %all_to_all.30.arrived_ref = bf16[8,8,2048]{2,1,0:T(8,128)(2,1)S(1)} all-to-all(bf16[8,8,2048]{2,1,0:T(8,128)(2,1)} %bitcast.27), channel_id=1, replica_groups=mesh['grp'=2,'far'=8,'chip'=4,'core'=2,'tp'=4] {'chip','core'}, dimensions={0} | all-to-all | bytes 524288 | tf_op jit(solution)/shard_map/all_to_all | solution.py:420
  21.0 0.7 shard_map.159
  21.7 0.0 copy-start.7
  21.7 0.0 copy-start.8
  21.7 0.0 copy-start.9
  21.7 55.9 %all-to-all-start.1 = ((bf16[8,8,1152]{2,1,0:T(8,128)(2,1)}), bf16[8,8,1152]{2,1,0:T(8,128)(2,1)}, u32[]{:S(2)}, u32[]{:S(2)}) async-start(bf16[8,8,1152]{2,1,0:T(8,128)(2,1)} %shard_map.159), calls=%async_computation.1 | async-start | bytes 294912 | tf_op jit(solution)/shard_map/all_to_all | solution.py:428
  77.6 0.0 copy-start.3
  77.6 0.0 copy-start.4
  77.6 0.0 copy-start.5
  77.6 0.0 copy-start.6
  77.6 0.0 copy-done
  77.6 0.0 copy-done.7
  77.6 0.0 copy-done.8
  77.7 0.0 copy-done.9
  77.7 0.6 copy-done.3
  78.3 0.0 copy-done.4
  78.3 0.0 copy-done.5
  78.3 0.0 copy-done.6
  78.3 0.0 copy-start.1
  78.3 1.2 copy-done.1
  79.5 2.2 %shard_map.157 = (bf16[4,1024,128]{2,1,0:T(8,128)(2,1)S(1)}, bf16[4,1024,128]{2,1,0:T(8,128)(2,1)S(1)}, bf16[4,1024,128]{2,1,0:T(8,128)(2,1)}, bf16[4,1024,128]{2,1,0:T(8,128)(2,1)}, f32[656,128]{1,0:T(8,128)S(1)}) custom-call(s32[4]{0:T(128)S(1)} %copy-done.5, s32[4]{0:T(128)S(1)} %copy-done.6, s32[4,16]{1,0:T(4,128)S(1)} %copy-done.3, f32[4]{0:T(128)S(1)} %copy-done.7, ...), custom_call_target="tpu_custom_call" | custom-call | flops 1000000 | bytes 1000000 | tf_op jit(solution)/shard_map/pallas_call | solution.py:432
  81.7 10.7 %all-to-all-done.1.arrived_ref = bf16[8,8,1152]{2,1,0:T(8,128)(2,1)} async-done(((bf16[8,8,1152]{2,1,0:T(8,128)(2,1)}), bf16[8,8,1152]{2,1,0:T(8,128)(2,1)}, u32[]{:S(2)}, u32[]{:S(2)}) %all-to-all-start.1) | async-done | bytes 147488 | tf_op jit(solution)/shard_map/all_to_all | solution.py:428
  92.5 1.0 shard_map.160
  93.5 9.9 %all_to_all.31 = bf16[8,8,512]{2,1,0:T(8,128)(2,1)S(1)} all-to-all(bf16[8,8,512]{2,1,0:T(8,128)(2,1)S(1)} %get-tuple-element.11), channel_id=1, replica_groups=mesh['grp'=2,'far'=8,'chip'=4,'core'=2,'tp'=4] {'chip','core'}, dimensions={0} | all-to-all | bytes 131072 | tf_op jit(solution)/shard_map/all_to_all | solution.py:458
  103.5 2.6 %shard_map.161 = bf16[8,4,24,128]{3,2,1,0:T(8,128)(2,1)S(1)} custom-call(f32[656,128]{1,0:T(8,128)S(1)} %get-tuple-element.10.facts_ref, bf16[64,512]{1,0:T(8,128)(2,1)S(1)} %bitcast.16, bf16[8,128]{1,0:T(8,128)(2,1)S(1)} %get-tuple-element.12.row_ref, bf16[4,1024,128]{2,1,0:T(8,128)(2,1)S(1)} %get-tuple-element.13.keys_ref, ...), custom_call_target="tpu_custom_call" | custom-call | flops 10000000 | bytes 1000000 | tf_op jit(solution)/shard_map/pallas_call | solution.py:459
  106.1 14.9 %all_to_all.32 = bf16[32,24,128]{2,1,0:T(8,128)(2,1)S(1)} all-to-all(bf16[32,24,128]{2,1,0:T(8,128)(2,1)S(1)} %bitcast.14), channel_id=1, replica_groups=mesh['grp'=2,'far'=8,'chip'=4,'core'=2,'tp'=4] {'chip','core','tp'}, dimensions={0} | all-to-all | bytes 393216 | tf_op jit(solution)/shard_map/all_to_all | solution.py:462
  120.9 0.4 shard_map.162
  121.3 45.1 %all_to_all.33.arrived_ref = bf16[8,80,128]{2,1,0:T(8,128)(2,1)S(1)} all-to-all(bf16[8,80,128]{2,1,0:T(8,128)(2,1)S(1)} %shard_map.162), channel_id=1, replica_groups={{224,192,160,128,96,64,32,0},{225,193,161,129,97,65,33,1},{226,194,162,..., dimensions={0} | all-to-all | bytes 327680 | tf_op jit(solution)/shard_map/all_to_all | solution.py:471
  166.4 1.1 shard_map.163
  167.5 0.0 copy-start.2
  167.5 7.6 %all-to-all-start.5 = ((bf16[8,96,128]{2,1,0:T(8,128)(2,1)}), bf16[8,96,128]{2,1,0:T(8,128)(2,1)S(1)}, u32[]{:S(2)}, u32[]{:S(2)}) async-start(bf16[8,96,128]{2,1,0:T(8,128)(2,1)} %shard_map.163), calls=%async_computation.5 | async-start | bytes 393216 | tf_op jit(solution)/shard_map/all_to_all | solution.py:479
  175.1 0.0 copy-done.2
  175.1 3.1 %collective-permute-start.2 = (bf16[64,512]{1,0:T(8,128)(2,1)S(1)}, bf16[64,512]{1,0:T(8,128)(2,1)S(1)}, u32[]{:S(2)}, u32[]{:S(2)}) collective-permute-start(bf16[64,512]{1,0:T(8,128)(2,1)S(1)} %bitcast.17), channel_id=1, source_target_pairs={{0,3},{1,0},{2,1},{3,2},{4,7},{5,4},{6,5},{7,6},{8,11},{9,8},{10,9... | collective-permute-start | bytes 196616 | tf_op jit(solution)/shard_map/ppermute | solution.py:484
  178.2 3.3 %collective-permute-start.1 = (bf16[64,512]{1,0:T(8,128)(2,1)S(1)}, bf16[64,512]{1,0:T(8,128)(2,1)S(1)}, u32[]{:S(2)}, u32[]{:S(2)}) collective-permute-start(bf16[64,512]{1,0:T(8,128)(2,1)S(1)} %bitcast.18), channel_id=1, source_target_pairs={{0,2},{1,3},{2,0},{3,1},{4,6},{5,7},{6,4},{7,5},{8,10},{9,11},{10,... | collective-permute-start | bytes 196616 | tf_op jit(solution)/shard_map/ppermute | solution.py:484
  181.5 2.0 %collective-permute-start = (bf16[64,512]{1,0:T(8,128)(2,1)S(1)}, bf16[64,512]{1,0:T(8,128)(2,1)S(1)}, u32[]{:S(2)}, u32[]{:S(2)}) collective-permute-start(bf16[64,512]{1,0:T(8,128)(2,1)S(1)} %bitcast.19), channel_id=1, source_target_pairs={{0,1},{1,2},{2,3},{3,0},{4,5},{5,6},{6,7},{7,4},{8,9},{9,10},{10,1... | collective-permute-start | bytes 196616 | tf_op jit(solution)/shard_map/ppermute | solution.py:484
  183.5 0.0 collective-permute-done.2.third_ref
  183.5 2.4 %collective-permute-done.1.second_ref = bf16[64,512]{1,0:T(8,128)(2,1)S(1)} collective-permute-done((bf16[64,512]{1,0:T(8,128)(2,1)S(1)}, bf16[64,512]{1,0:T(8,128)(2,1)S(1)}, u32[]{:S(2)}, u32[]{:S(2)}) %collective-permute-start.1) | collective-permute-done | bytes 65568 | tf_op jit(solution)/shard_map/ppermute | solution.py:484
  185.9 3.0 %collective-permute-done.first_ref = bf16[64,512]{1,0:T(8,128)(2,1)S(1)} collective-permute-done((bf16[64,512]{1,0:T(8,128)(2,1)S(1)}, bf16[64,512]{1,0:T(8,128)(2,1)S(1)}, u32[]{:S(2)}, u32[]{:S(2)}) %collective-permute-start) | collective-permute-done | bytes 65568 | tf_op jit(solution)/shard_map/ppermute | solution.py:484
  188.9 0.0 all-to-all-done.5.arrived_ref
  188.9 1.4 shard_map.164
Async XLA Ops:
  2.7 75.0 %copy-start = (bf16[4,256,4,128]{3,2,1,0:T(4,128)(2,1)S(1)}, bf16[4,256,4,128]{3,2,1,0:T(4,128)(2,1)}, u32[]{:S(2)}) copy-start(bf16[4,256,4,128]{3,2,1,0:T(4,128)(2,1)} %param.23) | copy-start | bytes 3145732
  21.7 55.9 %copy-start.7 = (f32[4]{0:T(128)S(1)}, f32[4]{0:T(128)}, u32[]{:S(2)}) copy-start(f32[4]{0:T(128)} %lambda_ref.1) | copy-start | bytes 52
  21.7 55.9 %copy-start.8 = (f32[64]{0:T(128)S(1)}, f32[64]{0:T(128)}, u32[]{:S(2)}) copy-start(f32[64]{0:T(128)} %param.18) | copy-start | bytes 772
  21.7 55.9 %copy-start.9 = (f32[64]{0:T(128)S(1)}, f32[64]{0:T(128)}, u32[]{:S(2)}) copy-start(f32[64]{0:T(128)} %param.19) | copy-start | bytes 772
  21.7 70.7 %all-to-all-start.1 = ((bf16[8,8,1152]{2,1,0:T(8,128)(2,1)}), bf16[8,8,1152]{2,1,0:T(8,128)(2,1)}, u32[]{:S(2)}, u32[]{:S(2)}) async-start(bf16[8,8,1152]{2,1,0:T(8,128)(2,1)} %shard_map.159), calls=%async_computation.1 | async-start | bytes 294912 | tf_op jit(solution)/shard_map/all_to_all | solution.py:428
  77.6 0.7 copy-start.3
  77.6 0.7 copy-start.4
  77.6 0.7 copy-start.5
  77.6 0.7 copy-start.6
  78.3 1.2 copy-start.1
  167.5 7.6 %copy-start.2 = (bf16[512,64]{0,1:T(8,128)(2,1)S(1)}, bf16[512,64]{0,1:T(8,128)(2,1)}, u32[]{:S(2)}) copy-start(bf16[512,64]{0,1:T(8,128)(2,1)} %param.22) | copy-start | bytes 196612
  167.5 21.4 %all-to-all-start.5 = ((bf16[8,96,128]{2,1,0:T(8,128)(2,1)}), bf16[8,96,128]{2,1,0:T(8,128)(2,1)S(1)}, u32[]{:S(2)}, u32[]{:S(2)}) async-start(bf16[8,96,128]{2,1,0:T(8,128)(2,1)} %shard_map.163), calls=%async_computation.5 | async-start | bytes 393216 | tf_op jit(solution)/shard_map/all_to_all | solution.py:479
  175.1 8.4 %collective-permute-start.2 = (bf16[64,512]{1,0:T(8,128)(2,1)S(1)}, bf16[64,512]{1,0:T(8,128)(2,1)S(1)}, u32[]{:S(2)}, u32[]{:S(2)}) collective-permute-start(bf16[64,512]{1,0:T(8,128)(2,1)S(1)} %bitcast.17), channel_id=1, source_target_pairs={{0,3},{1,0},{2,1},{3,2},{4,7},{5,4},{6,5},{7,6},{8,11},{9,8},{10,9... | collective-permute-start | bytes 196616 | tf_op jit(solution)/shard_map/ppermute | solution.py:484
  178.2 7.7 %collective-permute-start.1 = (bf16[64,512]{1,0:T(8,128)(2,1)S(1)}, bf16[64,512]{1,0:T(8,128)(2,1)S(1)}, u32[]{:S(2)}, u32[]{:S(2)}) collective-permute-start(bf16[64,512]{1,0:T(8,128)(2,1)S(1)} %bitcast.18), channel_id=1, source_target_pairs={{0,2},{1,3},{2,0},{3,1},{4,6},{5,7},{6,4},{7,5},{8,10},{9,11},{10,... | collective-permute-start | bytes 196616 | tf_op jit(solution)/shard_map/ppermute | solution.py:484
  181.5 7.4 %collective-permute-start = (bf16[64,512]{1,0:T(8,128)(2,1)S(1)}, bf16[64,512]{1,0:T(8,128)(2,1)S(1)}, u32[]{:S(2)}, u32[]{:S(2)}) collective-permute-start(bf16[64,512]{1,0:T(8,128)(2,1)S(1)} %bitcast.19), channel_id=1, source_target_pairs={{0,1},{1,2},{2,3},{3,0},{4,5},{5,6},{6,7},{7,4},{8,9},{9,10},{10,1... | collective-permute-start | bytes 196616 | tf_op jit(solution)/shard_map/ppermute | solution.py:484

commit v5 on v3

--- a/solution.py
+++ b/solution.py
@@ -138,15 +138,17 @@
     keys_out_ref,
     values_out_ref,
     facts_ref,
+    raw,
+    wide,
     sems,
 ):
     taken = [
-        pltpu.make_async_copy(keys_ref, keys_vmem_ref, sems.at[0]),
-        pltpu.make_async_copy(values_ref, values_vmem_ref, sems.at[1]),
+        pltpu.make_async_copy(keys_ref, raw.at[0], sems.at[0]),
+        pltpu.make_async_copy(values_ref, raw.at[1], sems.at[1]),
     ]
     put = [
-        pltpu.make_async_copy(keys_vmem_ref, keys_out_ref, sems.at[2]),
-        pltpu.make_async_copy(values_vmem_ref, values_out_ref, sems.at[3]),
+        pltpu.make_async_copy(raw.at[0], keys_out_ref, sems.at[2]),
+        pltpu.make_async_copy(raw.at[1], values_out_ref, sems.at[3]),
     ]
     for c in taken:
         c.start()
@@ -162,23 +164,29 @@
         above = jnp.where(parent >= 0, (below >> jnp.maximum(parent, 0)) & 1, 0)
         below = below | (jnp.where(own_order == j, 1, above) << j)
     row = iota((rows, 128), 0)
-    under = (below >> (2 * (row >> 4) + ((row >> 2) & 1))) & 1
+    under = (below >> (2 * ((row >> 2) & 7) + (row & 1))) & 1
     limit = jnp.zeros((8, 128), jnp.int32)
     for s in range(seqs):
         limit = jnp.where(iota((8, 128), 0) == s, past_ref[s] + accepted_ref[s] - offset, limit)
         facts_ref[rows * s : rows * (s + 1)] = jnp.where(own_seq == s, under, 0).astype(f32)
     scale = jnp.ones((rows, 128), f32)
     for h in range(4):
-        scale = jnp.where(((row & 3) == h) & (((row >> 3) & 1) == 1), lambda_ref[h], scale)
+        scale = jnp.where(((row >> 5) == h) & (((row >> 1) & 1) == 1), lambda_ref[h], scale)
     facts_ref[rows * seqs : rows * (seqs + 1)] = scale
     last = rows * (seqs + 1)
     facts_ref[last : last + 8] = limit.astype(f32)
     gains = [jnp.concatenate([ref[...]] * 2, axis=1) for ref in (query_gain_ref, key_gain_ref)]
     gains += [head_gain_ref[...], jnp.zeros((5, 128), f32)]
     facts_ref[last + 8 :] = jnp.concatenate(gains, axis=0)
-    for c, d in zip(taken, put):
-        c.wait()
-        d.start()
+    heads = keys_vmem_ref.shape[0] // seqs
+    for k, out_ref in enumerate((keys_vmem_ref, values_vmem_ref)):
+        taken[k].wait()
+        put[k].start()
+        for q in range(seqs):
+            wide[...] = raw[k, q].astype(f32)
+            for h in range(heads):
+                part = wide[pl.ds(h, out_ref.shape[1], stride=heads), :]
+                out_ref[q * heads + h] = part.astype(bf16)
     for d in put:
         d.wait()
 
@@ -191,54 +199,61 @@
     values_ref,
     out_ref,
 ):
-    seqs, columns = keys_ref.shape[:2]
+    seqs = out_ref.shape[1]
+    heads = keys_ref.shape[0] // seqs
+    positions_dev = keys_ref.shape[1]
     proposals = query_ref.shape[0] // seqs
-    row = iota((rows, 128), 0)
-    lane = iota((rows, 128), 1)
-    row_head, row_comp = row & 3, (row >> 3) & 1
-    row_order = 2 * (row >> 4) + ((row >> 2) & 1)
-    spread = (iota((rows, proposals), 1) == row_order[:, :proposals]).astype(bf16)
-    head_at = [row_head == h for h in range(4)]
-    comp_at = (lane >= 64) == (row_comp == 1)
-    column = iota((rows, columns), 1)
-    same_head = (column & 3) == (iota((rows, columns), 0) & 3)
-    position = jnp.where(same_head, (column >> 2).astype(f32), float(columns))
-    scale = facts_ref[rows * seqs : rows * (seqs + 1)]
+    count = rows // heads
+    line = iota((count, 128), 0)
+    line_order = 2 * (line >> 2) + (line & 1)
+    spread = (iota((count, proposals), 1) == line_order[:, :proposals]).astype(bf16)
+    comp_at = (iota((count, 128), 1) >= 64) == (((line >> 1) & 1) == 1)
+    row = iota((rows, rows), 0)
+    lane = iota((rows, rows), 1)
+    sent = (lane == count * (row & 3) + (row >> 2)).astype(bf16)
     last = rows * (seqs + 1)
     limits = facts_ref[last : last + 8]
+    scale = facts_ref[rows * seqs : last]
+    position = iota((count, positions_dev), 1).astype(f32)
     new_row = row_ref[...].astype(f32)
-    new_key = jnp.concatenate([new_row[:4]] * (rows // 4), axis=0)
-    new_value = jnp.concatenate([new_row[4:]] * (rows // 4), axis=0)
     for s in range(seqs):
         wide = jnp.dot(
             spread, query_ref[s * proposals : (s + 1) * proposals, :], preferred_element_type=f32
         )
-        query = jnp.zeros((rows, 128), f32)
-        for h in range(4):
-            query = jnp.where(head_at[h], wide[:, 128 * h : 128 * (h + 1)], query)
-        query = jnp.where(comp_at, query, 0.0)
-        scores = lax.dot_general(
-            query.astype(bf16),
-            keys_ref[s],
-            (((1,), (1,)), ((), ())),
-            preferred_element_type=f32,
-        )
-        visible = position < jnp.minimum(limits[s : s + 1, :1], float(columns))
-        masked = jnp.where(visible, scores * 0.125, floor_value)
-        tree_score = jnp.sum(query * new_key, axis=-1, keepdims=True) * 0.125
-        tree_visible = facts_ref[rows * s : rows * (s + 1), :1] > 0.5
-        tree_masked = jnp.where(tree_visible, tree_score, floor_value)
-        top = jnp.maximum(jnp.max(masked, axis=-1, keepdims=True), tree_masked)
-        weights = jnp.where(visible, jnp.exp(masked - top), 0.0)
-        tree_weight = jnp.where(tree_visible, jnp.exp(tree_masked - top), 0.0)
-        total = jnp.sum(weights, axis=-1, keepdims=True) + tree_weight
-        acc = jnp.dot(weights.astype(bf16), values_ref[s], preferred_element_type=f32)
-        acc = (acc + tree_weight.astype(bf16).astype(f32) * new_value) * scale
-        acc = acc.astype(bf16)
+        visible = position < jnp.minimum(limits[s : s + 1, :1], float(positions_dev))
+        tree_visible = facts_ref[rows * s : rows * s + count, :1] > 0.5
+        accs, tops, totals = [], [], []
+        for h in range(heads):
+            query = jnp.where(comp_at, wide[:, 128 * h : 128 * (h + 1)], 0.0)
+            scores = lax.dot_general(
+                query.astype(bf16),
+                keys_ref[s * heads + h],
+                (((1,), (1,)), ((), ())),
+                preferred_element_type=f32,
+            )
+            masked = jnp.where(visible, scores * 0.125, floor_value)
+            tree_score = jnp.sum(query * new_row[h : h + 1], axis=-1, keepdims=True) * 0.125
+            tree_masked = jnp.where(tree_visible, tree_score, floor_value)
+            top = jnp.maximum(jnp.max(masked, axis=-1, keepdims=True), tree_masked)
+            weights = jnp.where(visible, jnp.exp(masked - top), 0.0)
+            tree_weight = jnp.where(tree_visible, jnp.exp(tree_masked - top), 0.0)
+            acc = jnp.dot(
+                weights.astype(bf16), values_ref[s * heads + h], preferred_element_type=f32
+            )
+            value = new_row[heads + h : heads + h + 1]
+            accs.append(acc + tree_weight.astype(bf16).astype(f32) * value)
+            tops.append(top)
+            totals.append(jnp.sum(weights, axis=-1, keepdims=True) + tree_weight)
+        acc = jnp.concatenate(accs, axis=0) * scale
+        top = jnp.concatenate(tops, axis=0)
+        total = jnp.concatenate(totals, axis=0)
         stats = jnp.zeros((rows, 128), f32)
         for k, part in enumerate((*parts_of(top), *parts_of(total))):
             stats = jnp.where(lane == k, part, stats)
-        stats = jnp.transpose(stats)[:8].astype(bf16)
+        both = jnp.concatenate([acc.astype(bf16), stats.astype(bf16)], axis=1)
+        both = jnp.dot(sent, both, preferred_element_type=f32)
+        acc = both[:, :128].astype(bf16)
+        stats = jnp.transpose(both[:, 128:])[:8].astype(bf16)
         for r in range(out_ref.shape[0]):
             out_ref[r, s, :16, :] = acc[16 * r : 16 * (r + 1)]
             out_ref[r, s, 16:, :] = stats
@@ -426,12 +441,18 @@
     keys, values, keys_copy, values_copy, facts = call(
         stage,
         (
-            *[shape(flat, bf16)] * 4,
+            *[shape((seqs * heads, positions_dev, 128), bf16)] * 2,
+            *[shape(flat, bf16)] * 2,
             shape((rows * (seqs + 1) + 16, 128), f32),
         ),
         [smem] * 4 + [vmem] * 3 + [hbm] * 2,
         (vmem, vmem, hbm, hbm, vmem),
-        scratch_shapes=[pltpu.SemaphoreType.DMA((4,))],
+        scratch_shapes=[
+            pltpu.VMEM((2, *flat), bf16),
+            pltpu.VMEM(flat[1:], f32),
+            pltpu.SemaphoreType.DMA((4,)),
+        ],
+        room=8,
     )(
         past_lengths,
         accepted,

time: 177 us -> 180 us (1.017)
  Pallas kernels: 11.4 us -> 14.6 us
    pallas_call x1, Pallas kernels: 2.61 us -> 5.84 us  [on_device(): call(attend, shape((nears, tps, 24, 128), bf16), [vmem] * 5, flops=100000...]
where the time goes in v5:
time: 180 us
  blocking collectives  75.1 us (42%)
  starting transfers between devices  56.6 us (31%)
  waiting for transfers between devices  30.7 us (17%)
  Pallas kernels  14.6 us (8%)
  local copies, waits for them, and re-layouts  1.88 us (1%)
    all_to_all x1, starting transfers between devices, on_device(): shared = lax.all_to_all(shared, far, 0, 0, tiled=True)  40.9 us
    all_to_all x1, blocking collectives, on_device(): part = lax.all_to_all(part, far, 0, 0, tiled=True)  32.2 us
    all_to_all x1, waiting for transfers between devices, on_device(): shared = lax.all_to_all(shared, far, 0, 0, tiled=True)  25.2 us
    all_to_all x1, blocking collectives, on_device(): lax.all_to_all(terms.reshape(nears, chunk, -1), near, 0, 0, tiled=True)  18.3 us
    all_to_all x1, blocking collectives, on_device(): lax.all_to_all(part.reshape(nears * tps, 24, 128), (*near, tp), 0, 0, til...  14.9 us
    all_to_all x1, blocking collectives, on_device(): query = lax.all_to_all(query, near, 0, 0, tiled=True).reshape(tokens, width)  9.7 us
    ppermute x3, starting transfers between devices, on_device(): weights.append(lax.ppermute(own, tp, ring))  9.49 us
    all_to_all x1, starting transfers between devices, on_device(): mixed = lax.all_to_all(mixed, near, 0, 0, tiled=True)  6.19 us
  transfers between devices with their start and end apart: 5, of which 3 were waited for; matrix products, arithmetic and copies ran while one was open for 0% of the time, Pallas kernels for 1%

profile of v5, /device:TPU:40, one launch (start us, length us, event | category | flops | bytes accessed | tf_op | source)
XLA Modules:
  0.0 179.6 jit_solution(6044462750334537181)
XLA Ops:
  0.6 2.0 %shard_map.158 = bf16[64,2048]{1,0:T(8,128)(2,1)} custom-call(bf16[64,64]{1,0:T(8,128)(2,1)} %hidden_ref.1, bf16[64,512]{1,0:T(8,128)(2,1)} %query_ref.1, bf16[64,512]{1,0:T(8,128)(2,1)} %key_ref.1, bf16[64,512]{1,0:T(8,128)(2,1)} %value_ref.1), custom_call_target="tpu_custom_call" | custom-call | flops 1000000 | bytes 1000000 | tf_op jit(solution)/shard_map/pallas_call | solution.py:420
  2.7 0.0 copy-start
  2.7 18.3 %all_to_all.30.arrived_ref = bf16[8,8,2048]{2,1,0:T(8,128)(2,1)S(1)} all-to-all(bf16[8,8,2048]{2,1,0:T(8,128)(2,1)} %bitcast.27), channel_id=1, replica_groups=mesh['grp'=2,'far'=8,'chip'=4,'core'=2,'tp'=4] {'chip','core'}, dimensions={0} | all-to-all | bytes 524288 | tf_op jit(solution)/shard_map/all_to_all | solution.py:431
  21.0 0.7 shard_map.159
  21.7 0.0 copy-start.7
  21.7 0.0 copy-start.8
  21.7 0.0 copy-start.9
  21.7 40.9 %all-to-all-start.1 = ((bf16[8,8,1152]{2,1,0:T(8,128)(2,1)}), bf16[8,8,1152]{2,1,0:T(8,128)(2,1)}, u32[]{:S(2)}, u32[]{:S(2)}) async-start(bf16[8,8,1152]{2,1,0:T(8,128)(2,1)} %shard_map.159), calls=%async_computation.1 | async-start | bytes 294912 | tf_op jit(solution)/shard_map/all_to_all | solution.py:439
  62.6 0.0 copy-start.3
  62.6 0.0 copy-start.4
  62.6 0.0 copy-start.5
  62.6 0.0 copy-start.6
  62.7 0.0 copy-done
  62.7 0.0 copy-done.7
  62.7 0.0 copy-done.8
  62.7 0.0 copy-done.9
  62.7 0.6 copy-done.3
  63.3 0.0 copy-done.4
  63.3 0.0 copy-done.5
  63.3 0.0 copy-done.6
  63.3 0.0 copy-start.1
  63.3 1.2 copy-done.1
  64.5 2.2 %shard_map.157 = (bf16[16,256,128]{2,1,0:T(8,128)(2,1)S(1)}, bf16[16,256,128]{2,1,0:T(8,128)(2,1)S(1)}, bf16[4,1024,128]{2,1,0:T(8,128)(2,1)}, bf16[4,1024,128]{2,1,0:T(8,128)(2,1)}, f32[656,128]{1,0:T(8,128)S(1)}) custom-call(s32[4]{0:T(128)S(1)} %copy-done.5, s32[4]{0:T(128)S(1)} %copy-done.6, s32[4,16]{1,0:T(4,128)S(1)} %copy-done.3, f32[4]{0:T(128)S(1)} %copy-done.7, ...), custom_call_target="tpu_custom_call" | custom-call | flops 1000000 | bytes 1000000 | tf_op jit(solution)/shard_map/pallas_call | solution.py:441
  66.8 25.2 %all-to-all-done.1.arrived_ref = bf16[8,8,1152]{2,1,0:T(8,128)(2,1)} async-done(((bf16[8,8,1152]{2,1,0:T(8,128)(2,1)}), bf16[8,8,1152]{2,1,0:T(8,128)(2,1)}, u32[]{:S(2)}, u32[]{:S(2)}) %all-to-all-start.1) | async-done | bytes 147488 | tf_op jit(solution)/shard_map/all_to_all | solution.py:439
  92.0 1.0 shard_map.160
  93.0 9.7 %all_to_all.31 = bf16[8,8,512]{2,1,0:T(8,128)(2,1)S(1)} all-to-all(bf16[8,8,512]{2,1,0:T(8,128)(2,1)S(1)} %get-tuple-element.11), channel_id=1, replica_groups=mesh['grp'=2,'far'=8,'chip'=4,'core'=2,'tp'=4] {'chip','core'}, dimensions={0} | all-to-all | bytes 131072 | tf_op jit(solution)/shard_map/all_to_all | solution.py:473
  102.7 5.8 %shard_map.161 = bf16[8,4,24,128]{3,2,1,0:T(8,128)(2,1)S(1)} custom-call(f32[656,128]{1,0:T(8,128)S(1)} %get-tuple-element.10.facts_ref, bf16[64,512]{1,0:T(8,128)(2,1)S(1)} %bitcast.16, bf16[8,128]{1,0:T(8,128)(2,1)S(1)} %get-tuple-element.12.row_ref, bf16[16,256,128]{2,1,0:T(8,128)(2,1)S(1)} %get-tuple-element.13.keys_ref, ...), custom_call_target="tpu_custom_call" | custom-call | flops 10000000 | bytes 1000000 | tf_op jit(solution)/shard_map/pallas_call | solution.py:474
  108.6 14.9 %all_to_all.32 = bf16[32,24,128]{2,1,0:T(8,128)(2,1)S(1)} all-to-all(bf16[32,24,128]{2,1,0:T(8,128)(2,1)S(1)} %bitcast.14), channel_id=1, replica_groups=mesh['grp'=2,'far'=8,'chip'=4,'core'=2,'tp'=4] {'chip','core','tp'}, dimensions={0} | all-to-all | bytes 393216 | tf_op jit(solution)/shard_map/all_to_all | solution.py:477
  123.4 0.4 shard_map.162
  123.8 32.2 %all_to_all.33.arrived_ref = bf16[8,80,128]{2,1,0:T(8,128)(2,1)S(1)} all-to-all(bf16[8,80,128]{2,1,0:T(8,128)(2,1)S(1)} %shard_map.162), channel_id=1, replica_groups=mesh['grp'=2,'far'=8,'chip'=4,'core'=2,'tp'=4] {'far'}, dimensions={0} | all-to-all | bytes 327680 | tf_op jit(solution)/shard_map/all_to_all | solution.py:486
  156.0 1.1 shard_map.163
  157.1 0.0 copy-start.2
  157.1 6.2 %all-to-all-start.5 = ((bf16[8,96,128]{2,1,0:T(8,128)(2,1)}), bf16[8,96,128]{2,1,0:T(8,128)(2,1)S(1)}, u32[]{:S(2)}, u32[]{:S(2)}) async-start(bf16[8,96,128]{2,1,0:T(8,128)(2,1)} %shard_map.163), calls=%async_computation.5 | async-start | bytes 393216 | tf_op jit(solution)/shard_map/all_to_all | solution.py:488
  163.3 0.0 copy-done.2
  163.3 2.8 %collective-permute-start.2 = (bf16[64,512]{1,0:T(8,128)(2,1)S(1)}, bf16[64,512]{1,0:T(8,128)(2,1)S(1)}, u32[]{:S(2)}, u32[]{:S(2)}) collective-permute-start(bf16[64,512]{1,0:T(8,128)(2,1)S(1)} %bitcast.17), channel_id=1, source_target_pairs={{0,3},{1,0},{2,1},{3,2},{4,7},{5,4},{6,5},{7,6},{8,11},{9,8},{10,9... | collective-permute-start | bytes 196616 | tf_op jit(solution)/shard_map/ppermute | solution.py:493
  166.0 4.8 %collective-permute-start.1 = (bf16[64,512]{1,0:T(8,128)(2,1)S(1)}, bf16[64,512]{1,0:T(8,128)(2,1)S(1)}, u32[]{:S(2)}, u32[]{:S(2)}) collective-permute-start(bf16[64,512]{1,0:T(8,128)(2,1)S(1)} %bitcast.18), channel_id=1, source_target_pairs={{0,2},{1,3},{2,0},{3,1},{4,6},{5,7},{6,4},{7,5},{8,10},{9,11},{10,... | collective-permute-start | bytes 196616 | tf_op jit(solution)/shard_map/ppermute | solution.py:493
  170.8 2.0 %collective-permute-start = (bf16[64,512]{1,0:T(8,128)(2,1)S(1)}, bf16[64,512]{1,0:T(8,128)(2,1)S(1)}, u32[]{:S(2)}, u32[]{:S(2)}) collective-permute-start(bf16[64,512]{1,0:T(8,128)(2,1)S(1)} %bitcast.19), channel_id=1, source_target_pairs={{0,1},{1,2},{2,3},{3,0},{4,5},{5,6},{6,7},{7,4},{8,9},{9,10},{10,1... | collective-permute-start | bytes 196616 | tf_op jit(solution)/shard_map/ppermute | solution.py:493
  172.8 0.0 collective-permute-done.2.third_ref
  172.8 0.9 collective-permute-done.1.second_ref
  173.7 4.5 %collective-permute-done.first_ref = bf16[64,512]{1,0:T(8,128)(2,1)S(1)} collective-permute-done((bf16[64,512]{1,0:T(8,128)(2,1)S(1)}, bf16[64,512]{1,0:T(8,128)(2,1)S(1)}, u32[]{:S(2)}, u32[]{:S(2)}) %collective-permute-start) | collective-permute-done | bytes 65568 | tf_op jit(solution)/shard_map/ppermute | solution.py:493
  178.2 0.0 all-to-all-done.5.arrived_ref
  178.2 1.4 shard_map.164
Async XLA Ops:
  2.7 60.0 %copy-start = (bf16[4,256,4,128]{3,2,1,0:T(4,128)(2,1)S(1)}, bf16[4,256,4,128]{3,2,1,0:T(4,128)(2,1)}, u32[]{:S(2)}) copy-start(bf16[4,256,4,128]{3,2,1,0:T(4,128)(2,1)} %param.23) | copy-start | bytes 3145732
  21.7 40.9 %copy-start.7 = (f32[4]{0:T(128)S(1)}, f32[4]{0:T(128)}, u32[]{:S(2)}) copy-start(f32[4]{0:T(128)} %lambda_ref.1) | copy-start | bytes 52
  21.7 40.9 %copy-start.8 = (f32[64]{0:T(128)S(1)}, f32[64]{0:T(128)}, u32[]{:S(2)}) copy-start(f32[64]{0:T(128)} %param.18) | copy-start | bytes 772
  21.7 41.0 %copy-start.9 = (f32[64]{0:T(128)S(1)}, f32[64]{0:T(128)}, u32[]{:S(2)}) copy-start(f32[64]{0:T(128)} %param.19) | copy-start | bytes 772
  21.7 70.3 %all-to-all-start.1 = ((bf16[8,8,1152]{2,1,0:T(8,128)(2,1)}), bf16[8,8,1152]{2,1,0:T(8,128)(2,1)}, u32[]{:S(2)}, u32[]{:S(2)}) async-start(bf16[8,8,1152]{2,1,0:T(8,128)(2,1)} %shard_map.159), calls=%async_computation.1 | async-start | bytes 294912 | tf_op jit(solution)/shard_map/all_to_all | solution.py:439
  62.6 0.7 copy-start.3
  62.6 0.7 copy-start.4
  62.6 0.7 copy-start.5
  62.6 0.7 copy-start.6
  63.3 1.2 copy-start.1
  157.1 6.2 %copy-start.2 = (bf16[512,64]{0,1:T(8,128)(2,1)S(1)}, bf16[512,64]{0,1:T(8,128)(2,1)}, u32[]{:S(2)}) copy-start(bf16[512,64]{0,1:T(8,128)(2,1)} %param.22) | copy-start | bytes 196612
  157.1 21.2 %all-to-all-start.5 = ((bf16[8,96,128]{2,1,0:T(8,128)(2,1)}), bf16[8,96,128]{2,1,0:T(8,128)(2,1)S(1)}, u32[]{:S(2)}, u32[]{:S(2)}) async-start(bf16[8,96,128]{2,1,0:T(8,128)(2,1)} %shard_map.163), calls=%async_computation.5 | async-start | bytes 393216 | tf_op jit(solution)/shard_map/all_to_all | solution.py:488
  163.3 9.5 %collective-permute-start.2 = (bf16[64,512]{1,0:T(8,128)(2,1)S(1)}, bf16[64,512]{1,0:T(8,128)(2,1)S(1)}, u32[]{:S(2)}, u32[]{:S(2)}) collective-permute-start(bf16[64,512]{1,0:T(8,128)(2,1)S(1)} %bitcast.17), channel_id=1, source_target_pairs={{0,3},{1,0},{2,1},{3,2},{4,7},{5,4},{6,5},{7,6},{8,11},{9,8},{10,9... | collective-permute-start | bytes 196616 | tf_op jit(solution)/shard_map/ppermute | solution.py:493
  166.0 7.7 %collective-permute-start.1 = (bf16[64,512]{1,0:T(8,128)(2,1)S(1)}, bf16[64,512]{1,0:T(8,128)(2,1)S(1)}, u32[]{:S(2)}, u32[]{:S(2)}) collective-permute-start(bf16[64,512]{1,0:T(8,128)(2,1)S(1)} %bitcast.18), channel_id=1, source_target_pairs={{0,2},{1,3},{2,0},{3,1},{4,6},{5,7},{6,4},{7,5},{8,10},{9,11},{10,... | collective-permute-start | bytes 196616 | tf_op jit(solution)/shard_map/ppermute | solution.py:493
  170.8 7.4 %collective-permute-start = (bf16[64,512]{1,0:T(8,128)(2,1)S(1)}, bf16[64,512]{1,0:T(8,128)(2,1)S(1)}, u32[]{:S(2)}, u32[]{:S(2)}) collective-permute-start(bf16[64,512]{1,0:T(8,128)(2,1)S(1)} %bitcast.19), channel_id=1, source_target_pairs={{0,1},{1,2},{2,3},{3,0},{4,5},{5,6},{6,7},{7,4},{8,9},{9,10},{10,1... | collective-permute-start | bytes 196616 | tf_op jit(solution)/shard_map/ppermute | solution.py:493

commit v6 on v5

--- a/solution.py
+++ b/solution.py
@@ -17,7 +17,9 @@
 interpreted = False
 near_chips = 4
 near_cores = 2
-far, chip, core, tp = "far", "chip", "core", "tp"
+half, quarter, chip, core, tp = "half", "quarter", "chip", "core", "tp"
+far = (half, quarter)
+listed = (quarter, half)
 near = (chip, core)
 near_terms = 2
 far_terms = 2
@@ -90,13 +92,13 @@
     return query, total[:, terms * width :]
 
 
-def sum_near(arrived_ref, out_ref, *, width):
+def sum_near(arrived_ref, out_ref, *, width, order):
     query, rest = arrived_sum(arrived_ref, width, near_terms)
     terms = terms_of(query, far_terms)
-    for k in range(out_ref.shape[0]):
+    for k, to in enumerate(order):
         for i, term in enumerate(terms):
             out_ref[k, :, i * width : (i + 1) * width] = term
-        row = [rest[k : k + 1, 128 * i : 128 * (i + 1)] for i in range(8)]
+        row = [rest[to : to + 1, 128 * i : 128 * (i + 1)] for i in range(8)]
         out_ref[k, :, far_terms * width :] = jnp.concatenate(row, axis=0).astype(bf16)
 
 
@@ -214,49 +216,92 @@
     last = rows * (seqs + 1)
     limits = facts_ref[last : last + 8]
     scale = facts_ref[rows * seqs : last]
-    position = iota((count, positions_dev), 1).astype(f32)
+    position = iota((rows, positions_dev), 1).astype(f32)
     new_row = row_ref[...].astype(f32)
-    for s in range(seqs):
-        wide = jnp.dot(
+    new_key, new_value = (
+        jnp.concatenate(
+            [jnp.broadcast_to(new_row[h : h + 1], (count, 128)) for h in at], axis=0
+        )
+        for at in (range(heads), range(heads, 2 * heads))
+    )
+    every = range(seqs)
+    parts = [slice(count * h, count * (h + 1)) for h in range(heads)]
+    wide = [
+        jnp.dot(
             spread, query_ref[s * proposals : (s + 1) * proposals, :], preferred_element_type=f32
         )
-        visible = position < jnp.minimum(limits[s : s + 1, :1], float(positions_dev))
-        tree_visible = facts_ref[rows * s : rows * s + count, :1] > 0.5
-        accs, tops, totals = [], [], []
-        for h in range(heads):
-            query = jnp.where(comp_at, wide[:, 128 * h : 128 * (h + 1)], 0.0)
-            scores = lax.dot_general(
-                query.astype(bf16),
-                keys_ref[s * heads + h],
-                (((1,), (1,)), ((), ())),
-                preferred_element_type=f32,
-            )
-            masked = jnp.where(visible, scores * 0.125, floor_value)
-            tree_score = jnp.sum(query * new_row[h : h + 1], axis=-1, keepdims=True) * 0.125
-            tree_masked = jnp.where(tree_visible, tree_score, floor_value)
-            top = jnp.maximum(jnp.max(masked, axis=-1, keepdims=True), tree_masked)
-            weights = jnp.where(visible, jnp.exp(masked - top), 0.0)
-            tree_weight = jnp.where(tree_visible, jnp.exp(tree_masked - top), 0.0)
-            acc = jnp.dot(
-                weights.astype(bf16), values_ref[s * heads + h], preferred_element_type=f32
-            )
-            value = new_row[heads + h : heads + h + 1]
-            accs.append(acc + tree_weight.astype(bf16).astype(f32) * value)
-            tops.append(top)
-            totals.append(jnp.sum(weights, axis=-1, keepdims=True) + tree_weight)
-        acc = jnp.concatenate(accs, axis=0) * scale
-        top = jnp.concatenate(tops, axis=0)
-        total = jnp.concatenate(totals, axis=0)
-        stats = jnp.zeros((rows, 128), f32)
-        for k, part in enumerate((*parts_of(top), *parts_of(total))):
-            stats = jnp.where(lane == k, part, stats)
-        both = jnp.concatenate([acc.astype(bf16), stats.astype(bf16)], axis=1)
-        both = jnp.dot(sent, both, preferred_element_type=f32)
-        acc = both[:, :128].astype(bf16)
-        stats = jnp.transpose(both[:, 128:])[:8].astype(bf16)
+        for s in every
+    ]
+    query = [
+        jnp.concatenate(
+            [jnp.where(comp_at, wide[s][:, 128 * h : 128 * (h + 1)], 0.0) for h in range(heads)],
+            axis=0,
+        )
+        for s in every
+    ]
+    scores = [
+        jnp.concatenate(
+            [
+                lax.dot_general(
+                    query[s][parts[h]].astype(bf16),
+                    keys_ref[s * heads + h],
+                    (((1,), (1,)), ((), ())),
+                    preferred_element_type=f32,
+                )
+                for h in range(heads)
+            ],
+            axis=0,
+        )
+        for s in every
+    ]
+    tree = [jnp.sum(query[s] * new_key, axis=-1, keepdims=True) * 0.125 for s in every]
+    visible = [
+        position < jnp.minimum(limits[s : s + 1, :1], float(positions_dev)) for s in every
+    ]
+    tree_visible = [facts_ref[rows * s : rows * (s + 1), :1] > 0.5 for s in every]
+    masked = [jnp.where(visible[s], scores[s] * 0.125, floor_value) for s in every]
+    tree = [jnp.where(tree_visible[s], tree[s], floor_value) for s in every]
+    top = [jnp.maximum(jnp.max(masked[s], axis=-1, keepdims=True), tree[s]) for s in every]
+    weights = [jnp.where(visible[s], jnp.exp(masked[s] - top[s]), 0.0) for s in every]
+    tree_weight = [jnp.where(tree_visible[s], jnp.exp(tree[s] - top[s]), 0.0) for s in every]
+    total = [jnp.sum(weights[s], axis=-1, keepdims=True) + tree_weight[s] for s in every]
+    acc = [
+        jnp.concatenate(
+            [
+                jnp.dot(
+                    weights[s][parts[h]].astype(bf16),
+                    values_ref[s * heads + h],
+                    preferred_element_type=f32,
+                )
+                for h in range(heads)
+            ],
+            axis=0,
+        )
+        for s in every
+    ]
+    acc = [
+        (acc[s] + tree_weight[s].astype(bf16).astype(f32) * new_value) * scale for s in every
+    ]
+    stats = []
+    for s in every:
+        stat = jnp.zeros((rows, 128), f32)
+        for k, part in enumerate((*parts_of(top[s]), *parts_of(total[s]))):
+            stat = jnp.where(lane == k, part, stat)
+        stats.append(stat)
+    both = [
+        jnp.dot(
+            sent,
+            jnp.concatenate([acc[s].astype(bf16), stats[s].astype(bf16)], axis=1),
+            preferred_element_type=f32,
+        )
+        for s in every
+    ]
+    stats = [jnp.transpose(both[s][:, 128:])[:8].astype(bf16) for s in every]
+    for s in every:
+        sums = both[s][:, :128].astype(bf16)
         for r in range(out_ref.shape[0]):
-            out_ref[r, s, :16, :] = acc[16 * r : 16 * (r + 1)]
-            out_ref[r, s, 16:, :] = stats
+            out_ref[r, s, :16, :] = sums[16 * r : 16 * (r + 1)]
+            out_ref[r, s, 16:, :] = stats[s]
 
 
 def stat_rows(stats):
@@ -296,7 +341,7 @@
         out_ref[k, 72:80, :] = row_ref[...]
 
 
-def combine_far(arrived_ref, gain_ref, out_ref):
+def combine_far(arrived_ref, gain_ref, out_ref, *, order):
     sources = arrived_ref.shape[0]
     tops, sums = zip(*[stat_rows(arrived_ref[q, 64:72, :].astype(f32)) for q in range(sources)])
     top = functools.reduce(jnp.maximum, tops)
@@ -316,8 +361,9 @@
     for k in range(out_ref.shape[0]):
         for g in range(4):
             out_ref[k, 8 * g : 8 * (g + 1), :] = heads[g]
-        for q in range(sources):
-            out_ref[k, 32 + 8 * q : 40 + 8 * q, :] = arrived_ref[q, 72:80, :]
+        for q, source in enumerate(order):
+            at = 32 + 8 * source
+            out_ref[k, at : at + 8, :] = arrived_ref[q, 72:80, :]
 
 
 def finish(
@@ -415,8 +461,10 @@
     tokens = hidden_states.shape[0]
     width = w_query.shape[1]
     positions_dev, heads = cache_keys.shape[1:3]
-    nears, fars, tps = (math.prod(lax.axis_size(a) for a in axes) for axes in (near, (far,), (tp,)))
+    nears, fars, tps = (math.prod(lax.axis_size(a) for a in axes) for axes in (near, far, (tp,)))
     chunk = tokens // nears
+    halves = lax.axis_size(half)
+    order = [(k % halves) * (fars // halves) + k // halves for k in range(fars)]
     terms = call(
         project,
         shape((tokens, (near_terms + 2) * width), bf16),
@@ -432,11 +480,11 @@
         terms.reshape(nears, chunk, -1), near, 0, 0, tiled=True
     )
     shared = call(
-        functools.partial(sum_near, width=width),
+        functools.partial(sum_near, width=width, order=order),
         shape((fars, chunk, far_terms * width + 128), bf16),
         [vmem],
     )(terms)
-    shared = lax.all_to_all(shared, far, 0, 0, tiled=True)
+    shared = lax.all_to_all(shared, listed, 0, 0, tiled=True)
     flat = (seqs, positions_dev * heads, 128)
     keys, values, keys_copy, values_copy, facts = call(
         stage,
@@ -483,8 +531,10 @@
         [vmem, vmem],
         scratch_shapes=[pltpu.VMEM((128, 128), f32)],
     )(part.reshape(nears, tps, 24, 128), row)
-    part = lax.all_to_all(part, far, 0, 0, tiled=True)
-    mixed = call(combine_far, shape((nears, 96, 128), bf16), [vmem] * 2)(part, head_gain[None])
+    part = lax.all_to_all(part, listed, 0, 0, tiled=True)
+    mixed = call(
+        functools.partial(combine_far, order=order), shape((nears, 96, 128), bf16), [vmem] * 2
+    )(part, head_gain[None])
     mixed = lax.all_to_all(mixed, near, 0, 0, tiled=True)
     own = w_output.T
     weights = [own]
@@ -514,9 +564,9 @@
 
 def solution(mesh):
     groups, shards, tps = (mesh.shape[a] for a in ("grp", "kv", "tp"))
-    split = (groups, shards // (near_chips * near_cores), near_chips, near_cores, tps)
-    finer = Mesh(mesh.devices.reshape(split), ("grp", far, chip, core, tp))
-    kv = (far, chip, core)
+    split = (groups, 2, shards // (2 * near_chips * near_cores), near_chips, near_cores, tps)
+    finer = Mesh(mesh.devices.reshape(split), ("grp", half, quarter, chip, core, tp))
+    kv = (half, quarter, chip, core)
     cache = P("grp", kv, tp, None)
     placed = (
         P("grp", kv),

time: 180 us -> 170 us (0.944)
  waiting for transfers between devices: 30.7 us -> 26.1 us
  Pallas kernels: 14.6 us -> 10.5 us
  starting transfers between devices: 56.6 us -> 54.3 us
    pallas_call x1, Pallas kernels: 5.84 us -> 1.72 us  [on_device(): call(attend, shape((nears, tps, 24, 128), bf16), [vmem] * 5, flops=100000...]
    all_to_all x1, waiting for transfers between devices: 25.2 us -> 21.5 us  [on_device(): shared = lax.all_to_all(shared, listed, 0, 0, tiled=True)]
where the time goes in v6:
time: 170 us; the launch traced here: 169 us
  blocking collectives  75.8 us (45%)
  starting transfers between devices  54.3 us (32%)
  waiting for transfers between devices  26.1 us (15%)
  Pallas kernels  10.5 us (6%)
  local copies, waits for them, and re-layouts  1.88 us (1%)
    all_to_all x1, starting transfers between devices, on_device(): shared = lax.all_to_all(shared, listed, 0, 0, tiled=True)  40.9 us
    all_to_all x1, blocking collectives, on_device(): part = lax.all_to_all(part, listed, 0, 0, tiled=True)  33.5 us
    all_to_all x1, waiting for transfers between devices, on_device(): shared = lax.all_to_all(shared, listed, 0, 0, tiled=True)  21.5 us
    all_to_all x1, blocking collectives, on_device(): lax.all_to_all(terms.reshape(nears, chunk, -1), near, 0, 0, tiled=True)  18.3 us
    all_to_all x1, blocking collectives, on_device(): lax.all_to_all(part.reshape(nears * tps, 24, 128), (*near, tp), 0, 0, til...  14.9 us
    all_to_all x1, blocking collectives, on_device(): query = lax.all_to_all(query, near, 0, 0, tiled=True).reshape(tokens, width)  9.12 us
    ppermute x3, starting transfers between devices, on_device(): weights.append(lax.ppermute(own, tp, ring))  8.07 us
    all_to_all x1, starting transfers between devices, on_device(): mixed = lax.all_to_all(mixed, near, 0, 0, tiled=True)  5.32 us
  transfers between devices with their start and end apart: 5, of which 3 were waited for; matrix products, arithmetic and copies ran while one was open for 0% of the time, Pallas kernels for 1%

profile of v6, /device:TPU:40, one launch (start us, length us, event | category | flops | bytes accessed | tf_op | source)
XLA Modules:
  0.0 169.4 jit_solution(8068285596029573327)
XLA Ops:
  0.6 2.0 %shard_map.158 = bf16[64,2048]{1,0:T(8,128)(2,1)} custom-call(bf16[64,64]{1,0:T(8,128)(2,1)} %hidden_ref.1, bf16[64,512]{1,0:T(8,128)(2,1)} %query_ref.1, bf16[64,512]{1,0:T(8,128)(2,1)} %key_ref.1, bf16[64,512]{1,0:T(8,128)(2,1)} %value_ref.1), custom_call_target="tpu_custom_call" | custom-call | flops 1000000 | bytes 1000000 | tf_op jit(solution)/shard_map/pallas_call | solution.py:468
  2.7 0.0 copy-start
  2.7 18.3 %all_to_all.30.arrived_ref = bf16[8,8,2048]{2,1,0:T(8,128)(2,1)S(1)} all-to-all(bf16[8,8,2048]{2,1,0:T(8,128)(2,1)} %bitcast.27), channel_id=1, replica_groups=mesh['grp'=2,'half'=2,'quarter'=4,'chip'=4,'core'=2,'tp'=4] {'chip','core'}, dimensions={0} | all-to-all | bytes 524288 | tf_op jit(solution)/shard_map/all_to_all | solution.py:479
  21.0 0.7 shard_map.159
  21.7 0.0 copy-start.7
  21.7 0.0 copy-start.8
  21.7 0.0 copy-start.9
  21.7 40.9 %all-to-all-start.1 = ((bf16[8,8,1152]{2,1,0:T(8,128)(2,1)}), bf16[8,8,1152]{2,1,0:T(8,128)(2,1)}, u32[]{:S(2)}, u32[]{:S(2)}) async-start(bf16[8,8,1152]{2,1,0:T(8,128)(2,1)} %shard_map.159), calls=%async_computation.1 | async-start | bytes 294912 | tf_op jit(solution)/shard_map/all_to_all | solution.py:487
  62.6 0.0 copy-start.3
  62.6 0.0 copy-start.4
  62.6 0.0 copy-start.5
  62.6 0.0 copy-start.6
  62.7 0.0 copy-done
  62.7 0.0 copy-done.7
  62.7 0.0 copy-done.8
  62.7 0.0 copy-done.9
  62.7 0.6 copy-done.3
  63.3 0.0 copy-done.4
  63.3 0.0 copy-done.5
  63.3 0.0 copy-done.6
  63.3 0.0 copy-start.1
  63.3 1.2 copy-done.1
  64.5 2.2 %shard_map.157 = (bf16[16,256,128]{2,1,0:T(8,128)(2,1)S(1)}, bf16[16,256,128]{2,1,0:T(8,128)(2,1)S(1)}, bf16[4,1024,128]{2,1,0:T(8,128)(2,1)}, bf16[4,1024,128]{2,1,0:T(8,128)(2,1)}, f32[656,128]{1,0:T(8,128)S(1)}) custom-call(s32[4]{0:T(128)S(1)} %copy-done.5, s32[4]{0:T(128)S(1)} %copy-done.6, s32[4,16]{1,0:T(4,128)S(1)} %copy-done.3, f32[4]{0:T(128)S(1)} %copy-done.7, ...), custom_call_target="tpu_custom_call" | custom-call | flops 1000000 | bytes 1000000 | tf_op jit(solution)/shard_map/pallas_call | solution.py:489
  66.8 21.5 %all-to-all-done.1.arrived_ref = bf16[8,8,1152]{2,1,0:T(8,128)(2,1)} async-done(((bf16[8,8,1152]{2,1,0:T(8,128)(2,1)}), bf16[8,8,1152]{2,1,0:T(8,128)(2,1)}, u32[]{:S(2)}, u32[]{:S(2)}) %all-to-all-start.1) | async-done | bytes 147488 | tf_op jit(solution)/shard_map/all_to_all | solution.py:487
  88.2 1.0 shard_map.160
  89.2 9.1 %all_to_all.31 = bf16[8,8,512]{2,1,0:T(8,128)(2,1)S(1)} all-to-all(bf16[8,8,512]{2,1,0:T(8,128)(2,1)S(1)} %get-tuple-element.11), channel_id=1, replica_groups=mesh['grp'=2,'half'=2,'quarter'=4,'chip'=4,'core'=2,'tp'=4] {'chip','core'}, dimensions={0} | all-to-all | bytes 131072 | tf_op jit(solution)/shard_map/all_to_all | solution.py:521
  98.4 1.7 %shard_map.161 = bf16[8,4,24,128]{3,2,1,0:T(8,128)(2,1)S(1)} custom-call(f32[656,128]{1,0:T(8,128)S(1)} %get-tuple-element.10.facts_ref, bf16[64,512]{1,0:T(8,128)(2,1)S(1)} %bitcast.16, bf16[8,128]{1,0:T(8,128)(2,1)S(1)} %get-tuple-element.12.row_ref, bf16[16,256,128]{2,1,0:T(8,128)(2,1)S(1)} %get-tuple-element.13.keys_ref, ...), custom_call_target="tpu_custom_call" | custom-call | flops 10000000 | bytes 1000000 | tf_op jit(solution)/shard_map/pallas_call | solution.py:522
  100.1 14.9 %all_to_all.32 = bf16[32,24,128]{2,1,0:T(8,128)(2,1)S(1)} all-to-all(bf16[32,24,128]{2,1,0:T(8,128)(2,1)S(1)} %bitcast.14), channel_id=1, replica_groups=mesh['grp'=2,'half'=2,'quarter'=4,'chip'=4,'core'=2,'tp'=4] {'chip','cor..., dimensions={0} | all-to-all | bytes 393216 | tf_op jit(solution)/shard_map/all_to_all | solution.py:525
  115.0 0.4 shard_map.162
  115.3 33.5 %all_to_all.33.arrived_ref = bf16[8,80,128]{2,1,0:T(8,128)(2,1)S(1)} all-to-all(bf16[8,80,128]{2,1,0:T(8,128)(2,1)S(1)} %shard_map.162), channel_id=1, replica_groups=mesh['grp'=2,'half'=2,'quarter'=4,'chip'=4,'core'=2,'tp'=4] {'quarter','..., dimensions={0} | all-to-all | bytes 327680 | tf_op jit(solution)/shard_map/all_to_all | solution.py:534
  148.8 1.1 shard_map.163
  149.9 0.0 copy-start.2
  149.9 5.3 %all-to-all-start.5 = ((bf16[8,96,128]{2,1,0:T(8,128)(2,1)}), bf16[8,96,128]{2,1,0:T(8,128)(2,1)S(1)}, u32[]{:S(2)}, u32[]{:S(2)}) async-start(bf16[8,96,128]{2,1,0:T(8,128)(2,1)} %shard_map.163), calls=%async_computation.5 | async-start | bytes 393216 | tf_op jit(solution)/shard_map/all_to_all | solution.py:538
  155.2 0.0 copy-done.2
  155.2 2.0 %collective-permute-start.2 = (bf16[64,512]{1,0:T(8,128)(2,1)S(1)}, bf16[64,512]{1,0:T(8,128)(2,1)S(1)}, u32[]{:S(2)}, u32[]{:S(2)}) collective-permute-start(bf16[64,512]{1,0:T(8,128)(2,1)S(1)} %bitcast.17), channel_id=1, source_target_pairs={{0,3},{1,0},{2,1},{3,2},{4,7},{5,4},{6,5},{7,6},{8,11},{9,8},{10,9... | collective-permute-start | bytes 196616 | tf_op jit(solution)/shard_map/ppermute | solution.py:543
  157.2 2.8 %collective-permute-start.1 = (bf16[64,512]{1,0:T(8,128)(2,1)S(1)}, bf16[64,512]{1,0:T(8,128)(2,1)S(1)}, u32[]{:S(2)}, u32[]{:S(2)}) collective-permute-start(bf16[64,512]{1,0:T(8,128)(2,1)S(1)} %bitcast.18), channel_id=1, source_target_pairs={{0,2},{1,3},{2,0},{3,1},{4,6},{5,7},{6,4},{7,5},{8,10},{9,11},{10,... | collective-permute-start | bytes 196616 | tf_op jit(solution)/shard_map/ppermute | solution.py:543
  160.0 3.3 %collective-permute-start = (bf16[64,512]{1,0:T(8,128)(2,1)S(1)}, bf16[64,512]{1,0:T(8,128)(2,1)S(1)}, u32[]{:S(2)}, u32[]{:S(2)}) collective-permute-start(bf16[64,512]{1,0:T(8,128)(2,1)S(1)} %bitcast.19), channel_id=1, source_target_pairs={{0,1},{1,2},{2,3},{3,0},{4,5},{5,6},{6,7},{7,4},{8,9},{9,10},{10,1... | collective-permute-start | bytes 196616 | tf_op jit(solution)/shard_map/ppermute | solution.py:543
  163.3 0.0 collective-permute-done.2.third_ref
  163.3 1.8 %collective-permute-done.1.second_ref = bf16[64,512]{1,0:T(8,128)(2,1)S(1)} collective-permute-done((bf16[64,512]{1,0:T(8,128)(2,1)S(1)}, bf16[64,512]{1,0:T(8,128)(2,1)S(1)}, u32[]{:S(2)}, u32[]{:S(2)}) %collective-permute-start.1) | collective-permute-done | bytes 65568 | tf_op jit(solution)/shard_map/ppermute | solution.py:543
  165.1 2.9 %collective-permute-done.first_ref = bf16[64,512]{1,0:T(8,128)(2,1)S(1)} collective-permute-done((bf16[64,512]{1,0:T(8,128)(2,1)S(1)}, bf16[64,512]{1,0:T(8,128)(2,1)S(1)}, u32[]{:S(2)}, u32[]{:S(2)}) %collective-permute-start) | collective-permute-done | bytes 65568 | tf_op jit(solution)/shard_map/ppermute | solution.py:543
  168.0 0.0 all-to-all-done.5.arrived_ref
  168.0 1.4 shard_map.164
Async XLA Ops:
  2.7 60.0 %copy-start = (bf16[4,256,4,128]{3,2,1,0:T(4,128)(2,1)S(1)}, bf16[4,256,4,128]{3,2,1,0:T(4,128)(2,1)}, u32[]{:S(2)}) copy-start(bf16[4,256,4,128]{3,2,1,0:T(4,128)(2,1)} %param.23) | copy-start | bytes 3145732
  21.7 40.9 %copy-start.7 = (f32[4]{0:T(128)S(1)}, f32[4]{0:T(128)}, u32[]{:S(2)}) copy-start(f32[4]{0:T(128)} %lambda_ref.1) | copy-start | bytes 52
  21.7 40.9 %copy-start.8 = (f32[64]{0:T(128)S(1)}, f32[64]{0:T(128)}, u32[]{:S(2)}) copy-start(f32[64]{0:T(128)} %param.18) | copy-start | bytes 772
  21.7 41.0 %copy-start.9 = (f32[64]{0:T(128)S(1)}, f32[64]{0:T(128)}, u32[]{:S(2)}) copy-start(f32[64]{0:T(128)} %param.19) | copy-start | bytes 772
  21.7 66.5 %all-to-all-start.1 = ((bf16[8,8,1152]{2,1,0:T(8,128)(2,1)}), bf16[8,8,1152]{2,1,0:T(8,128)(2,1)}, u32[]{:S(2)}, u32[]{:S(2)}) async-start(bf16[8,8,1152]{2,1,0:T(8,128)(2,1)} %shard_map.159), calls=%async_computation.1 | async-start | bytes 294912 | tf_op jit(solution)/shard_map/all_to_all | solution.py:487
  62.6 0.7 copy-start.3
  62.6 0.7 copy-start.4
  62.6 0.7 copy-start.5
  62.6 0.7 copy-start.6
  63.3 1.2 copy-start.1
  149.9 5.3 %copy-start.2 = (bf16[512,64]{0,1:T(8,128)(2,1)S(1)}, bf16[512,64]{0,1:T(8,128)(2,1)}, u32[]{:S(2)}) copy-start(bf16[512,64]{0,1:T(8,128)(2,1)} %param.22) | copy-start | bytes 196612
  149.9 18.1 %all-to-all-start.5 = ((bf16[8,96,128]{2,1,0:T(8,128)(2,1)}), bf16[8,96,128]{2,1,0:T(8,128)(2,1)S(1)}, u32[]{:S(2)}, u32[]{:S(2)}) async-start(bf16[8,96,128]{2,1,0:T(8,128)(2,1)} %shard_map.163), calls=%async_computation.5 | async-start | bytes 393216 | tf_op jit(solution)/shard_map/all_to_all | solution.py:538
  155.2 8.1 %collective-permute-start.2 = (bf16[64,512]{1,0:T(8,128)(2,1)S(1)}, bf16[64,512]{1,0:T(8,128)(2,1)S(1)}, u32[]{:S(2)}, u32[]{:S(2)}) collective-permute-start(bf16[64,512]{1,0:T(8,128)(2,1)S(1)} %bitcast.17), channel_id=1, source_target_pairs={{0,3},{1,0},{2,1},{3,2},{4,7},{5,4},{6,5},{7,6},{8,11},{9,8},{10,9... | collective-permute-start | bytes 196616 | tf_op jit(solution)/shard_map/ppermute | solution.py:543
  157.2 7.9 %collective-permute-start.1 = (bf16[64,512]{1,0:T(8,128)(2,1)S(1)}, bf16[64,512]{1,0:T(8,128)(2,1)S(1)}, u32[]{:S(2)}, u32[]{:S(2)}) collective-permute-start(bf16[64,512]{1,0:T(8,128)(2,1)S(1)} %bitcast.18), channel_id=1, source_target_pairs={{0,2},{1,3},{2,0},{3,1},{4,6},{5,7},{6,4},{7,5},{8,10},{9,11},{10,... | collective-permute-start | bytes 196616 | tf_op jit(solution)/shard_map/ppermute | solution.py:543
  160.0 8.0 %collective-permute-start = (bf16[64,512]{1,0:T(8,128)(2,1)S(1)}, bf16[64,512]{1,0:T(8,128)(2,1)S(1)}, u32[]{:S(2)}, u32[]{:S(2)}) collective-permute-start(bf16[64,512]{1,0:T(8,128)(2,1)S(1)} %bitcast.19), channel_id=1, source_target_pairs={{0,1},{1,2},{2,3},{3,0},{4,5},{5,6},{6,7},{7,4},{8,9},{9,10},{10,1... | collective-permute-start | bytes 196616 | tf_op jit(solution)/shard_map/ppermute | solution.py:543

commit v7 on v6

--- a/solution.py
+++ b/solution.py
@@ -17,9 +17,10 @@
 interpreted = False
 near_chips = 4
 near_cores = 2
-half, quarter, chip, core, tp = "half", "quarter", "chip", "core", "tp"
-far = (half, quarter)
-listed = (quarter, half)
+half, quarter, eighth, chip, core, tp = "half", "quarter", "eighth", "chip", "core", "tp"
+far = (half, quarter, eighth)
+first_list = (eighth, quarter, half)
+second_list = (eighth, quarter, half)
 near = (chip, core)
 near_terms = 2
 far_terms = 2
@@ -32,6 +33,19 @@
 
 def near_place():
     return lax.axis_index(chip) * lax.axis_size(core) + lax.axis_index(core)
+
+
+def blocks_of(axes):
+    blocks = []
+    for k in range(math.prod(lax.axis_size(a) for a in axes)):
+        at = {}
+        for a in reversed(axes):
+            k, at[a] = divmod(k, lax.axis_size(a))
+        block = 0
+        for a in far:
+            block = block * lax.axis_size(a) + at[a]
+        blocks.append(block)
+    return blocks
 
 
 def iota(shape, dim):
@@ -463,8 +477,7 @@
     positions_dev, heads = cache_keys.shape[1:3]
     nears, fars, tps = (math.prod(lax.axis_size(a) for a in axes) for axes in (near, far, (tp,)))
     chunk = tokens // nears
-    halves = lax.axis_size(half)
-    order = [(k % halves) * (fars // halves) + k // halves for k in range(fars)]
+    first_order, second_order = (blocks_of(axes) for axes in (first_list, second_list))
     terms = call(
         project,
         shape((tokens, (near_terms + 2) * width), bf16),
@@ -480,11 +493,11 @@
         terms.reshape(nears, chunk, -1), near, 0, 0, tiled=True
     )
     shared = call(
-        functools.partial(sum_near, width=width, order=order),
+        functools.partial(sum_near, width=width, order=first_order),
         shape((fars, chunk, far_terms * width + 128), bf16),
         [vmem],
     )(terms)
-    shared = lax.all_to_all(shared, listed, 0, 0, tiled=True)
+    shared = lax.all_to_all(shared, first_list, 0, 0, tiled=True)
     flat = (seqs, positions_dev * heads, 128)
     keys, values, keys_copy, values_copy, facts = call(
         stage,
@@ -531,9 +544,11 @@
         [vmem, vmem],
         scratch_shapes=[pltpu.VMEM((128, 128), f32)],
     )(part.reshape(nears, tps, 24, 128), row)
-    part = lax.all_to_all(part, listed, 0, 0, tiled=True)
+    part = lax.all_to_all(part, second_list, 0, 0, tiled=True)
     mixed = call(
-        functools.partial(combine_far, order=order), shape((nears, 96, 128), bf16), [vmem] * 2
+        functools.partial(combine_far, order=second_order),
+        shape((nears, 96, 128), bf16),
+        [vmem] * 2,
     )(part, head_gain[None])
     mixed = lax.all_to_all(mixed, near, 0, 0, tiled=True)
     own = w_output.T
@@ -564,9 +579,9 @@
 
 def solution(mesh):
     groups, shards, tps = (mesh.shape[a] for a in ("grp", "kv", "tp"))
-    split = (groups, 2, shards // (2 * near_chips * near_cores), near_chips, near_cores, tps)
-    finer = Mesh(mesh.devices.reshape(split), ("grp", half, quarter, chip, core, tp))
-    kv = (half, quarter, chip, core)
+    split = (groups, 2, 2, shards // (4 * near_chips * near_cores), near_chips, near_cores, tps)
+    finer = Mesh(mesh.devices.reshape(split), ("grp", half, quarter, eighth, chip, core, tp))
+    kv = (half, quarter, eighth, chip, core)
     cache = P("grp", kv, tp, None)
     placed = (
         P("grp", kv),

time: 170 us -> 171 us (level)
    all_to_all x1, blocking collectives: 9.12 us -> 11.5 us  [on_device(): query = lax.all_to_all(query, near, 0, 0, tiled=True).reshape(tokens, width)]
    all_to_all x1, blocking collectives: 33.5 us -> 31.2 us  [on_device(): part = lax.all_to_all(part, second_list, 0, 0, tiled=True)]
    ppermute x3, starting transfers between devices: 8.07 us -> 10.3 us  [on_device(): weights.append(lax.ppermute(own, tp, ring))]
where the time goes in v7:
time: 171 us; the launch traced here: 170 us
  blocking collectives  75.9 us (44%)
  starting transfers between devices  55.4 us (32%)
  waiting for transfers between devices  25.5 us (15%)
  Pallas kernels  10.5 us (6%)
  local copies, waits for them, and re-layouts  1.88 us (1%)
    all_to_all x1, starting transfers between devices, on_device(): shared = lax.all_to_all(shared, first_list, 0, 0, tiled=True)  40.9 us
    all_to_all x1, blocking collectives, on_device(): part = lax.all_to_all(part, second_list, 0, 0, tiled=True)  31.2 us
    all_to_all x1, waiting for transfers between devices, on_device(): shared = lax.all_to_all(shared, first_list, 0, 0, tiled=True)  21.4 us
    all_to_all x1, blocking collectives, on_device(): lax.all_to_all(terms.reshape(nears, chunk, -1), near, 0, 0, tiled=True)  18.3 us
    all_to_all x1, blocking collectives, on_device(): lax.all_to_all(part.reshape(nears * tps, 24, 128), (*near, tp), 0, 0, til...  14.9 us
    all_to_all x1, blocking collectives, on_device(): query = lax.all_to_all(query, near, 0, 0, tiled=True).reshape(tokens, width)  11.5 us
    ppermute x3, starting transfers between devices, on_device(): weights.append(lax.ppermute(own, tp, ring))  10.3 us
    all_to_all x1, starting transfers between devices, on_device(): mixed = lax.all_to_all(mixed, near, 0, 0, tiled=True)  4.23 us
  transfers between devices with their start and end apart: 5, of which 3 were waited for; matrix products, arithmetic and copies ran while one was open for 0% of the time, Pallas kernels for 1%

profile of v7, /device:TPU:40, one launch (start us, length us, event | category | flops | bytes accessed | tf_op | source)
XLA Modules:
  0.0 169.9 jit_solution(12188433693186302305)
XLA Ops:
  0.6 2.0 %shard_map.158 = bf16[64,2048]{1,0:T(8,128)(2,1)} custom-call(bf16[64,64]{1,0:T(8,128)(2,1)} %hidden_ref.1, bf16[64,512]{1,0:T(8,128)(2,1)} %query_ref.1, bf16[64,512]{1,0:T(8,128)(2,1)} %key_ref.1, bf16[64,512]{1,0:T(8,128)(2,1)} %value_ref.1), custom_call_target="tpu_custom_call" | custom-call | flops 1000000 | bytes 1000000 | tf_op jit(solution)/shard_map/pallas_call | solution.py:481
  2.7 0.0 copy-start
  2.7 18.3 %all_to_all.30.arrived_ref = bf16[8,8,2048]{2,1,0:T(8,128)(2,1)S(1)} all-to-all(bf16[8,8,2048]{2,1,0:T(8,128)(2,1)} %bitcast.27), channel_id=1, replica_groups=mesh['grp'=2,'half'=2,'quarter'=2,'eighth'=2,'chip'=4,'core'=2,'tp'=4] {..., dimensions={0} | all-to-all | bytes 524288 | tf_op jit(solution)/shard_map/all_to_all | solution.py:492
  21.0 0.7 shard_map.159
  21.7 0.0 copy-start.7
  21.7 0.0 copy-start.8
  21.7 0.0 copy-start.9
  21.7 40.9 %all-to-all-start.1 = ((bf16[8,8,1152]{2,1,0:T(8,128)(2,1)}), bf16[8,8,1152]{2,1,0:T(8,128)(2,1)}, u32[]{:S(2)}, u32[]{:S(2)}) async-start(bf16[8,8,1152]{2,1,0:T(8,128)(2,1)} %shard_map.159), calls=%async_computation.1 | async-start | bytes 294912 | tf_op jit(solution)/shard_map/all_to_all | solution.py:500
  62.6 0.0 copy-start.3
  62.6 0.0 copy-start.4
  62.6 0.0 copy-start.5
  62.6 0.0 copy-start.6
  62.7 0.0 copy-done
  62.7 0.0 copy-done.7
  62.7 0.0 copy-done.8
  62.7 0.0 copy-done.9
  62.7 0.6 copy-done.3
  63.3 0.0 copy-done.4
  63.3 0.0 copy-done.5
  63.3 0.0 copy-done.6
  63.3 0.0 copy-start.1
  63.3 1.2 copy-done.1
  64.5 2.2 %shard_map.157 = (bf16[16,256,128]{2,1,0:T(8,128)(2,1)S(1)}, bf16[16,256,128]{2,1,0:T(8,128)(2,1)S(1)}, bf16[4,1024,128]{2,1,0:T(8,128)(2,1)}, bf16[4,1024,128]{2,1,0:T(8,128)(2,1)}, f32[656,128]{1,0:T(8,128)S(1)}) custom-call(s32[4]{0:T(128)S(1)} %copy-done.5, s32[4]{0:T(128)S(1)} %copy-done.6, s32[4,16]{1,0:T(4,128)S(1)} %copy-done.3, f32[4]{0:T(128)S(1)} %copy-done.7, ...), custom_call_target="tpu_custom_call" | custom-call | flops 1000000 | bytes 1000000 | tf_op jit(solution)/shard_map/pallas_call | solution.py:502
  66.8 21.4 %all-to-all-done.1.arrived_ref = bf16[8,8,1152]{2,1,0:T(8,128)(2,1)} async-done(((bf16[8,8,1152]{2,1,0:T(8,128)(2,1)}), bf16[8,8,1152]{2,1,0:T(8,128)(2,1)}, u32[]{:S(2)}, u32[]{:S(2)}) %all-to-all-start.1) | async-done | bytes 147488 | tf_op jit(solution)/shard_map/all_to_all | solution.py:500
  88.2 1.0 shard_map.160
  89.2 11.5 %all_to_all.31 = bf16[8,8,512]{2,1,0:T(8,128)(2,1)S(1)} all-to-all(bf16[8,8,512]{2,1,0:T(8,128)(2,1)S(1)} %get-tuple-element.11), channel_id=1, replica_groups=mesh['grp'=2,'half'=2,'quarter'=2,'eighth'=2,'chip'=4,'core'=2,'tp'=4] {..., dimensions={0} | all-to-all | bytes 131072 | tf_op jit(solution)/shard_map/all_to_all | solution.py:534
  100.7 1.7 %shard_map.161 = bf16[8,4,24,128]{3,2,1,0:T(8,128)(2,1)S(1)} custom-call(f32[656,128]{1,0:T(8,128)S(1)} %get-tuple-element.10.facts_ref, bf16[64,512]{1,0:T(8,128)(2,1)S(1)} %bitcast.16, bf16[8,128]{1,0:T(8,128)(2,1)S(1)} %get-tuple-element.12.row_ref, bf16[16,256,128]{2,1,0:T(8,128)(2,1)S(1)} %get-tuple-element.13.keys_ref, ...), custom_call_target="tpu_custom_call" | custom-call | flops 10000000 | bytes 1000000 | tf_op jit(solution)/shard_map/pallas_call | solution.py:535
  102.4 14.9 %all_to_all.32 = bf16[32,24,128]{2,1,0:T(8,128)(2,1)S(1)} all-to-all(bf16[32,24,128]{2,1,0:T(8,128)(2,1)S(1)} %bitcast.14), channel_id=1, replica_groups=mesh['grp'=2,'half'=2,'quarter'=2,'eighth'=2,'chip'=4,'core'=2,'tp'=4] {..., dimensions={0} | all-to-all | bytes 393216 | tf_op jit(solution)/shard_map/all_to_all | solution.py:538
  117.3 0.4 shard_map.162
  117.7 31.2 %all_to_all.33.arrived_ref = bf16[8,80,128]{2,1,0:T(8,128)(2,1)S(1)} all-to-all(bf16[8,80,128]{2,1,0:T(8,128)(2,1)S(1)} %shard_map.162), channel_id=1, replica_groups=mesh['grp'=2,'half'=2,'quarter'=2,'eighth'=2,'chip'=4,'core'=2,'tp'=4] {..., dimensions={0} | all-to-all | bytes 327680 | tf_op jit(solution)/shard_map/all_to_all | solution.py:547
  148.8 1.1 shard_map.163
  149.9 0.0 copy-start.2
  149.9 4.2 %all-to-all-start.5 = ((bf16[8,96,128]{2,1,0:T(8,128)(2,1)}), bf16[8,96,128]{2,1,0:T(8,128)(2,1)S(1)}, u32[]{:S(2)}, u32[]{:S(2)}) async-start(bf16[8,96,128]{2,1,0:T(8,128)(2,1)} %shard_map.163), calls=%async_computation.5 | async-start | bytes 393216 | tf_op jit(solution)/shard_map/all_to_all | solution.py:553
  154.2 0.0 copy-done.2
  154.2 3.2 %collective-permute-start.2 = (bf16[64,512]{1,0:T(8,128)(2,1)S(1)}, bf16[64,512]{1,0:T(8,128)(2,1)S(1)}, u32[]{:S(2)}, u32[]{:S(2)}) collective-permute-start(bf16[64,512]{1,0:T(8,128)(2,1)S(1)} %bitcast.17), channel_id=1, source_target_pairs={{0,3},{1,0},{2,1},{3,2},{4,7},{5,4},{6,5},{7,6},{8,11},{9,8},{10,9... | collective-permute-start | bytes 196616 | tf_op jit(solution)/shard_map/ppermute | solution.py:558
  157.3 3.8 %collective-permute-start.1 = (bf16[64,512]{1,0:T(8,128)(2,1)S(1)}, bf16[64,512]{1,0:T(8,128)(2,1)S(1)}, u32[]{:S(2)}, u32[]{:S(2)}) collective-permute-start(bf16[64,512]{1,0:T(8,128)(2,1)S(1)} %bitcast.18), channel_id=1, source_target_pairs={{0,2},{1,3},{2,0},{3,1},{4,6},{5,7},{6,4},{7,5},{8,10},{9,11},{10,... | collective-permute-start | bytes 196616 | tf_op jit(solution)/shard_map/ppermute | solution.py:558
  161.1 3.3 %collective-permute-start = (bf16[64,512]{1,0:T(8,128)(2,1)S(1)}, bf16[64,512]{1,0:T(8,128)(2,1)S(1)}, u32[]{:S(2)}, u32[]{:S(2)}) collective-permute-start(bf16[64,512]{1,0:T(8,128)(2,1)S(1)} %bitcast.19), channel_id=1, source_target_pairs={{0,1},{1,2},{2,3},{3,0},{4,5},{5,6},{6,7},{7,4},{8,9},{9,10},{10,1... | collective-permute-start | bytes 196616 | tf_op jit(solution)/shard_map/ppermute | solution.py:558
  164.5 0.0 collective-permute-done.2.third_ref
  164.5 0.6 collective-permute-done.1.second_ref
  165.0 3.5 %collective-permute-done.first_ref = bf16[64,512]{1,0:T(8,128)(2,1)S(1)} collective-permute-done((bf16[64,512]{1,0:T(8,128)(2,1)S(1)}, bf16[64,512]{1,0:T(8,128)(2,1)S(1)}, u32[]{:S(2)}, u32[]{:S(2)}) %collective-permute-start) | collective-permute-done | bytes 65568 | tf_op jit(solution)/shard_map/ppermute | solution.py:558
  168.5 0.0 all-to-all-done.5.arrived_ref
  168.5 1.4 shard_map.164
Async XLA Ops:
  2.7 60.0 %copy-start = (bf16[4,256,4,128]{3,2,1,0:T(4,128)(2,1)S(1)}, bf16[4,256,4,128]{3,2,1,0:T(4,128)(2,1)}, u32[]{:S(2)}) copy-start(bf16[4,256,4,128]{3,2,1,0:T(4,128)(2,1)} %param.23) | copy-start | bytes 3145732
  21.7 40.9 %copy-start.7 = (f32[4]{0:T(128)S(1)}, f32[4]{0:T(128)}, u32[]{:S(2)}) copy-start(f32[4]{0:T(128)} %lambda_ref.1) | copy-start | bytes 52
  21.7 40.9 %copy-start.8 = (f32[64]{0:T(128)S(1)}, f32[64]{0:T(128)}, u32[]{:S(2)}) copy-start(f32[64]{0:T(128)} %param.18) | copy-start | bytes 772
  21.7 41.0 %copy-start.9 = (f32[64]{0:T(128)S(1)}, f32[64]{0:T(128)}, u32[]{:S(2)}) copy-start(f32[64]{0:T(128)} %param.19) | copy-start | bytes 772
  21.7 66.4 %all-to-all-start.1 = ((bf16[8,8,1152]{2,1,0:T(8,128)(2,1)}), bf16[8,8,1152]{2,1,0:T(8,128)(2,1)}, u32[]{:S(2)}, u32[]{:S(2)}) async-start(bf16[8,8,1152]{2,1,0:T(8,128)(2,1)} %shard_map.159), calls=%async_computation.1 | async-start | bytes 294912 | tf_op jit(solution)/shard_map/all_to_all | solution.py:500
  62.6 0.7 copy-start.3
  62.6 0.7 copy-start.4
  62.6 0.7 copy-start.5
  62.6 0.7 copy-start.6
  63.3 1.2 copy-start.1
  149.9 4.2 %copy-start.2 = (bf16[512,64]{0,1:T(8,128)(2,1)S(1)}, bf16[512,64]{0,1:T(8,128)(2,1)}, u32[]{:S(2)}) copy-start(bf16[512,64]{0,1:T(8,128)(2,1)} %param.22) | copy-start | bytes 196612
  149.9 18.6 %all-to-all-start.5 = ((bf16[8,96,128]{2,1,0:T(8,128)(2,1)}), bf16[8,96,128]{2,1,0:T(8,128)(2,1)S(1)}, u32[]{:S(2)}, u32[]{:S(2)}) async-start(bf16[8,96,128]{2,1,0:T(8,128)(2,1)} %shard_map.163), calls=%async_computation.5 | async-start | bytes 393216 | tf_op jit(solution)/shard_map/all_to_all | solution.py:553
  154.2 10.3 %collective-permute-start.2 = (bf16[64,512]{1,0:T(8,128)(2,1)S(1)}, bf16[64,512]{1,0:T(8,128)(2,1)S(1)}, u32[]{:S(2)}, u32[]{:S(2)}) collective-permute-start(bf16[64,512]{1,0:T(8,128)(2,1)S(1)} %bitcast.17), channel_id=1, source_target_pairs={{0,3},{1,0},{2,1},{3,2},{4,7},{5,4},{6,5},{7,6},{8,11},{9,8},{10,9... | collective-permute-start | bytes 196616 | tf_op jit(solution)/shard_map/ppermute | solution.py:558
  157.3 7.7 %collective-permute-start.1 = (bf16[64,512]{1,0:T(8,128)(2,1)S(1)}, bf16[64,512]{1,0:T(8,128)(2,1)S(1)}, u32[]{:S(2)}, u32[]{:S(2)}) collective-permute-start(bf16[64,512]{1,0:T(8,128)(2,1)S(1)} %bitcast.18), channel_id=1, source_target_pairs={{0,2},{1,3},{2,0},{3,1},{4,6},{5,7},{6,4},{7,5},{8,10},{9,11},{10,... | collective-permute-start | bytes 196616 | tf_op jit(solution)/shard_map/ppermute | solution.py:558
  161.1 7.4 %collective-permute-start = (bf16[64,512]{1,0:T(8,128)(2,1)S(1)}, bf16[64,512]{1,0:T(8,128)(2,1)S(1)}, u32[]{:S(2)}, u32[]{:S(2)}) collective-permute-start(bf16[64,512]{1,0:T(8,128)(2,1)S(1)} %bitcast.19), channel_id=1, source_target_pairs={{0,1},{1,2},{2,3},{3,0},{4,5},{5,6},{6,7},{7,4},{8,9},{9,10},{10,1... | collective-permute-start | bytes 196616 | tf_op jit(solution)/shard_map/ppermute | solution.py:558
